TPU v7x, 32 devices: a whole 2x2x4 slice. The times are simulated.
32 devices in a mesh: sp: 8 (over z, x), tp: 4 (over y, core).
Axes of the slice: x: 2, y: 2, z: 4, core: 2. Of those that a mesh axis runs over, the one named last changes fastest.
Arguments:
- query_wide: bfloat16 [1024, 1536], P('sp', 'tp'), may hold values from -600 to 600
- query_narrow: bfloat16 [1024, 1024], P('sp', 'tp'), may hold values from -600 to 600
- latent: bfloat16 [1024, 512], P('sp'), may hold values from -6 to 6
- rope_key: bfloat16 [1024, 64], P('sp'), may hold values from -6 to 6
- latent_norm_weight: float32 [512], replicated, may hold values from 0.1 to 1.9
- broad_key_lift: bfloat16 [512, 1024], P(None, 'tp'), may hold values from -0.25 to 0.25
- broad_value_lift: bfloat16 [512, 1024], P(None, 'tp'), may hold values from -0.25 to 0.25
- slim_key_lift: bfloat16 [512, 512], P(None, 'tp'), may hold values from -0.25 to 0.25
- slim_value_lift: bfloat16 [512, 512], P(None, 'tp'), may hold values from -0.25 to 0.25
- out_wide: bfloat16 [1024, 2048], P('tp'), may hold values from -0.4375 to 0.4375
- out_narrow: bfloat16 [512, 2048], P('tp'), may hold values from -0.4375 to 0.4375
- resid: bfloat16 [1024, 2048], P('sp'), may hold values from -20 to 20
- ffn_gain: float32 [2048], replicated, may hold values from 0.1 to 1.9
- group_route: int32 [1024], P('sp'), may hold values from 0 to 7, as said below
- expert_pair: int32 [1024, 2], P('sp'), may hold values from 0 to 3, all different within a row
- group_prob: float32 [1024], P('sp'), may hold values from 0.2 to 1
- expert_prob: float32 [1024, 2], P('sp'), may hold values from 0.05 to 1
- gate_weight: bfloat16 [8, 4, 2048, 512], P('sp', None, None, 'tp'), may hold values from -0.125 to 0.125
- up_weight: bfloat16 [8, 4, 2048, 512], P('sp', None, None, 'tp'), may hold values from -0.125 to 0.125
- down_weight: bfloat16 [8, 4, 512, 2048], P('sp', None, 'tp'), may hold values from -0.25 to 0.25
Outputs:
- mixed: bfloat16 [1024, 2048], P('sp', 'tp')
Inputs may be any that keep to these rules, and one draw needn't show every extreme that they name: `group_route`: of the 128 tokens of one index of sp at most 32 name one group; in every draw one group is named by exactly 32 tokens of every index of sp, and every index of sp names one more group exactly 32 times. `expert_pair`: A token's two experts are different.
All inputs are finite; a program needn't handle non-finite values.
Results may differ from a plain program's by a relative error of at most 0.017.
Values may be sent and summed in bfloat16 or wider, within the bound.
No kernel may reach another device: no remote copies, remote signals or barrier semaphores. Data moves between devices by JAX's collectives and lax.ppermute only.
A program may use at most 128 MiB of HBM per device.

v0:
```python
import functools

import jax
import jax.numpy as jnp
from jax import lax
from jax.experimental import pallas as pl
from jax.experimental.pallas import tpu as pltpu
from jax.sharding import PartitionSpec as P


PLAIN_WIDTH_WIDE = 128
PLAIN_WIDTH_SLIM = 64
ROPE = 64
VALUE_WIDTH_WIDE = 128
VALUE_WIDTH_SLIM = 64
EPG = 4
LANES = 128

ROPE_BASE = 10000.0
EPSILON = 1e-06
MASKED = -1e30


F32 = jnp.float32
BF16 = jnp.bfloat16
VMEM = pl.BlockSpec(memory_space=pltpu.VMEM)
HBM = pl.BlockSpec(memory_space=pltpu.HBM)


def angles(positions, width):
    frequency = 1.0 / ROPE_BASE ** (jnp.arange(0, width, 2).astype(F32) / width)
    return positions.astype(F32)[:, None] * frequency[None, :]


def turn(values, cosine, sine, axis):
    first_half, second = jnp.split(values, 2, axis=axis)
    return jnp.concatenate(
        [first_half * cosine - second * sine, second * cosine + first_half * sine], axis=axis
    )


def exchange(values, axis, mask):
    size = lax.axis_size(axis)
    return lax.ppermute(values, axis, [(i, i ^ mask) for i in range(size)])


def dot(a, b):
    return jnp.dot(a, b, preferred_element_type=F32)


def dot_t(a, b):
    return lax.dot_general(a, b, (((1,), (1,)), ((), ())), preferred_element_type=F32)


def iota(shape, dim):
    return lax.broadcasted_iota(jnp.int32, shape, dim)


def prefix_count(rows):
    size = rows.shape[1]
    upto = (iota((size, size), 0) <= iota((size, size), 1)).astype(BF16)
    return dot(rows.astype(BF16), upto)


def pack_kernel(
    cos_ref, sin_ref, latent_ref, rope_ref, gain_ref, route_ref, pair_ref, group_ref, prob_ref,
    half_ref, rest_ref,
):
    rank = latent_ref.shape[1]
    half = half_ref.shape[0]
    tokens = latent_ref.shape[0]
    odd = (lax.axis_index("tp") & 1) == 1
    widened = latent_ref[...].astype(F32)
    scale = lax.rsqrt(jnp.mean(widened * widened, axis=-1, keepdims=True) + EPSILON)
    normed = (widened * scale * gain_ref[...]).astype(BF16)
    turned = turn(rope_ref[...].astype(F32), cos_ref[...], sin_ref[...], 0)
    shares = group_ref[...] * prob_ref[...] / jnp.sum(prob_ref[...], axis=0, keepdims=True)
    rows = iota((LANES - ROPE, tokens), 0)
    meta = jnp.where(rows == EPG, route_ref[...].astype(F32), 0.0)
    for expert in range(EPG):
        chosen = jnp.sum(jnp.where(pair_ref[...] == expert, shares, 0.0), axis=0, keepdims=True)
        meta = jnp.where(rows == expert, chosen, meta)
    tail = jnp.concatenate([turned, meta], axis=0).T.astype(BF16)
    half_ref[:, :rank] = jnp.where(odd, normed[half:], normed[:half])
    half_ref[:, rank:] = jnp.where(odd, tail[half:], tail[:half])
    rest_ref[:, :rank] = jnp.where(odd, normed[:half], normed[half:])
    rest_ref[:, rank:] = jnp.where(odd, tail[:half], tail[half:])


def query_kernel(cos_ref, sin_ref, wide_ref, slim_ref, out_ref):
    tokens = wide_ref.shape[0]
    heads_w = wide_ref.shape[1] // (PLAIN_WIDTH_WIDE + ROPE)
    heads_n = slim_ref.shape[1] // (PLAIN_WIDTH_SLIM + ROPE)
    cosine, sine = cos_ref[...], sin_ref[...]
    spare = jnp.zeros((tokens, LANES - ROPE), F32)
    for h in range(heads_w + heads_n):
        wide = h < heads_w
        plain = PLAIN_WIDTH_WIDE if wide else PLAIN_WIDTH_SLIM
        start = (h if wide else h - heads_w) * (plain + ROPE)
        part = (wide_ref if wide else slim_ref)[:, start : start + plain + ROPE].astype(F32)
        pieces = [part[:, :plain], turn(part[:, plain:], cosine, sine, 1), spare]
        if not wide:
            before = (h - heads_w) * plain
            after = heads_n * plain - before - plain
            if before:
                pieces = [jnp.zeros((tokens, before), F32)] + pieces
            if after:
                pieces = pieces[:-2] + [jnp.zeros((tokens, after), F32)] + pieces[-2:]
        out_ref[h] = jnp.concatenate(pieces, axis=1).astype(BF16)


def pieces_of(refs):
    return [
        piece
        for ref in refs
        for piece in ([ref[...]] if len(ref.shape) == 2 else [ref[i] for i in range(ref.shape[0])])
    ]


def attend_body(q_ref, stacks, kw_ref, vw_ref, kn_ref, vn_ref, state, masks):
    count = len(stacks) // 2
    mine, other = pieces_of(stacks[:count]), pieces_of(stacks[count:])
    heads_w = kw_ref.shape[1] // PLAIN_WIDTH_WIDE
    heads_n = kn_ref.shape[1] // PLAIN_WIDTH_SLIM
    half = mine[0].shape[0]
    tokens = q_ref.shape[1]
    rank = kw_ref.shape[0]
    place = lax.axis_index("sp")
    core = lax.axis_index("tp") & 1
    shift = half.bit_length() - 1
    step = 5
    for start in range(0, len(mine), step):
        group = mine[start : start + step]
        rows = len(group) * half
        lat = jnp.concatenate(group + other[start : start + step], axis=0)
        flat = lat[:, :rank]
        rot = lat[:, rank:]
        key_w = dot(flat, kw_ref[...]).astype(BF16)
        key_n = dot(flat, kn_ref[...]).astype(BF16)
        val_w = dot(flat, vw_ref[...]).astype(BF16)
        val_n = dot(flat, vn_ref[...]).astype(BF16)
        lane = iota((1, 2 * rows), 1)
        first = lane < rows
        inner = jnp.where(first, lane, lane - rows)
        piece = inner >> shift
        mask = jnp.zeros_like(piece)
        for i in range(len(group)):
            mask = jnp.where(piece == i, masks[start + i], mask)
        block = place ^ mask
        offset = jnp.where(first, core, 1 - core)
        key_pos = (block * 2 + offset) * half + (inner & (half - 1))
        visible = iota((tokens, 1), 0) + place * tokens >= key_pos
        new_state = []
        for h in range(heads_w + heads_n):
            if h < heads_w:
                keys = key_w[:, h * PLAIN_WIDTH_WIDE : (h + 1) * PLAIN_WIDTH_WIDE]
                values = val_w[:, h * VALUE_WIDTH_WIDE : (h + 1) * VALUE_WIDTH_WIDE]
                scale = (PLAIN_WIDTH_WIDE + ROPE) ** (-0.5)
            else:
                keys = key_n
                values = val_n
                scale = (PLAIN_WIDTH_SLIM + ROPE) ** (-0.5)
            scores = dot_t(q_ref[h], jnp.concatenate([keys, rot], axis=1)) * scale
            scores = jnp.where(visible, scores, MASKED)
            peak = jnp.max(scores, axis=-1, keepdims=True)
            if state is not None:
                peak = jnp.maximum(peak, state[h][0])
            weights = jnp.exp(scores - peak)
            total = jnp.sum(weights, axis=-1, keepdims=True)
            acc = dot(weights.astype(BF16), values)
            if state is not None:
                keep = jnp.exp(state[h][0] - peak)
                total = total + state[h][1] * keep
                acc = acc + state[h][2] * keep
            new_state.append((peak, total, acc))
        state = new_state
    return state


def first_kernel(masks, *refs):
    q_ref, kw_ref, vw_ref, kn_ref, vn_ref = refs[:5]
    peak_ref, total_ref, acc_ref = refs[-3:]
    state = attend_body(q_ref, refs[5:-3], kw_ref, vw_ref, kn_ref, vn_ref, None, masks)
    for h, (peak, total, acc) in enumerate(state):
        peak_ref[h] = jnp.broadcast_to(peak, peak_ref.shape[1:])
        total_ref[h] = jnp.broadcast_to(total, total_ref.shape[1:])
        acc_ref[h] = acc


def second_kernel(masks, *refs):
    q_ref, kw_ref, vw_ref, kn_ref, vn_ref, peak_ref, total_ref, acc_ref, ow_ref, on_ref = refs[:10]
    keep_ref, send_ref = refs[-2:]
    heads = peak_ref.shape[0]
    heads_w = kw_ref.shape[1] // PLAIN_WIDTH_WIDE
    state = [(peak_ref[h, :, :1], total_ref[h, :, :1], acc_ref[h]) for h in range(heads)]
    state = attend_body(q_ref, refs[10:-2], kw_ref, vw_ref, kn_ref, vn_ref, state, masks)
    done = [acc / total for _, total, acc in state]
    att_w = jnp.concatenate(done[:heads_w], axis=1).astype(BF16)
    slim = done[heads_w]
    for h in range(1, heads - heads_w):
        lane = iota(slim.shape, 1)
        slim = jnp.where(lane >= h * VALUE_WIDTH_SLIM, done[heads_w + h], slim)
    att_n = slim.astype(BF16)
    core = lax.axis_index("tp") & 1
    project(att_w, att_n, ow_ref, on_ref, send_ref, 1 - core)
    project(att_w, att_n, ow_ref, on_ref, keep_ref, core)


def project(att_w, att_n, ow_ref, on_ref, out_ref, bit):
    pieces, _, quarter = out_ref.shape
    for piece in range(pieces):
        cols = pl.ds(pl.multiple_of((2 * piece + bit) * quarter, LANES), quarter)
        out_ref[piece] = (dot(att_w, ow_ref[:, cols]) + dot(att_n, on_ref[:, cols])).astype(BF16)


def slots_of(route, groups, capacity):
    tokens = route.shape[1]
    member = (iota((groups, tokens), 0) == route).astype(F32)
    rank_of = jnp.sum(prefix_count(member) * member, axis=0, keepdims=True).astype(jnp.int32) - 1
    slot = route * capacity + rank_of
    return (iota((groups * capacity, tokens), 0) == slot).astype(BF16)


def weights_kernel(masks, *refs):
    out_ref = refs[-1]
    count = (len(refs) - 1) // 2
    mine_all, other_all = pieces_of(refs[:count]), pieces_of(refs[count:-1])
    half, width = mine_all[0].shape
    place = lax.axis_index("sp")
    odd = (lax.axis_index("tp") & 1) == 1
    capacity = out_ref.shape[0] // len(mine_all)
    base = width - LANES
    for mask, mine, other in zip(masks, mine_all, other_all):
        mine, other = mine[:, base:], other[:, base:]
        data = jnp.concatenate(
            [jnp.where(odd, other, mine), jnp.where(odd, mine, other)], axis=0
        )
        route = data.astype(F32).T[ROPE + EPG : ROPE + EPG + 1]
        here = (route == place.astype(F32)).astype(F32)
        order = prefix_count(here) - 1.0
        hot = jnp.where((iota((capacity, 2 * half), 0).astype(F32) == order) & (here > 0), 1.0, 0.0)
        start = pl.multiple_of((place ^ mask) * capacity, capacity)
        out_ref[pl.ds(start, capacity), :] = dot(hot.astype(BF16), data)


def place_kernel(keep_ref, got_ref, resid_ref, route_ref, stream_ref, placed_ref):
    groups, capacity, _ = placed_ref.shape
    stream = keep_ref[...].astype(F32) + got_ref[...].astype(F32) + resid_ref[...].astype(F32)
    stream = stream.astype(BF16)
    stream_ref[...] = stream
    hot = slots_of(route_ref[...], groups, capacity)
    placed_ref[...] = dot(hot, stream).astype(BF16).reshape(placed_ref.shape)


def final_kernel(stream_ref, back_ref, route_ref, out_ref):
    groups, copies, capacity, quarter = back_ref.shape
    hot = slots_of(route_ref[...], groups, capacity)
    total = stream_ref[...].astype(F32)
    for copy in range(copies):
        rows = back_ref[:, copy].reshape(groups * capacity, quarter)
        total = total + lax.dot_general(hot, rows, (((0,), (0,)), ((), ())), preferred_element_type=F32)
    out_ref[...] = total.astype(BF16)


def expand_part(masks, gain_ref, gate_ref, up_ref, parts, acts, square):
    quarter = parts[0].shape[1]
    place = lax.axis_index("tp")
    for mask, part in zip(masks, parts):
        cols = pl.ds(pl.multiple_of((place ^ mask) * quarter, LANES), quarter)
        rows = part[...].astype(F32)
        square = square + jnp.sum(rows * rows, axis=-1, keepdims=True)
        scaled = (rows * gain_ref[:, cols]).astype(BF16)
        for e in range(len(acts)):
            both = jnp.concatenate([gate_ref[e, cols, :], up_ref[e, cols, :]], axis=1)
            acts[e] = acts[e] + dot(scaled, both)
    return square


def near_kernel(masks, gain_ref, gate_ref, up_ref, *refs):
    act_ref, square_ref = refs[-2:]
    acts = [0.0] * act_ref.shape[0]
    square = expand_part(masks, gain_ref, gate_ref, up_ref, refs[:-2], acts, 0.0)
    for e, act in enumerate(acts):
        act_ref[e] = act
    square_ref[...] = jnp.broadcast_to(square, square_ref.shape)


def contract(hidden, down_ref, out_ref, bit):
    groups, uppers, capacity, quarter = out_ref.shape
    for upper in range(uppers):
        cols = pl.ds(pl.multiple_of((2 * upper + bit) * quarter, LANES), quarter)
        out_ref[:, upper] = dot(hidden, down_ref[:, cols]).astype(BF16).reshape(groups, capacity, quarter)


def far_kernel(masks, gain_ref, gate_ref, up_ref, down_ref, weight_ref, act_ref, square_ref, *refs):
    send_ref, hidden_ref = refs[-2:]
    experts, model_width, hidden_width = gate_ref.shape
    acts = [act_ref[e] for e in range(experts)]
    square = expand_part(masks, gain_ref, gate_ref, up_ref, refs[:-2], acts, square_ref[:, :1])
    scale = lax.rsqrt(square / model_width + EPSILON)
    hidden = []
    for e in range(experts):
        gate, up = acts[e][:, :hidden_width] * scale, acts[e][:, hidden_width:] * scale
        weight = weight_ref[:, ROPE + e : ROPE + e + 1]
        hidden.append((gate / (1.0 + jnp.exp(-gate)) * up * weight).astype(BF16))
    hidden = jnp.concatenate(hidden, axis=1)
    hidden_ref[...] = hidden
    contract(hidden, down_ref, send_ref, 1 - (lax.axis_index("tp") & 1))


def stay_kernel(hidden_ref, down_ref, keep_ref):
    contract(hidden_ref[...], down_ref, keep_ref, lax.axis_index("tp") & 1)


def start_copies(sources, targets, semaphores):
    copies = [
        pltpu.make_async_copy(source, target, semaphores.at[i])
        for i, (source, target) in enumerate(zip(sources, targets))
    ]
    for copy in copies:
        copy.start()
    return copies


def call(kernel, outs, inputs, fetched=(), kept=(), mib=12):
    n_in, n_fetched, n_kept, n_out = len(inputs), len(fetched), len(kept), len(outs)

    def wrapped(*refs):
        refs = list(refs)
        take = lambda n: [refs.pop(0) for _ in range(n)]
        ins, sources, kept_sources = take(n_in), take(n_fetched), take(n_kept)
        results, kept_results, held = take(n_out), take(n_kept), take(n_fetched)
        first = start_copies(sources, held, refs[0]) if n_fetched else []
        second = start_copies(kept_sources, kept_results, refs[-1]) if n_kept else []
        for copy in first:
            copy.wait()
        kernel(*ins, *held, *results)
        for copy in second:
            copy.wait()

    semaphores = [pltpu.SemaphoreType.DMA((n,)) for n in (n_fetched, n_kept) if n]
    return pl.pallas_call(
        wrapped,
        out_shape=list(outs) + [held_shape(a.shape, a.dtype) for a in kept],
        in_specs=[VMEM] * n_in + [HBM] * (n_fetched + n_kept),
        out_specs=[VMEM] * (n_out + n_kept),
        scratch_shapes=[pltpu.VMEM(a.shape, a.dtype) for a in fetched] + semaphores,
        compiler_params=pltpu.CompilerParams(vmem_limit_bytes=mib * 2**20),
    )(
        *(pltpu.with_memory_space_constraint(a, pltpu.VMEM) for a in inputs),
        *(pltpu.with_memory_space_constraint(a, pltpu.HBM) for a in (*fetched, *kept)),
    )


def shape(dims, dtype=BF16):
    return jax.ShapeDtypeStruct(dims, dtype)


def held_shape(dims, dtype=BF16):
    return pltpu.VMEM(dims, dtype)


def halved(keep, got, first_bit, place):
    pieces = [keep[i].astype(F32) + got[i].astype(F32) for i in range(keep.shape[0])]
    bit = first_bit
    while True:
        mine = ((place >> bit) & 1) == 1
        low, high = pieces[0::2], pieces[1::2]
        send = [jnp.where(mine, a, b).astype(BF16) for a, b in zip(low, high)]
        stay = [jnp.where(mine, b, a) for a, b in zip(low, high)]
        if len(send) == 1:
            return stay[0].astype(BF16), exchange(send[0], "tp", 1 << bit)
        came = exchange(jnp.stack(send), "tp", 1 << bit)
        pieces = [a + came[i].astype(F32) for i, a in enumerate(stay)]
        bit += 1


def body(
    query_wide,
    query_narrow,
    latent,
    rope_key,
    latent_norm_weight,
    broad_key_lift,
    broad_value_lift,
    slim_key_lift,
    slim_value_lift,
    out_wide,
    out_narrow,
    resid,
    ffn_gain,
    group_route,
    expert_pair,
    group_prob,
    expert_prob,
    gate_weight,
    up_weight,
    down_weight,
):
    tokens, rank = latent.shape
    groups = lax.axis_size("sp")
    tp_size = lax.axis_size("tp")
    place = lax.axis_index("sp")
    lane_place = lax.axis_index("tp")
    half = tokens // 2
    capacity = 2 * tokens // groups
    slots = groups * capacity
    model_width = resid.shape[1]
    quarter = model_width // tp_size
    route = group_route[None, :]

    query_pos = place * tokens + jnp.arange(tokens, dtype=jnp.int32)
    table = angles(query_pos, ROPE).T
    packed = held_shape((half, rank + LANES))
    own, rest = call(
        pack_kernel, [packed, packed], [jnp.cos(table), jnp.sin(table)],
        [latent, rope_key.T, latent_norm_weight[None, :], route, expert_pair.T, group_prob[None, :], expert_prob.T],
        mib=4,
    )

    strides = list(range(groups - 2, 0, -2))
    got = []
    for k in strides:
        got.append(exchange(own, "sp", k))
    across = [exchange(own, "sp", 1)]
    across_rest = [exchange(across[0], "tp", 1)]
    cut = len(strides) // 2
    for pieces in (got[:cut], got[cut:]):
        across.append(exchange(jnp.stack(pieces), "sp", 1))
    column = [own, jnp.stack(got)]
    column_rest = [rest, exchange(column[1], "tp", 1)]
    across = [across[0], jnp.concatenate(across[1:])]
    across_rest.append(exchange(across[1], "tp", 1))
    first_masks = [0] + strides + [1]
    second_masks = [k ^ 1 for k in strides]

    heads = query_wide.shape[1] // (PLAIN_WIDTH_WIDE + ROPE) + query_narrow.shape[1] // (PLAIN_WIDTH_SLIM + ROPE)
    angle_rows = angles(query_pos, ROPE)
    queries, key_w, value_w, key_n, value_n, out_w, out_n = call(
        query_kernel, [held_shape((heads, tokens, 2 * LANES))], [jnp.cos(angle_rows), jnp.sin(angle_rows)],
        [query_wide, query_narrow],
        [broad_key_lift, broad_value_lift, slim_key_lift, slim_value_lift, out_wide, out_narrow], mib=4,
    )
    lifts = [key_w, value_w, key_n, value_n]
    state = call(
        functools.partial(first_kernel, first_masks), [held_shape((heads, tokens, LANES), F32)] * 3,
        [queries, *lifts, *column, across[0], *column_rest, across_rest[0]],
    )
    pieces_shape = held_shape((tp_size // 2, tokens, quarter))
    keep, send = call(
        functools.partial(second_kernel, second_masks), [pieces_shape] * 2,
        [queries, *lifts, *state, out_w, out_n, *across[1:], *across_rest[1:]],
    )
    slot_weights, gate, up, down, gain = call(
        functools.partial(weights_kernel, first_masks + second_masks), [held_shape((slots, LANES), F32)],
        [*column, *across, *column_rest, *across_rest], [],
        [gate_weight[0], up_weight[0], down_weight[0].reshape(-1, model_width), ffn_gain[None, :]], mib=4,
    )

    received = exchange(send, "tp", 1)
    stay, came = halved(keep, received, 1, lane_place)
    resid_cols = lax.dynamic_slice_in_dim(resid, lane_place * quarter, quarter, 1)
    stream_cols, placed = call(
        place_kernel, [held_shape((tokens, quarter)), held_shape((groups, capacity, quarter))],
        [stay, came, resid_cols, route], mib=4,
    )

    routed = lax.all_to_all(placed, "sp", split_axis=0, concat_axis=0, tiled=True)
    routed = routed.reshape(slots, quarter)
    far_masks = list(range(2, tp_size, 2))
    far = []
    for mask in far_masks:
        far.append(exchange(routed, "tp", mask))
    near = exchange(routed, "tp", 1)
    experts, _, hidden_width = gate_weight[0].shape
    acts, square = call(
        functools.partial(near_kernel, [0, 1]),
        [held_shape((experts, slots, 2 * hidden_width), F32), held_shape((slots, LANES), F32)],
        [gain, gate, up, routed, near],
    )
    far_near = [exchange(part, "tp", 1) for part in far]
    uppers = tp_size // 2
    cube = held_shape((groups, uppers, capacity, quarter))
    send, hidden = call(
        functools.partial(far_kernel, far_masks + [m | 1 for m in far_masks]),
        [cube, held_shape((slots, experts * hidden_width))],
        [gain, gate, up, down, slot_weights, acts, square, *far, *far_near],
    )
    received = exchange(send, "tp", 1)
    (keep,) = call(stay_kernel, [cube], [hidden, down])

    teams = [
        [g * tp_size + 2 * upper + low for g in range(groups) for upper in range(uppers)] for low in range(2)
    ]
    summed = (keep.astype(F32) + received.astype(F32)).astype(BF16)
    returned = lax.all_to_all(
        summed.reshape(groups * uppers, capacity, quarter),
        ("sp", "tp"), split_axis=0, concat_axis=0, axis_index_groups=teams, tiled=True,
    ).reshape(cube.shape)
    return call(final_kernel, [shape((tokens, quarter))], [stream_cols, returned, route], mib=4)[0]


def solution(mesh):
    placed = (
        P("sp", "tp"),
        P("sp", "tp"),
        P("sp", None),
        P("sp", None),
        P(),
        P(None, "tp"),
        P(None, "tp"),
        P(None, "tp"),
        P(None, "tp"),
        P("tp", None),
        P("tp", None),
        P("sp", None),
        P(),
        P("sp"),
        P("sp", None),
        P("sp"),
        P("sp", None),
        P("sp", None, None, "tp"),
        P("sp", None, None, "tp"),
        P("sp", None, "tp", None),
    )
    return jax.shard_map(body, mesh=mesh, in_specs=placed, out_specs=P("sp", "tp"), check_vma=False)
```

profile of v0, /device:TPU:0, one launch (start us, length us, event | category | flops | bytes accessed | tf_op | source)
XLA Modules:
  0.0 83.3 jit_solution(1965027811324811628)
XLA Ops:
  0.0 0.0 copy-start
  0.0 0.1 multiply_sine_fusion.1
  0.2 1.1 %shard_map.191 = (bf16[64,640]{1,0:T(8,128)(2,1)S(1)}, bf16[64,640]{1,0:T(8,128)(2,1)S(1)}) custom-call(f32[32,128]{1,0:T(8,128)S(1)} %get-tuple-element.58.refs_0_, f32[32,128]{1,0:T(8,128)S(1)} %get-tuple-element.57.refs_1_, bf16[128,512]{1,0:T(8,128)(2,1)} %refs_2_.3, bf16[64,128]{1,0:T(8,128)(2,1)} %bitcast.37, f32[1,512]{1,0:T(1,128)} %bitcast.39, ...), custom_call_target="tpu_custom_call" | custom-call | tf_op jit(solution)/shard_map/pallas_call | solution.py:342
  1.3 5.1 %collective-permute-start = (bf16[64,640]{1,0:T(8,128)(2,1)S(1)}, bf16[64,640]{1,0:T(8,128)(2,1)S(1)}, u32[]{:S(2)}, u32[]{:S(2)}) collective-permute-start(bf16[64,640]{1,0:T(8,128)(2,1)S(1)} %get-tuple-element.35.refs_5_.refs_0_), channel_id=1, source_target_pairs={{0,24},{4,28},{8,16},{12,20},{16,8},{20,12},{24,0},{28,4},{1,25},{... | collective-permute-start | bytes 245768 | tf_op jit(solution)/shard_map/ppermute | solution.py:44
  6.5 0.0 collective-permute-start.2
  6.5 0.6 collective-permute-start.1
  7.1 1.6 %collective-permute-start.3 = (bf16[64,640]{1,0:T(8,128)(2,1)S(1)}, bf16[64,640]{1,0:T(8,128)(2,1)S(1)}, u32[]{:S(2)}, u32[]{:S(2)}) collective-permute-start(bf16[64,640]{1,0:T(8,128)(2,1)S(1)} %get-tuple-element.35.refs_5_.refs_0_), channel_id=1, source_target_pairs={{0,4},{4,0},{8,12},{12,8},{16,20},{20,16},{24,28},{28,24},{1,5},{5... | collective-permute-start | bytes 245768 | tf_op jit(solution)/shard_map/ppermute | solution.py:44
  8.7 1.1 %collective-permute-done = bf16[64,640]{1,0:T(8,128)(2,1)S(1)} collective-permute-done((bf16[64,640]{1,0:T(8,128)(2,1)S(1)}, bf16[64,640]{1,0:T(8,128)(2,1)S(1)}, u32[]{:S(2)}, u32[]{:S(2)}) %collective-permute-start) | collective-permute-done | bytes 81952 | tf_op jit(solution)/shard_map/ppermute | solution.py:44
  9.8 1.6 %collective-permute-start.6 = (bf16[1,64,640]{2,1,0:T(8,128)(2,1)S(1)}, bf16[1,64,640]{2,1,0:T(8,128)(2,1)S(1)}, u32[]{:S(2)}, u32[]{:S(2)}) collective-permute-start(bf16[1,64,640]{2,1,0:T(8,128)(2,1)S(1)} %bitcast.35), channel_id=1, source_target_pairs={{0,4},{4,0},{8,12},{12,8},{16,20},{20,16},{24,28},{28,24},{1,5},{5... | collective-permute-start | bytes 245768 | tf_op jit(solution)/shard_map/ppermute | solution.py:44
  11.4 1.3 %collective-permute-done.2 = bf16[64,640]{1,0:T(8,128)(2,1)S(1)} collective-permute-done((bf16[64,640]{1,0:T(8,128)(2,1)S(1)}, bf16[64,640]{1,0:T(8,128)(2,1)S(1)}, u32[]{:S(2)}, u32[]{:S(2)}) %collective-permute-start.2) | collective-permute-done | bytes 81952 | tf_op jit(solution)/shard_map/ppermute | solution.py:44
  12.7 0.0 collective-permute-done.1
  12.7 1.7 %collective-permute-start.7 = (bf16[2,64,640]{2,1,0:T(8,128)(2,1)S(1)}, bf16[2,64,640]{2,1,0:T(8,128)(2,1)S(1)}, u32[]{:S(2)}, u32[]{:S(2)}) collective-permute-start(bf16[2,64,640]{2,1,0:T(8,128)(2,1)S(1)} %pad_maximum_fusion.1), channel_id=1, source_target_pairs={{0,4},{4,0},{8,12},{12,8},{16,20},{20,16},{24,28},{28,24},{1,5},{5... | collective-permute-start | bytes 491528 | tf_op jit(solution)/shard_map/ppermute | solution.py:44
  14.4 0.1 collective-permute-start.4
  14.5 0.0 collective-permute-done.6
  14.5 3.6 %collective-permute-done.7 = bf16[2,64,640]{2,1,0:T(8,128)(2,1)S(1)} collective-permute-done((bf16[2,64,640]{2,1,0:T(8,128)(2,1)S(1)}, bf16[2,64,640]{2,1,0:T(8,128)(2,1)S(1)}, u32[]{:S(2)}, u32[]{:S(2)}) %collective-permute-start.7) | collective-permute-done | bytes 163872 | tf_op jit(solution)/shard_map/ppermute | solution.py:44
  18.1 0.1 collective-permute-start.8
  18.2 0.0 collective-permute-done.3.refs_7_.refs_2_
  18.2 0.5 collective-permute-start.5
  18.7 0.3 multiply_sine_fusion
  19.0 2.2 %shard_map.190 = (bf16[4,128,256]{2,1,0:T(8,128)(2,1)S(1)}, bf16[512,256]{1,0:T(8,128)(2,1)S(1)}, bf16[512,256]{1,0:T(8,128)(2,1)S(1)}, bf16[512,128]{1,0:T(8,12...) custom-call(f32[128,32]{1,0:T(8,128)S(1)} %get-tuple-element.60.refs_0_, ...), custom_call_target="tpu_custom_call" | custom-call | tf_op jit(solution)/shard_map/pallas_call | solution.py:342
  21.2 0.0 collective-permute-done.5.refs_10_.refs_6_
  21.2 0.0 collective-permute-done.4.refs_9_.refs_5_
  21.2 2.2 %shard_map.192 = (f32[4,128,128]{2,1,0:T(8,128)S(1)}, f32[4,128,128]{2,1,0:T(8,128)S(1)}, f32[4,128,128]{2,1,0:T(8,128)S(1)}) custom-call(bf16[4,128,256]{2,1,0:T(8,128)(2,1)S(1)} %get-tuple-element.30.refs_0_, bf16[512,256]{1,0:T(8,128)(2,1)S(1)} %get-tuple-element.31.refs_1_, bf16[512,256]{1,0:T(8,128)(2,1)S(1)} %get-tuple-element.32.refs_2_, ...), custom_call_target="tpu_custom_call" | custom-call | tf_op jit(solution)/shard_map/pallas_call | solution.py:342
  23.4 0.0 collective-permute-done.8.refs_11_.refs_7_
  23.4 0.0 copy-start.1
  23.4 2.6 %shard_map.193 = (bf16[2,128,512]{2,1,0:T(8,128)(2,1)S(1)}, bf16[2,128,512]{2,1,0:T(8,128)(2,1)S(1)}) custom-call(bf16[4,128,256]{2,1,0:T(8,128)(2,1)S(1)} %get-tuple-element.30.refs_0_, bf16[512,256]{1,0:T(8,128)(2,1)S(1)} %get-tuple-element.31.refs_1_, bf16[512,256]{1,0:T(8,128)(2,1)S(1)} %get-tuple-element.32.refs_2_, ...), custom_call_target="tpu_custom_call" | custom-call | tf_op jit(solution)/shard_map/pallas_call | solution.py:342
  26.0 0.1 collective-permute-start.9
  26.2 1.5 %collective-permute-done.9 = bf16[2,128,512]{2,1,0:T(8,128)(2,1)S(1)} collective-permute-done((bf16[2,128,512]{2,1,0:T(8,128)(2,1)S(1)}, bf16[2,128,512]{2,1,0:T(8,128)(2,1)S(1)}, u32[]{:S(2)}, u32[]{:S(2)}) %collective-permute-start.9) | collective-permute-done | bytes 262176 | tf_op jit(solution)/shard_map/ppermute | solution.py:44
  27.6 0.1 fusion.1
  27.7 1.7 %collective-permute-start.10 = (bf16[128,512]{1,0:T(8,128)(2,1)S(1)}, bf16[128,512]{1,0:T(8,128)(2,1)S(1)}, u32[]{:S(2)}, u32[]{:S(2)}) collective-permute-start(bf16[128,512]{1,0:T(8,128)(2,1)S(1)} %get-tuple-element.55), channel_id=1, source_target_pairs={{0,2},{1,3},{2,0},{3,1},{4,6},{5,7},{6,4},{7,5},{8,10},{9,11},{10,... | collective-permute-start | bytes 393224 | tf_op jit(solution)/shard_map/ppermute | solution.py:44
  29.4 0.0 copy-done
  29.4 3.9 %collective-permute-done.10.refs_1_ = bf16[128,512]{1,0:T(8,128)(2,1)S(1)} collective-permute-done((bf16[128,512]{1,0:T(8,128)(2,1)S(1)}, bf16[128,512]{1,0:T(8,128)(2,1)S(1)}, u32[]{:S(2)}, u32[]{:S(2)}) %collective-permute-start.10) | collective-permute-done | bytes 131104 | tf_op jit(solution)/shard_map/ppermute | solution.py:44
  33.3 0.0 copy-done.1
  33.3 0.4 shard_map.194
  33.7 13.9 %all_to_all.10 = bf16[8,32,512]{2,1,0:T(8,128)(2,1)S(1)} all-to-all(bf16[8,32,512]{2,1,0:T(8,128)(2,1)S(1)} %get-tuple-element.50), channel_id=1, replica_groups=mesh['sp'=8,'tp'=4] {'sp'}, dimensions={0} | all-to-all | bytes 524288 | tf_op jit(solution)/shard_map/all_to_all | solution.py:468
  47.6 1.5 %collective-permute-start.12 = (bf16[256,512]{1,0:T(8,128)(2,1)S(1)}, bf16[256,512]{1,0:T(8,128)(2,1)S(1)}, u32[]{:S(2)}, u32[]{:S(2)}) collective-permute-start(bf16[256,512]{1,0:T(8,128)(2,1)S(1)} %bitcast.21), channel_id=1, source_target_pairs={{0,2},{1,3},{2,0},{3,1},{4,6},{5,7},{6,4},{7,5},{8,10},{9,11},{10,... | collective-permute-start | bytes 786440 | tf_op jit(solution)/shard_map/ppermute | solution.py:44
  49.1 0.0 collective-permute-start.11
  49.1 4.9 %collective-permute-done.12.refs_7_ = bf16[256,512]{1,0:T(8,128)(2,1)S(1)} collective-permute-done((bf16[256,512]{1,0:T(8,128)(2,1)S(1)}, bf16[256,512]{1,0:T(8,128)(2,1)S(1)}, u32[]{:S(2)}, u32[]{:S(2)}) %collective-permute-start.12) | collective-permute-done | bytes 262176 | tf_op jit(solution)/shard_map/ppermute | solution.py:44
  54.0 0.0 collective-permute-start.13
  54.0 3.0 %shard_map.195 = (f32[256,128]{1,0:T(8,128)S(1)}, bf16[4,2048,128]{2,1,0:T(8,128)(2,1)S(1)}, bf16[4,2048,128]{2,1,0:T(8,128)(2,1)S(1)}, bf16[512,2048]{1,0:T(8,128)(2,1)S(1)}, f32[1,2048]{1,0:T(1,128)S(1)}) custom-call(bf16[64,640]{1,0:T(8,128)(2,1)S(1)} %get-tuple-element.35.refs_5_.refs_0_, bf16[3,64,640]{2,1,0:T(8,128)(2,1)S(1)} %pad_maximum_fusion.refs_6_.refs_1_, ...), custom_call_target="tpu_custom_call" | custom-call | tf_op jit(solution)/shard_map/pallas_call | solution.py:342
  57.0 0.0 collective-permute-done.11.refs_4_
  57.0 0.7 shard_map.196
  57.8 0.0 collective-permute-done.13.refs_8_
  57.8 1.2 %shard_map.197 = (bf16[8,2,32,512]{3,2,1,0:T(8,128)(2,1)S(1)}, bf16[256,512]{1,0:T(8,128)(2,1)S(1)}) custom-call(f32[1,2048]{1,0:T(1,128)S(1)} %get-tuple-element.45.refs_0_, bf16[4,2048,128]{2,1,0:T(8,128)(2,1)S(1)} %get-tuple-element.46.refs_1_, bf16[4,2048,128]{2,1,0:T(8,128)(2,1)S(1)} %get-tuple-element.47.refs_2_, ...), custom_call_target="tpu_custom_call" | custom-call | tf_op jit(solution)/shard_map/pallas_call | solution.py:342
  59.0 0.6 collective-permute-start.14
  59.5 0.4 shard_map.198
  60.0 1.1 %collective-permute-done.14 = bf16[8,2,32,512]{3,2,1,0:T(8,128)(2,1)S(1)} collective-permute-done((bf16[8,2,32,512]{3,2,1,0:T(8,128)(2,1)S(1)}, bf16[8,2,32,512]{3,2,1,0:T(8,128)(2,1)S(1)}, u32[]{:S(2)}, u32[]{:S(2)}) %collective-permute-start.14) | collective-permute-done | bytes 524320 | tf_op jit(solution)/shard_map/ppermute | solution.py:44
  61.1 0.1 add_convert_fusion
  61.2 21.0 %all_to_all.11 = bf16[16,32,512]{2,1,0:T(8,128)(2,1)S(1)} all-to-all(bf16[16,32,512]{2,1,0:T(8,128)(2,1)S(1)} %bitcast.30), channel_id=1, replica_groups={{0,2,4,6,8,10,12,14,16,18,20,22,24,26,28,30},{1,3,5,7,9,11,13,15,17,19,..., dimensions={0} | all-to-all | bytes 1048576 | tf_op jit(solution)/shard_map/all_to_all | solution.py:496
  82.3 1.1 %shard_map.199 = bf16[128,512]{1,0:T(8,128)(2,1)} custom-call(bf16[128,512]{1,0:T(8,128)(2,1)S(1)} %get-tuple-element.44.refs_0_, bf16[8,2,32,512]{3,2,1,0:T(8,128)(2,1)S(1)} %bitcast.20, s32[1,128]{1,0:T(1,128)S(1)} %bitcast.26), custom_call_target="tpu_custom_call" | custom-call | tf_op jit(solution)/shard_map/pallas_call | solution.py:342
  (7 shorter events, 0.1 us)
Async XLA Ops:
  0.0 29.4 %copy-start = (bf16[128,2048]{1,0:T(8,128)(2,1)S(1)}, bf16[128,2048]{1,0:T(8,128)(2,1)}, u32[]{:S(2)}) copy-start(bf16[128,2048]{1,0:T(8,128)(2,1)} %param.31) | copy-start | bytes 1572868
  1.3 8.5 %collective-permute-start = (bf16[64,640]{1,0:T(8,128)(2,1)S(1)}, bf16[64,640]{1,0:T(8,128)(2,1)S(1)}, u32[]{:S(2)}, u32[]{:S(2)}) collective-permute-start(bf16[64,640]{1,0:T(8,128)(2,1)S(1)} %get-tuple-element.35.refs_5_.refs_0_), channel_id=1, source_target_pairs={{0,24},{4,28},{8,16},{12,20},{16,8},{20,12},{24,0},{28,4},{1,25},{... | collective-permute-start | bytes 245768 | tf_op jit(solution)/shard_map/ppermute | solution.py:44
  6.5 6.2 %collective-permute-start.2 = (bf16[64,640]{1,0:T(8,128)(2,1)S(1)}, bf16[64,640]{1,0:T(8,128)(2,1)S(1)}, u32[]{:S(2)}, u32[]{:S(2)}) collective-permute-start(bf16[64,640]{1,0:T(8,128)(2,1)S(1)} %get-tuple-element.35.refs_5_.refs_0_), channel_id=1, source_target_pairs={{0,8},{4,12},{8,0},{12,4},{16,24},{20,28},{24,16},{28,20},{1,9},{5... | collective-permute-start | bytes 245768 | tf_op jit(solution)/shard_map/ppermute | solution.py:44
  6.5 6.2 %collective-permute-start.1 = (bf16[64,640]{1,0:T(8,128)(2,1)S(1)}, bf16[64,640]{1,0:T(8,128)(2,1)S(1)}, u32[]{:S(2)}, u32[]{:S(2)}) collective-permute-start(bf16[64,640]{1,0:T(8,128)(2,1)S(1)} %get-tuple-element.35.refs_5_.refs_0_), channel_id=1, source_target_pairs={{0,16},{4,20},{8,24},{12,28},{16,0},{20,4},{24,8},{28,12},{1,17},{... | collective-permute-start | bytes 245768 | tf_op jit(solution)/shard_map/ppermute | solution.py:44
  7.1 11.1 %collective-permute-start.3 = (bf16[64,640]{1,0:T(8,128)(2,1)S(1)}, bf16[64,640]{1,0:T(8,128)(2,1)S(1)}, u32[]{:S(2)}, u32[]{:S(2)}) collective-permute-start(bf16[64,640]{1,0:T(8,128)(2,1)S(1)} %get-tuple-element.35.refs_5_.refs_0_), channel_id=1, source_target_pairs={{0,4},{4,0},{8,12},{12,8},{16,20},{20,16},{24,28},{28,24},{1,5},{5... | collective-permute-start | bytes 245768 | tf_op jit(solution)/shard_map/ppermute | solution.py:44
  9.8 4.7 %collective-permute-start.6 = (bf16[1,64,640]{2,1,0:T(8,128)(2,1)S(1)}, bf16[1,64,640]{2,1,0:T(8,128)(2,1)S(1)}, u32[]{:S(2)}, u32[]{:S(2)}) collective-permute-start(bf16[1,64,640]{2,1,0:T(8,128)(2,1)S(1)} %bitcast.35), channel_id=1, source_target_pairs={{0,4},{4,0},{8,12},{12,8},{16,20},{20,16},{24,28},{28,24},{1,5},{5... | collective-permute-start | bytes 245768 | tf_op jit(solution)/shard_map/ppermute | solution.py:44
  12.7 5.4 %collective-permute-start.7 = (bf16[2,64,640]{2,1,0:T(8,128)(2,1)S(1)}, bf16[2,64,640]{2,1,0:T(8,128)(2,1)S(1)}, u32[]{:S(2)}, u32[]{:S(2)}) collective-permute-start(bf16[2,64,640]{2,1,0:T(8,128)(2,1)S(1)} %pad_maximum_fusion.1), channel_id=1, source_target_pairs={{0,4},{4,0},{8,12},{12,8},{16,20},{20,16},{24,28},{28,24},{1,5},{5... | collective-permute-start | bytes 491528 | tf_op jit(solution)/shard_map/ppermute | solution.py:44
  14.4 6.8 %collective-permute-start.4 = (bf16[3,64,640]{2,1,0:T(8,128)(2,1)S(1)}, bf16[3,64,640]{2,1,0:T(8,128)(2,1)S(1)}, u32[]{:S(2)}, u32[]{:S(2)}) collective-permute-start(bf16[3,64,640]{2,1,0:T(8,128)(2,1)S(1)} %pad_maximum_fusion.refs_6_.refs_1_), channel_id=1, source_target_pairs={{0,1},{1,0},{2,3},{3,2},{4,5},{5,4},{6,7},{7,6},{8,9},{9,8},{10,11... | collective-permute-start | bytes 737288 | tf_op jit(solution)/shard_map/ppermute | solution.py:44
  18.1 5.2 %collective-permute-start.8 = (bf16[3,64,640]{2,1,0:T(8,128)(2,1)S(1)}, bf16[3,64,640]{2,1,0:T(8,128)(2,1)S(1)}, u32[]{:S(2)}, u32[]{:S(2)}) collective-permute-start(bf16[3,64,640]{2,1,0:T(8,128)(2,1)S(1)} %constant_dynamic-update-slice_fusion.refs_10_.refs_3_), channel_id=1, source_target_pairs={{0,1},{1,0},{2,3},{3,2},{4,5},{5,4},{6,7},{7,6},{8,9},{9,8},{10,11... | collective-permute-start | bytes 737288 | tf_op jit(solution)/shard_map/ppermute | solution.py:44
  18.2 3.0 %collective-permute-start.5 = (bf16[64,640]{1,0:T(8,128)(2,1)S(1)}, bf16[64,640]{1,0:T(8,128)(2,1)S(1)}, u32[]{:S(2)}, u32[]{:S(2)}) collective-permute-start(bf16[64,640]{1,0:T(8,128)(2,1)S(1)} %collective-permute-done.3.refs_7_.refs_2_), channel_id=1, source_target_pairs={{0,1},{1,0},{2,3},{3,2},{4,5},{5,4},{6,7},{7,6},{8,9},{9,8},{10,11... | collective-permute-start | bytes 245768 | tf_op jit(solution)/shard_map/ppermute | solution.py:44
  23.4 9.9 %copy-start.1 = (s32[128]{0:T(128)S(1)}, s32[128]{0:T(128)}, u32[]{:S(2)}) copy-start(s32[128]{0:T(128)} %param.33) | copy-start | bytes 1540
  26.0 1.6 %collective-permute-start.9 = (bf16[2,128,512]{2,1,0:T(8,128)(2,1)S(1)}, bf16[2,128,512]{2,1,0:T(8,128)(2,1)S(1)}, u32[]{:S(2)}, u32[]{:S(2)}) collective-permute-start(bf16[2,128,512]{2,1,0:T(8,128)(2,1)S(1)} %get-tuple-element.43), channel_id=1, source_target_pairs={{0,1},{1,0},{2,3},{3,2},{4,5},{5,4},{6,7},{7,6},{8,9},{9,8},{10,11... | collective-permute-start | bytes 786440 | tf_op jit(solution)/shard_map/ppermute | solution.py:44
  27.7 5.6 %collective-permute-start.10 = (bf16[128,512]{1,0:T(8,128)(2,1)S(1)}, bf16[128,512]{1,0:T(8,128)(2,1)S(1)}, u32[]{:S(2)}, u32[]{:S(2)}) collective-permute-start(bf16[128,512]{1,0:T(8,128)(2,1)S(1)} %get-tuple-element.55), channel_id=1, source_target_pairs={{0,2},{1,3},{2,0},{3,1},{4,6},{5,7},{6,4},{7,5},{8,10},{9,11},{10,... | collective-permute-start | bytes 393224 | tf_op jit(solution)/shard_map/ppermute | solution.py:44
  47.6 6.4 %collective-permute-start.12 = (bf16[256,512]{1,0:T(8,128)(2,1)S(1)}, bf16[256,512]{1,0:T(8,128)(2,1)S(1)}, u32[]{:S(2)}, u32[]{:S(2)}) collective-permute-start(bf16[256,512]{1,0:T(8,128)(2,1)S(1)} %bitcast.21), channel_id=1, source_target_pairs={{0,2},{1,3},{2,0},{3,1},{4,6},{5,7},{6,4},{7,5},{8,10},{9,11},{10,... | collective-permute-start | bytes 786440 | tf_op jit(solution)/shard_map/ppermute | solution.py:44
  49.1 7.9 %collective-permute-start.11 = (bf16[256,512]{1,0:T(8,128)(2,1)S(1)}, bf16[256,512]{1,0:T(8,128)(2,1)S(1)}, u32[]{:S(2)}, u32[]{:S(2)}) collective-permute-start(bf16[256,512]{1,0:T(8,128)(2,1)S(1)} %bitcast.22), channel_id=1, source_target_pairs={{0,1},{1,0},{2,3},{3,2},{4,5},{5,4},{6,7},{7,6},{8,9},{9,8},{10,11... | collective-permute-start | bytes 786440 | tf_op jit(solution)/shard_map/ppermute | solution.py:44
  54.0 3.8 %collective-permute-start.13 = (bf16[256,512]{1,0:T(8,128)(2,1)S(1)}, bf16[256,512]{1,0:T(8,128)(2,1)S(1)}, u32[]{:S(2)}, u32[]{:S(2)}) collective-permute-start(bf16[256,512]{1,0:T(8,128)(2,1)S(1)} %collective-permute-done.12.refs_7_), channel_id=1, source_target_pairs={{0,1},{1,0},{2,3},{3,2},{4,5},{5,4},{6,7},{7,6},{8,9},{9,8},{10,11... | collective-permute-start | bytes 786440 | tf_op jit(solution)/shard_map/ppermute | solution.py:44
  59.0 2.1 %collective-permute-start.14 = (bf16[8,2,32,512]{3,2,1,0:T(8,128)(2,1)S(1)}, bf16[8,2,32,512]{3,2,1,0:T(8,128)(2,1)S(1)}, u32[]{:S(2)}, u32[]{:S(2)}) collective-permute-start(bf16[8,2,32,512]{3,2,1,0:T(8,128)(2,1)S(1)} %get-tuple-element.54), channel_id=1, source_target_pairs={{0,1},{1,0},{2,3},{3,2},{4,5},{5,4},{6,7},{7,6},{8,9},{9,8},{10,11... | collective-permute-start | bytes 1572872 | tf_op jit(solution)/shard_map/ppermute | solution.py:44
where the time goes:
time: 83.6 us; the launch traced here: 83.3 us
  blocking collectives  35 us (42%)
  waiting for transfers between devices  17.3 us (21%)
  starting transfers between devices  15.2 us (18%)
  Pallas kernels  14.9 us (18%)
    all_to_all x1, blocking collectives, body(): lax.all_to_all(summed.reshape(groups * uppers, capacity, quarter), ('sp',...  21 us
    ppermute x15, waiting for transfers between devices, exchange(): return lax.ppermute(values, axis, [(i, i ^ mask) for i in range(size)])  17.3 us
    ppermute x15, starting transfers between devices, exchange(): return lax.ppermute(values, axis, [(i, i ^ mask) for i in range(size)])  15.2 us
    pallas_call x10, Pallas kernels, call(): pl.pallas_call(wrapped, out_shape=list(outs) + [held_shape(a.shape, a.dty...  14.9 us
    all_to_all x1, blocking collectives, body(): lax.all_to_all(placed, 'sp', split_axis=0, concat_axis=0, tiled=True)  13.9 us
  transfers between devices with their start and end apart: 15, of which 7 were waited for; matrix products, arithmetic and copies ran while one was open for 0% of the time, Pallas kernels for 10%

commit v1 on v0

--- a/solution.py
+++ b/solution.py
@@ -91,8 +91,8 @@
     tokens = wide_ref.shape[0]
     heads_w = wide_ref.shape[1] // (PLAIN_WIDTH_WIDE + ROPE)
     heads_n = slim_ref.shape[1] // (PLAIN_WIDTH_SLIM + ROPE)
-    cosine, sine = cos_ref[...], sin_ref[...]
     spare = jnp.zeros((tokens, LANES - ROPE), F32)
+    cosine, sine = cos_ref[...].T, sin_ref[...].T
     for h in range(heads_w + heads_n):
         wide = h < heads_w
         plain = PLAIN_WIDTH_WIDE if wide else PLAIN_WIDTH_SLIM
@@ -117,38 +117,34 @@
     ]
 
 
-def attend_body(q_ref, stacks, kw_ref, vw_ref, kn_ref, vn_ref, state, masks):
-    count = len(stacks) // 2
-    mine, other = pieces_of(stacks[:count]), pieces_of(stacks[count:])
+def attend_body(queries, pieces, masks, mine, kw_ref, vw_ref, kn_ref, vn_ref, state):
     heads_w = kw_ref.shape[1] // PLAIN_WIDTH_WIDE
     heads_n = kn_ref.shape[1] // PLAIN_WIDTH_SLIM
-    half = mine[0].shape[0]
-    tokens = q_ref.shape[1]
+    half = pieces[0].shape[0]
+    tokens = queries[0].shape[0]
     rank = kw_ref.shape[0]
     place = lax.axis_index("sp")
     core = lax.axis_index("tp") & 1
     shift = half.bit_length() - 1
-    step = 5
-    for start in range(0, len(mine), step):
-        group = mine[start : start + step]
+    step = 8
+    for start in range(0, len(pieces), step):
+        group = pieces[start : start + step]
         rows = len(group) * half
-        lat = jnp.concatenate(group + other[start : start + step], axis=0)
+        lat = jnp.concatenate(group, axis=0)
         flat = lat[:, :rank]
         rot = lat[:, rank:]
         key_w = dot(flat, kw_ref[...]).astype(BF16)
         key_n = dot(flat, kn_ref[...]).astype(BF16)
         val_w = dot(flat, vw_ref[...]).astype(BF16)
         val_n = dot(flat, vn_ref[...]).astype(BF16)
-        lane = iota((1, 2 * rows), 1)
-        first = lane < rows
-        inner = jnp.where(first, lane, lane - rows)
-        piece = inner >> shift
-        mask = jnp.zeros_like(piece)
+        lane = iota((1, rows), 1)
+        index = lane >> shift
+        mask = jnp.zeros_like(lane)
+        offset = jnp.zeros_like(lane)
         for i in range(len(group)):
-            mask = jnp.where(piece == i, masks[start + i], mask)
-        block = place ^ mask
-        offset = jnp.where(first, core, 1 - core)
-        key_pos = (block * 2 + offset) * half + (inner & (half - 1))
+            mask = jnp.where(index == i, masks[start + i], mask)
+            offset = jnp.where(index == i, core if mine[start + i] else 1 - core, offset)
+        key_pos = ((place ^ mask) * 2 + offset) * half + (lane & (half - 1))
         visible = iota((tokens, 1), 0) + place * tokens >= key_pos
         new_state = []
         for h in range(heads_w + heads_n):
@@ -160,7 +156,7 @@
                 keys = key_n
                 values = val_n
                 scale = (PLAIN_WIDTH_SLIM + ROPE) ** (-0.5)
-            scores = dot_t(q_ref[h], jnp.concatenate([keys, rot], axis=1)) * scale
+            scores = dot_t(queries[h], jnp.concatenate([keys, rot], axis=1)) * scale
             scores = jnp.where(visible, scores, MASKED)
             peak = jnp.max(scores, axis=-1, keepdims=True)
             if state is not None:
@@ -177,23 +173,40 @@
     return state
 
 
-def first_kernel(masks, *refs):
-    q_ref, kw_ref, vw_ref, kn_ref, vn_ref = refs[:5]
-    peak_ref, total_ref, acc_ref = refs[-3:]
-    state = attend_body(q_ref, refs[5:-3], kw_ref, vw_ref, kn_ref, vn_ref, None, masks)
+def store_state(state, refs):
+    peak_ref, total_ref, acc_ref = refs
     for h, (peak, total, acc) in enumerate(state):
         peak_ref[h] = jnp.broadcast_to(peak, peak_ref.shape[1:])
         total_ref[h] = jnp.broadcast_to(total, total_ref.shape[1:])
         acc_ref[h] = acc
 
 
-def second_kernel(masks, *refs):
-    q_ref, kw_ref, vw_ref, kn_ref, vn_ref, peak_ref, total_ref, acc_ref, ow_ref, on_ref = refs[:10]
+def load_state(refs):
+    peak_ref, total_ref, acc_ref = refs
+    return [(peak_ref[h, :, :1], total_ref[h, :, :1], acc_ref[h]) for h in range(peak_ref.shape[0])]
+
+
+def first_kernel(masks, q_ref, *refs):
+    lifts, blocks = refs[:4], refs[4:-3]
+    queries = [q_ref[h] for h in range(q_ref.shape[0])]
+    mine = [True] * len(masks) + [False] * len(masks)
+    store_state(attend_body(queries, pieces_of(blocks), masks * 2, mine, *lifts, None), refs[-3:])
+
+
+def second_kernel(masks, q_ref, *refs):
+    lifts, state_refs, blocks = refs[:4], refs[4:7], refs[7:-3]
+    queries = [q_ref[h] for h in range(q_ref.shape[0])]
+    state = attend_body(queries, pieces_of(blocks), masks, [True] * len(masks), *lifts, load_state(state_refs))
+    store_state(state, refs[-3:])
+
+
+def third_kernel(masks, q_ref, *refs):
+    lifts, state_refs, (ow_ref, on_ref), blocks = refs[:4], refs[4:7], refs[7:9], refs[9:-2]
     keep_ref, send_ref = refs[-2:]
-    heads = peak_ref.shape[0]
-    heads_w = kw_ref.shape[1] // PLAIN_WIDTH_WIDE
-    state = [(peak_ref[h, :, :1], total_ref[h, :, :1], acc_ref[h]) for h in range(heads)]
-    state = attend_body(q_ref, refs[10:-2], kw_ref, vw_ref, kn_ref, vn_ref, state, masks)
+    queries = [q_ref[h] for h in range(q_ref.shape[0])]
+    heads = len(queries)
+    heads_w = lifts[0].shape[1] // PLAIN_WIDTH_WIDE
+    state = attend_body(queries, pieces_of(blocks), masks, [False] * len(masks), *lifts, load_state(state_refs))
     done = [acc / total for _, total, acc in state]
     att_w = jnp.concatenate(done[:heads_w], axis=1).astype(BF16)
     slim = done[heads_w]
@@ -221,7 +234,8 @@
     return (iota((groups * capacity, tokens), 0) == slot).astype(BF16)
 
 
-def weights_kernel(masks, *refs):
+def weights_kernel(masks, route_ref, *refs):
+    refs, hot_ref = refs[:-1], refs[-1]
     out_ref = refs[-1]
     count = (len(refs) - 1) // 2
     mine_all, other_all = pieces_of(refs[:count]), pieces_of(refs[count:-1])
@@ -230,6 +244,7 @@
     odd = (lax.axis_index("tp") & 1) == 1
     capacity = out_ref.shape[0] // len(mine_all)
     base = width - LANES
+    hot_ref[...] = slots_of(route_ref[...], len(mine_all), capacity)
     for mask, mine, other in zip(masks, mine_all, other_all):
         mine, other = mine[:, base:], other[:, base:]
         data = jnp.concatenate(
@@ -243,23 +258,28 @@
         out_ref[pl.ds(start, capacity), :] = dot(hot.astype(BF16), data)
 
 
-def place_kernel(keep_ref, got_ref, resid_ref, route_ref, stream_ref, placed_ref):
-    groups, capacity, _ = placed_ref.shape
-    stream = keep_ref[...].astype(F32) + got_ref[...].astype(F32) + resid_ref[...].astype(F32)
+def pair_kernel(masks, keep_ref, got_ref, stay_ref, *send_refs):
+    upper = lax.axis_index("tp") >> 1
+    for ref, mask in zip((stay_ref, *send_refs), [0] + masks):
+        piece = upper ^ (mask >> 1)
+        ref[...] = (keep_ref[piece].astype(F32) + got_ref[piece].astype(F32)).astype(BF16)
+
+
+def place_kernel(resid_ref, hot_ref, *refs):
+    stream_ref, placed_ref = refs[-2:]
+    stream = resid_ref[...].astype(F32)
+    for ref in refs[:-2]:
+        stream = stream + ref[...].astype(F32)
     stream = stream.astype(BF16)
     stream_ref[...] = stream
-    hot = slots_of(route_ref[...], groups, capacity)
-    placed_ref[...] = dot(hot, stream).astype(BF16).reshape(placed_ref.shape)
-
-
-def final_kernel(stream_ref, back_ref, route_ref, out_ref):
-    groups, copies, capacity, quarter = back_ref.shape
-    hot = slots_of(route_ref[...], groups, capacity)
-    total = stream_ref[...].astype(F32)
-    for copy in range(copies):
-        rows = back_ref[:, copy].reshape(groups * capacity, quarter)
-        total = total + lax.dot_general(hot, rows, (((0,), (0,)), ((), ())), preferred_element_type=F32)
-    out_ref[...] = total.astype(BF16)
+    placed_ref[...] = dot(hot_ref[...], stream).astype(BF16).reshape(placed_ref.shape)
+
+
+def final_kernel(stream_ref, back_ref, hot_ref, out_ref):
+    groups, capacity, quarter = back_ref.shape
+    rows = back_ref[...].reshape(groups * capacity, quarter)
+    moe = lax.dot_general(hot_ref[...], rows, (((0,), (0,)), ((), ())), preferred_element_type=F32)
+    out_ref[...] = (stream_ref[...].astype(F32) + moe).astype(BF16)
 
 
 def expand_part(masks, gain_ref, gate_ref, up_ref, parts, acts, square):
@@ -285,31 +305,76 @@
     square_ref[...] = jnp.broadcast_to(square, square_ref.shape)
 
 
-def contract(hidden, down_ref, out_ref, bit):
-    groups, uppers, capacity, quarter = out_ref.shape
-    for upper in range(uppers):
-        cols = pl.ds(pl.multiple_of((2 * upper + bit) * quarter, LANES), quarter)
-        out_ref[:, upper] = dot(hidden, down_ref[:, cols]).astype(BF16).reshape(groups, capacity, quarter)
-
-
-def far_kernel(masks, gain_ref, gate_ref, up_ref, down_ref, weight_ref, act_ref, square_ref, *refs):
-    send_ref, hidden_ref = refs[-2:]
+def places_of(weight_ref, span, experts):
+    firsts, seconds = [], []
+    seen = 0.0
+    for e in range(experts):
+        chosen = jnp.where(weight_ref[span, ROPE + e : ROPE + e + 1] != 0.0, 1.0, 0.0)
+        firsts.append((chosen > 0.0) & (seen == 0.0))
+        seconds.append((chosen > 0.0) & (seen == 1.0))
+        seen = seen + chosen
+    return firsts, seconds
+
+
+def far_kernel(masks, gain_ref, gate_ref, up_ref, weight_ref, act_ref, square_ref, *refs):
+    hidden_ref, pair_ref = refs[-2:]
+    halves = (refs[: len(masks)], refs[len(masks) : -2])
     experts, model_width, hidden_width = gate_ref.shape
-    acts = [act_ref[e] for e in range(experts)]
-    square = expand_part(masks, gain_ref, gate_ref, up_ref, refs[:-2], acts, square_ref[:, :1])
-    scale = lax.rsqrt(square / model_width + EPSILON)
-    hidden = []
-    for e in range(experts):
-        gate, up = acts[e][:, :hidden_width] * scale, acts[e][:, hidden_width:] * scale
-        weight = weight_ref[:, ROPE + e : ROPE + e + 1]
-        hidden.append((gate / (1.0 + jnp.exp(-gate)) * up * weight).astype(BF16))
-    hidden = jnp.concatenate(hidden, axis=1)
-    hidden_ref[...] = hidden
-    contract(hidden, down_ref, send_ref, 1 - (lax.axis_index("tp") & 1))
-
-
-def stay_kernel(hidden_ref, down_ref, keep_ref):
-    contract(hidden_ref[...], down_ref, keep_ref, lax.axis_index("tp") & 1)
+    rows = hidden_ref.shape[0] // 2
+    for first, parts in zip((0, rows), halves):
+        span = slice(first, first + rows)
+        acts = [act_ref[e, span, :] for e in range(experts)]
+        square = expand_part(masks, gain_ref, gate_ref, up_ref, parts, acts, square_ref[span, :1])
+        scale = lax.rsqrt(square / model_width + EPSILON)
+        firsts, seconds = places_of(weight_ref, span, experts)
+        pair = [jnp.zeros((rows, hidden_width), F32)] * 2
+        for e in range(experts):
+            gate, up = acts[e][:, :hidden_width] * scale, acts[e][:, hidden_width:] * scale
+            weight = weight_ref[span, ROPE + e : ROPE + e + 1]
+            hidden = gate / (1.0 + jnp.exp(-gate)) * up * weight
+            hidden_ref[span, e * hidden_width : (e + 1) * hidden_width] = hidden.astype(BF16)
+            pair = [jnp.where(firsts[e], hidden, pair[0]), jnp.where(seconds[e], hidden, pair[1])]
+        pair_ref[span, :] = jnp.concatenate(pair, axis=1).astype(BF16)
+
+
+def own_kernel(hidden_ref, down_ref, send_ref, keep_ref):
+    place = lax.axis_index("tp")
+    quarter = send_ref.shape[1]
+    hidden = hidden_ref[...]
+    for ref, mask in ((send_ref, 1), (keep_ref, 0)):
+        cols = pl.ds(pl.multiple_of((place ^ mask) * quarter, LANES), quarter)
+        ref[...] = dot(hidden, down_ref[:, cols])
+
+
+def join_kernel(weight_ref, part_send_ref, part_keep_ref, *refs):
+    send_ref, keep_ref = refs[-2:]
+    count = (len(refs) - 2) // 3
+    pairs, lows, highs = refs[:count], refs[count : 2 * count], refs[2 * count : -2]
+    rows, quarter = send_ref.shape
+    width = pairs[0].shape[1] // 2
+    half_rows = lows[0].shape[0]
+    experts = 2 * half_rows // width
+    firsts, seconds = places_of(weight_ref, slice(0, rows), experts)
+    send, keep = part_send_ref[...], part_keep_ref[...]
+    core = lax.axis_index("tp") & 1
+    for pair_ref, low_ref, high_ref in zip(pairs, lows, highs):
+        pair = pair_ref[...]
+        zero = jnp.zeros((rows, width), F32)
+        one, two = pair[:, :width].astype(F32), pair[:, width:].astype(F32)
+        hidden = jnp.concatenate(
+            [jnp.where(firsts[e], one, jnp.where(seconds[e], two, zero)) for e in range(experts)], axis=1
+        ).astype(BF16)
+        for which, ref in enumerate((low_ref, high_ref)):
+            part = hidden[:, which * half_rows : (which + 1) * half_rows]
+            for bit in range(2):
+                cols = pl.ds(pl.multiple_of((core ^ bit) * quarter, LANES), quarter)
+                product = dot(part, ref[:, cols])
+                if bit:
+                    send = send + product
+                else:
+                    keep = keep + product
+    send_ref[...] = send.astype(BF16)
+    keep_ref[...] = keep.astype(BF16)
 
 
 def start_copies(sources, targets, semaphores):
@@ -322,7 +387,10 @@
     return copies
 
 
-def call(kernel, outs, inputs, fetched=(), kept=(), mib=12):
+def call(kernel, outs, inputs, fetched=(), kept=(), cuts=(), mib=12):
+    whole = lambda ref: ref
+    pieces = [(a, whole, a.shape) for a in kept] + list(cuts)
+    kept = [a for a, _, _ in pieces]
     n_in, n_fetched, n_kept, n_out = len(inputs), len(fetched), len(kept), len(outs)
 
     def wrapped(*refs):
@@ -331,6 +399,7 @@
         ins, sources, kept_sources = take(n_in), take(n_fetched), take(n_kept)
         results, kept_results, held = take(n_out), take(n_kept), take(n_fetched)
         first = start_copies(sources, held, refs[0]) if n_fetched else []
+        kept_sources = [piece[1](source) for piece, source in zip(pieces, kept_sources)]
         second = start_copies(kept_sources, kept_results, refs[-1]) if n_kept else []
         for copy in first:
             copy.wait()
@@ -341,7 +410,7 @@
     semaphores = [pltpu.SemaphoreType.DMA((n,)) for n in (n_fetched, n_kept) if n]
     return pl.pallas_call(
         wrapped,
-        out_shape=list(outs) + [held_shape(a.shape, a.dtype) for a in kept],
+        out_shape=list(outs) + [held_shape(dims, a.dtype) for a, _, dims in pieces],
         in_specs=[VMEM] * n_in + [HBM] * (n_fetched + n_kept),
         out_specs=[VMEM] * (n_out + n_kept),
         scratch_shapes=[pltpu.VMEM(a.shape, a.dtype) for a in fetched] + semaphores,
@@ -358,21 +427,6 @@
 
 def held_shape(dims, dtype=BF16):
     return pltpu.VMEM(dims, dtype)
-
-
-def halved(keep, got, first_bit, place):
-    pieces = [keep[i].astype(F32) + got[i].astype(F32) for i in range(keep.shape[0])]
-    bit = first_bit
-    while True:
-        mine = ((place >> bit) & 1) == 1
-        low, high = pieces[0::2], pieces[1::2]
-        send = [jnp.where(mine, a, b).astype(BF16) for a, b in zip(low, high)]
-        stay = [jnp.where(mine, b, a) for a, b in zip(low, high)]
-        if len(send) == 1:
-            return stay[0].astype(BF16), exchange(send[0], "tp", 1 << bit)
-        came = exchange(jnp.stack(send), "tp", 1 << bit)
-        pieces = [a + came[i].astype(F32) for i, a in enumerate(stay)]
-        bit += 1
 
 
 def body(
@@ -401,19 +455,29 @@
     groups = lax.axis_size("sp")
     tp_size = lax.axis_size("tp")
     place = lax.axis_index("sp")
-    lane_place = lax.axis_index("tp")
     half = tokens // 2
     capacity = 2 * tokens // groups
     slots = groups * capacity
     model_width = resid.shape[1]
     quarter = model_width // tp_size
     route = group_route[None, :]
+    far_masks = list(range(2, tp_size, 2))
+    down_rows = down_weight[0].reshape(-1, model_width)
+
+    def resid_cut(ref):
+        return ref.at[:, pl.ds(pl.multiple_of(lax.axis_index("tp") * quarter, LANES), quarter)]
+
+    def down_cut(mask, which, ref):
+        rows, width = down_rows.shape[0] // 2, 2 * quarter
+        upper = (lax.axis_index("tp") ^ mask) >> 1
+        return ref.at[pl.ds(which * rows, rows), pl.ds(pl.multiple_of(upper * width, LANES), width)]
 
     query_pos = place * tokens + jnp.arange(tokens, dtype=jnp.int32)
     table = angles(query_pos, ROPE).T
     packed = held_shape((half, rank + LANES))
+    tables = [jnp.cos(table), jnp.sin(table)]
     own, rest = call(
-        pack_kernel, [packed, packed], [jnp.cos(table), jnp.sin(table)],
+        pack_kernel, [packed, packed], tables,
         [latent, rope_key.T, latent_norm_weight[None, :], route, expert_pair.T, group_prob[None, :], expert_prob.T],
         mib=4,
     )
@@ -422,55 +486,63 @@
     got = []
     for k in strides:
         got.append(exchange(own, "sp", k))
-    across = [exchange(own, "sp", 1)]
-    across_rest = [exchange(across[0], "tp", 1)]
-    cut = len(strides) // 2
-    for pieces in (got[:cut], got[cut:]):
-        across.append(exchange(jnp.stack(pieces), "sp", 1))
+    beside = exchange(own, "sp", 1)
+    across = [beside[None], exchange(beside, "sp", strides[-1])[None]]
+    across.append(exchange(jnp.stack(got[:-1]), "sp", 1))
     column = [own, jnp.stack(got)]
     column_rest = [rest, exchange(column[1], "tp", 1)]
-    across = [across[0], jnp.concatenate(across[1:])]
-    across_rest.append(exchange(across[1], "tp", 1))
-    first_masks = [0] + strides + [1]
-    second_masks = [k ^ 1 for k in strides]
-
+    across = jnp.concatenate(across)
+    across_rest = exchange(across, "tp", 1)
+    first_masks = [0] + strides
+    second_masks = [1, strides[-1] ^ 1] + [k ^ 1 for k in strides[:-1]]
     heads = query_wide.shape[1] // (PLAIN_WIDTH_WIDE + ROPE) + query_narrow.shape[1] // (PLAIN_WIDTH_SLIM + ROPE)
-    angle_rows = angles(query_pos, ROPE)
-    queries, key_w, value_w, key_n, value_n, out_w, out_n = call(
-        query_kernel, [held_shape((heads, tokens, 2 * LANES))], [jnp.cos(angle_rows), jnp.sin(angle_rows)],
-        [query_wide, query_narrow],
-        [broad_key_lift, broad_value_lift, slim_key_lift, slim_value_lift, out_wide, out_narrow], mib=4,
-    )
-    lifts = [key_w, value_w, key_n, value_n]
+    queries, *weights = call(
+        query_kernel, [held_shape((heads, tokens, 2 * LANES))], tables, [query_wide, query_narrow],
+        [broad_key_lift, broad_value_lift, slim_key_lift, slim_value_lift, out_wide, out_narrow],
+        [
+            (down_rows, functools.partial(down_cut, mask, which), (down_rows.shape[0] // 2, 2 * quarter))
+            for mask in far_masks
+            for which in range(2)
+        ],
+        mib=4,
+    )
+    lifts, out_weights, down_cuts = weights[:4], weights[4:6], weights[6:]
+    down_low = [exchange(down_cuts[2 * i], "tp", mask) for i, mask in enumerate(far_masks)]
+    down_high = [exchange(down_cuts[2 * i + 1], "tp", mask) for i, mask in enumerate(far_masks)]
+    state_shape = [held_shape((heads, tokens, LANES), F32)] * 3
+    state = call(functools.partial(first_kernel, first_masks), state_shape, [queries, *lifts, *column, *column_rest])
     state = call(
-        functools.partial(first_kernel, first_masks), [held_shape((heads, tokens, LANES), F32)] * 3,
-        [queries, *lifts, *column, across[0], *column_rest, across_rest[0]],
-    )
-    pieces_shape = held_shape((tp_size // 2, tokens, quarter))
+        functools.partial(second_kernel, second_masks), state_shape, [queries, *lifts, *state, across]
+    )
     keep, send = call(
-        functools.partial(second_kernel, second_masks), [pieces_shape] * 2,
-        [queries, *lifts, *state, out_w, out_n, *across[1:], *across_rest[1:]],
-    )
-    slot_weights, gate, up, down, gain = call(
-        functools.partial(weights_kernel, first_masks + second_masks), [held_shape((slots, LANES), F32)],
-        [*column, *across, *column_rest, *across_rest], [],
-        [gate_weight[0], up_weight[0], down_weight[0].reshape(-1, model_width), ffn_gain[None, :]], mib=4,
+        functools.partial(third_kernel, second_masks), [held_shape((tp_size // 2, tokens, quarter))] * 2,
+        [queries, *lifts, *state, *out_weights, across_rest],
+    )
+    slot_weights, hot, gate, up, down, gain, resid_cols = call(
+        functools.partial(weights_kernel, first_masks + second_masks),
+        [held_shape((slots, LANES), F32), held_shape((slots, tokens))],
+        [route, *column, across, *column_rest, across_rest], [],
+        [gate_weight[0], up_weight[0], down_rows, ffn_gain[None, :]],
+        [(resid, resid_cut, (tokens, quarter))], mib=4,
     )
 
     received = exchange(send, "tp", 1)
-    stay, came = halved(keep, received, 1, lane_place)
-    resid_cols = lax.dynamic_slice_in_dim(resid, lane_place * quarter, quarter, 1)
+    thin_rows = held_shape((tokens, quarter))
+    stay, *sends = call(
+        functools.partial(pair_kernel, far_masks), [thin_rows] * (1 + len(far_masks)), [keep, received], mib=4
+    )
+    came = [exchange(part, "tp", mask) for part, mask in zip(sends, far_masks)]
     stream_cols, placed = call(
-        place_kernel, [held_shape((tokens, quarter)), held_shape((groups, capacity, quarter))],
-        [stay, came, resid_cols, route], mib=4,
+        place_kernel, [thin_rows, held_shape((groups, capacity, quarter))],
+        [resid_cols, hot, stay, *came], mib=4,
     )
 
     routed = lax.all_to_all(placed, "sp", split_axis=0, concat_axis=0, tiled=True)
     routed = routed.reshape(slots, quarter)
-    far_masks = list(range(2, tp_size, 2))
+    part_rows = slots // 2
     far = []
-    for mask in far_masks:
-        far.append(exchange(routed, "tp", mask))
+    for first in (0, part_rows):
+        far.append([exchange(routed[first : first + part_rows], "tp", mask) for mask in far_masks])
     near = exchange(routed, "tp", 1)
     experts, _, hidden_width = gate_weight[0].shape
     acts, square = call(
@@ -478,26 +550,25 @@
         [held_shape((experts, slots, 2 * hidden_width), F32), held_shape((slots, LANES), F32)],
         [gain, gate, up, routed, near],
     )
-    far_near = [exchange(part, "tp", 1) for part in far]
-    uppers = tp_size // 2
-    cube = held_shape((groups, uppers, capacity, quarter))
-    send, hidden = call(
+    far_near = []
+    for part in range(2):
+        far_near.append([exchange(rows, "tp", 1) for rows in far[part]])
+    hidden, pair = call(
         functools.partial(far_kernel, far_masks + [m | 1 for m in far_masks]),
-        [cube, held_shape((slots, experts * hidden_width))],
-        [gain, gate, up, down, slot_weights, acts, square, *far, *far_near],
-    )
+        [held_shape((slots, experts * hidden_width)), held_shape((slots, 2 * hidden_width))],
+        [gain, gate, up, slot_weights, acts, square, *far[0], *far_near[0], *far[1], *far_near[1]],
+    )
+    pairs = [exchange(pair, "tp", mask) for mask in far_masks]
+    wide = held_shape((slots, quarter), F32)
+    thin = held_shape((slots, quarter))
+    part_send, part_keep = call(own_kernel, [wide, wide], [hidden, down])
+    send, keep = call(join_kernel, [thin, thin], [slot_weights, part_send, part_keep, *pairs, *down_low, *down_high])
     received = exchange(send, "tp", 1)
-    (keep,) = call(stay_kernel, [cube], [hidden, down])
-
-    teams = [
-        [g * tp_size + 2 * upper + low for g in range(groups) for upper in range(uppers)] for low in range(2)
-    ]
     summed = (keep.astype(F32) + received.astype(F32)).astype(BF16)
     returned = lax.all_to_all(
-        summed.reshape(groups * uppers, capacity, quarter),
-        ("sp", "tp"), split_axis=0, concat_axis=0, axis_index_groups=teams, tiled=True,
-    ).reshape(cube.shape)
-    return call(final_kernel, [shape((tokens, quarter))], [stream_cols, returned, route], mib=4)[0]
+        summed.reshape(groups, capacity, quarter), "sp", split_axis=0, concat_axis=0, tiled=True
+    )
+    return call(final_kernel, [shape((tokens, quarter))], [stream_cols, returned, hot], mib=4)[0]
 
 
 def solution(mesh):

time: 83.6 us -> 105 us (1.26)
  waiting for transfers between devices: 17.3 us -> 42.7 us
  blocking collectives: 35 us -> 14.7 us
  local copies, waits for them, and re-layouts: 0.05 us -> 7.26 us
  starting transfers between devices: 15.2 us -> 21.2 us
  Pallas kernels: 14.9 us -> 18.3 us
    all_to_all x2 -> x1, blocking collectives: 35 us -> 14.7 us  [body(): lax.all_to_all(summed.reshape(groups, capacity, quarter), 'sp', split_axi...]
    ppermute x15 -> x19, waiting for transfers between devices: 17.3 us -> 35.6 us  [exchange(): return lax.ppermute(values, axis, [(i, i ^ mask) for i in range(size)])]
    unnamed x5 -> x22, local copies, waits for them, and re-layouts: 0.02 us -> 7.25 us
    all_to_all x0 -> x1, waiting for transfers between devices: none -> 7.15 us  [body(): lax.all_to_all(placed, 'sp', split_axis=0, concat_axis=0, tiled=True)]
    all_to_all x0 -> x1, starting transfers between devices: none -> 3.97 us  [body(): lax.all_to_all(placed, 'sp', split_axis=0, concat_axis=0, tiled=True)]
    pallas_call x10 -> x13, Pallas kernels: 14.9 us -> 18.3 us  [call(): pl.pallas_call(wrapped, out_shape=list(outs) + [held_shape(dims, a.dtype)...]
    ppermute x15 -> x19, starting transfers between devices: 15.2 us -> 17.3 us  [exchange(): return lax.ppermute(values, axis, [(i, i ^ mask) for i in range(size)])]
  transfers between devices with their start and end apart: 15 -> 20, of which waited for: 7 -> 10; matrix products, arithmetic and copies ran while one was open for 0% -> 0% of each run, Pallas kernels for 10% -> 12%
where the time goes in v1:
time: 105 us
  waiting for transfers between devices  42.7 us (41%)
  starting transfers between devices  21.2 us (20%)
  Pallas kernels  18.3 us (17%)
  blocking collectives  14.7 us (14%)
  local copies, waits for them, and re-layouts  7.26 us (7%)
    ppermute x19, waiting for transfers between devices, exchange(): return lax.ppermute(values, axis, [(i, i ^ mask) for i in range(size)])  35.6 us
    pallas_call x13, Pallas kernels, call(): pl.pallas_call(wrapped, out_shape=list(outs) + [held_shape(dims, a.dtype)...  18.3 us
    ppermute x19, starting transfers between devices, exchange(): return lax.ppermute(values, axis, [(i, i ^ mask) for i in range(size)])  17.3 us
    all_to_all x1, blocking collectives, body(): lax.all_to_all(summed.reshape(groups, capacity, quarter), 'sp', split_axi...  14.7 us
    unnamed x22, local copies, waits for them, and re-layouts  7.25 us
    all_to_all x1, waiting for transfers between devices, body(): lax.all_to_all(placed, 'sp', split_axis=0, concat_axis=0, tiled=True)  7.15 us
    all_to_all x1, starting transfers between devices, body(): lax.all_to_all(placed, 'sp', split_axis=0, concat_axis=0, tiled=True)  3.97 us
  transfers between devices with their start and end apart: 20, of which 10 were waited for; matrix products, arithmetic and copies ran while one was open for 0% of the time, Pallas kernels for 12%

profile of v1, /device:TPU:0, one launch (start us, length us, event | category | flops | bytes accessed | tf_op | source)
XLA Modules:
  0.0 104.8 jit_solution(5459046714958282556)
XLA Ops:
  0.0 0.1 multiply_sine_fusion
  0.2 1.1 %shard_map.190 = (bf16[64,640]{1,0:T(8,128)(2,1)S(1)}, bf16[64,640]{1,0:T(8,128)(2,1)S(1)}) custom-call(f32[32,128]{1,0:T(8,128)S(1)} %get-tuple-element.84.refs_0_, f32[32,128]{1,0:T(8,128)S(1)} %get-tuple-element.83.refs_1_, bf16[128,512]{1,0:T(8,128)(2,1)} %refs_2_.2, bf16[64,128]{1,0:T(8,128)(2,1)} %bitcast.38, f32[1,512]{1,0:T(1,128)} %bitcast.40, ...), custom_call_target="tpu_custom_call" | custom-call | tf_op jit(solution)/shard_map/pallas_call | solution.py:411
  1.3 5.1 %collective-permute-start = (bf16[64,640]{1,0:T(8,128)(2,1)S(1)}, bf16[64,640]{1,0:T(8,128)(2,1)S(1)}, u32[]{:S(2)}, u32[]{:S(2)}) collective-permute-start(bf16[64,640]{1,0:T(8,128)(2,1)S(1)} %get-tuple-element.43.refs_1_.refs_5_), channel_id=1, source_target_pairs={{0,24},{4,28},{8,16},{12,20},{16,8},{20,12},{24,0},{28,4},{1,25},{... | collective-permute-start | bytes 245768 | tf_op jit(solution)/shard_map/ppermute | solution.py:44
  6.5 0.0 collective-permute-start.1
  6.5 1.5 %collective-permute-start.3 = (bf16[64,640]{1,0:T(8,128)(2,1)S(1)}, bf16[64,640]{1,0:T(8,128)(2,1)S(1)}, u32[]{:S(2)}, u32[]{:S(2)}) collective-permute-start(bf16[64,640]{1,0:T(8,128)(2,1)S(1)} %get-tuple-element.43.refs_1_.refs_5_), channel_id=1, source_target_pairs={{0,4},{4,0},{8,12},{12,8},{16,20},{20,16},{24,28},{28,24},{1,5},{5... | collective-permute-start | bytes 245768 | tf_op jit(solution)/shard_map/ppermute | solution.py:44
  8.0 1.5 %collective-permute-done = bf16[64,640]{1,0:T(8,128)(2,1)S(1)} collective-permute-done((bf16[64,640]{1,0:T(8,128)(2,1)S(1)}, bf16[64,640]{1,0:T(8,128)(2,1)S(1)}, u32[]{:S(2)}, u32[]{:S(2)}) %collective-permute-start) | collective-permute-done | bytes 81952 | tf_op jit(solution)/shard_map/ppermute | solution.py:44
  9.4 3.9 %collective-permute-done.1 = bf16[64,640]{1,0:T(8,128)(2,1)S(1)} collective-permute-done((bf16[64,640]{1,0:T(8,128)(2,1)S(1)}, bf16[64,640]{1,0:T(8,128)(2,1)S(1)}, u32[]{:S(2)}, u32[]{:S(2)}) %collective-permute-start.1) | collective-permute-done | bytes 81952 | tf_op jit(solution)/shard_map/ppermute | solution.py:44
  13.3 1.6 %collective-permute-start.5 = (bf16[2,64,640]{2,1,0:T(8,128)(2,1)S(1)}, bf16[2,64,640]{2,1,0:T(8,128)(2,1)S(1)}, u32[]{:S(2)}, u32[]{:S(2)}) collective-permute-start(bf16[2,64,640]{2,1,0:T(8,128)(2,1)S(1)} %pad_maximum_fusion.2), channel_id=1, source_target_pairs={{0,4},{4,0},{8,12},{12,8},{16,20},{20,16},{24,28},{28,24},{1,5},{5... | collective-permute-start | bytes 491528 | tf_op jit(solution)/shard_map/ppermute | solution.py:44
  14.9 0.0 collective-permute-done.3
  14.9 0.0 collective-permute-start.4
  14.9 2.0 %collective-permute-start.2 = (bf16[64,640]{1,0:T(8,128)(2,1)S(1)}, bf16[64,640]{1,0:T(8,128)(2,1)S(1)}, u32[]{:S(2)}, u32[]{:S(2)}) collective-permute-start(bf16[64,640]{1,0:T(8,128)(2,1)S(1)} %get-tuple-element.43.refs_1_.refs_5_), channel_id=1, source_target_pairs={{0,8},{4,12},{8,0},{12,4},{16,24},{20,28},{24,16},{28,20},{1,9},{5... | collective-permute-start | bytes 245768 | tf_op jit(solution)/shard_map/ppermute | solution.py:44
  16.9 2.4 %collective-permute-done.4 = bf16[64,640]{1,0:T(8,128)(2,1)S(1)} collective-permute-done((bf16[64,640]{1,0:T(8,128)(2,1)S(1)}, bf16[64,640]{1,0:T(8,128)(2,1)S(1)}, u32[]{:S(2)}, u32[]{:S(2)}) %collective-permute-start.4) | collective-permute-done | bytes 81952 | tf_op jit(solution)/shard_map/ppermute | solution.py:44
  19.3 0.0 collective-permute-done.5
  19.4 0.1 collective-permute-start.7
  19.5 0.7 collective-permute-done.2
  20.3 0.1 collective-permute-start.6
  20.3 3.2 %shard_map.192 = (bf16[4,128,256]{2,1,0:T(8,128)(2,1)S(1)}, bf16[512,256]{1,0:T(8,128)(2,1)S(1)}, bf16[512,256]{1,0:T(8,128)(2,1)S(1)}, bf16[512,128]{1,0:T(8,12...) custom-call(f32[32,128]{1,0:T(8,128)S(1)} %get-tuple-element.84.refs, ...), custom_call_target="tpu_custom_call" | custom-call | tf_op jit(solution)/shard_map/pallas_call | solution.py:411
  23.6 0.8 copy-done.10
  24.4 0.0 collective-permute-done.6.refs_5_.refs_8_
  24.4 1.9 %shard_map.193 = (f32[4,128,128]{2,1,0:T(8,128)S(1)}, f32[4,128,128]{2,1,0:T(8,128)S(1)}, f32[4,128,128]{2,1,0:T(8,128)S(1)}) custom-call(bf16[4,128,256]{2,1,0:T(8,128)(2,1)S(1)} %get-tuple-element.47.refs_0_, bf16[512,256]{1,0:T(8,128)(2,1)S(1)} %get-tuple-element.48.refs_1_, bf16[512,256]{1,0:T(8,128)(2,1)S(1)} %get-tuple-element.49.refs_2_, ...), custom_call_target="tpu_custom_call" | custom-call | tf_op jit(solution)/shard_map/pallas_call | solution.py:411
  26.3 1.6 %shard_map.194 = (f32[4,128,128]{2,1,0:T(8,128)S(1)}, f32[4,128,128]{2,1,0:T(8,128)S(1)}, f32[4,128,128]{2,1,0:T(8,128)S(1)}) custom-call(bf16[4,128,256]{2,1,0:T(8,128)(2,1)S(1)} %get-tuple-element.47.refs_0_, bf16[512,256]{1,0:T(8,128)(2,1)S(1)} %get-tuple-element.48.refs_1_, bf16[512,256]{1,0:T(8,128)(2,1)S(1)} %get-tuple-element.49.refs_2_, ...), custom_call_target="tpu_custom_call" | custom-call | tf_op jit(solution)/shard_map/pallas_call | solution.py:411
  28.0 0.0 collective-permute-done.7.refs_6_.refs_10_
  28.0 0.0 copy-start.9
  28.0 2.1 %shard_map.195 = (bf16[2,128,512]{2,1,0:T(8,128)(2,1)S(1)}, bf16[2,128,512]{2,1,0:T(8,128)(2,1)S(1)}) custom-call(bf16[4,128,256]{2,1,0:T(8,128)(2,1)S(1)} %get-tuple-element.47.refs_0_, bf16[512,256]{1,0:T(8,128)(2,1)S(1)} %get-tuple-element.48.refs_1_, bf16[512,256]{1,0:T(8,128)(2,1)S(1)} %get-tuple-element.49.refs_2_, ...), custom_call_target="tpu_custom_call" | custom-call | tf_op jit(solution)/shard_map/pallas_call | solution.py:411
  30.1 0.5 collective-permute-start.8
  30.6 1.2 %collective-permute-done.8.refs_1_ = bf16[2,128,512]{2,1,0:T(8,128)(2,1)S(1)} collective-permute-done((bf16[2,128,512]{2,1,0:T(8,128)(2,1)S(1)}, bf16[2,128,512]{2,1,0:T(8,128)(2,1)S(1)}, u32[]{:S(2)}, u32[]{:S(2)}) %collective-permute-start.8) | collective-permute-done | bytes 262176 | tf_op jit(solution)/shard_map/ppermute | solution.py:44
  31.8 0.1 shard_map.196
  31.8 1.6 %collective-permute-start.9 = (bf16[128,512]{1,0:T(8,128)(2,1)S(1)}, bf16[128,512]{1,0:T(8,128)(2,1)S(1)}, u32[]{:S(2)}, u32[]{:S(2)}) collective-permute-start(bf16[128,512]{1,0:T(8,128)(2,1)S(1)} %get-tuple-element.63), channel_id=1, source_target_pairs={{0,2},{1,3},{2,0},{3,1},{4,6},{5,7},{6,4},{7,5},{8,10},{9,11},{10,... | collective-permute-start | bytes 393224 | tf_op jit(solution)/shard_map/ppermute | solution.py:44
  33.4 3.0 %shard_map.191 = (f32[256,128]{1,0:T(8,128)S(1)}, bf16[256,128]{1,0:T(8,128)(2,1)S(1)}, bf16[4,2048,128]{2,1,0:T(8,128)(2,1)S(1)}, bf16[4,2048,128]{2,1,0:T(8,12...) custom-call(s32[1,128]{1,0:T(1,128)S(1)} %bitcast.22, ...), custom_call_target="tpu_custom_call" | custom-call | tf_op jit(solution)/shard_map/pallas_call | solution.py:411
  36.4 1.3 %copy-done = bf16[4,2048,128]{2,1,0:T(8,128)(2,1)} copy-done((bf16[4,2048,128]{2,1,0:T(8,128)(2,1)}, bf16[4,2048,128]{2,1,0:T(8,128)(2,1)S(1)}, u32[]{:S(2)}) %copy-start) | copy-done | bytes 2097176
  37.7 1.3 %copy-done.3 = bf16[512,2048]{1,0:T(8,128)(2,1)} copy-done((bf16[512,2048]{1,0:T(8,128)(2,1)}, bf16[512,2048]{1,0:T(8,128)(2,1)S(1)}, u32[]{:S(2)}) %copy-start.3) | copy-done | bytes 2097176
  39.1 0.0 collective-permute-done.9.refs_3_
  39.1 1.0 shard_map.197
  40.1 0.6 copy-done.5
  40.7 0.7 copy-done.7
  41.3 4.0 %all-to-all-start = ((bf16[8,32,512]{2,1,0:T(8,128)(2,1)}), bf16[8,32,512]{2,1,0:T(8,128)(2,1)S(1)}, u32[]{:S(2)}, u32[]{:S(2)}) async-start(bf16[8,32,512]{2,1,0:T(8,128)(2,1)} %get-tuple-element.69), calls=%async_computation | async-start | bytes 524288 | tf_op jit(solution)/shard_map/all_to_all | solution.py:540
  45.3 0.5 collective-permute-start.16
  45.8 1.5 %collective-permute-start.17 = (bf16[256,1024]{1,0:T(8,128)(2,1)}, bf16[256,1024]{1,0:T(8,128)(2,1)S(1)}, u32[]{:S(2)}, u32[]{:S(2)}) collective-permute-start(bf16[256,1024]{1,0:T(8,128)(2,1)} %copy-done.10), channel_id=1, source_target_pairs={{0,2},{1,3},{2,0},{3,1},{4,6},{5,7},{6,4},{7,5},{8,10},{9,11},{10,... | collective-permute-start | bytes 1572872 | tf_op jit(solution)/shard_map/ppermute | solution.py:44
  47.3 7.1 %all-to-all-done = bf16[8,32,512]{2,1,0:T(8,128)(2,1)S(1)} async-done(((bf16[8,32,512]{2,1,0:T(8,128)(2,1)}), bf16[8,32,512]{2,1,0:T(8,128)(2,1)S(1)}, u32[]{:S(2)}, u32[]{:S(2)}) %all-to-all-start) | async-done | bytes 262176 | tf_op jit(solution)/shard_map/all_to_all | solution.py:540
  54.5 0.0 collective-permute-start.10
  54.5 0.6 collective-permute-start.11
  55.1 1.5 %collective-permute-start.13 = (bf16[128,512]{1,0:T(8,128)(2,1)S(1)}, bf16[128,512]{1,0:T(8,128)(2,1)S(1)}, u32[]{:S(2)}, u32[]{:S(2)}) collective-permute-start(bf16[128,512]{1,0:T(8,128)(2,1)S(1)} %bitcast.33), channel_id=1, source_target_pairs={{0,2},{1,3},{2,0},{3,1},{4,6},{5,7},{6,4},{7,5},{8,10},{9,11},{10,... | collective-permute-start | bytes 393224 | tf_op jit(solution)/shard_map/ppermute | solution.py:44
  56.6 17.8 %collective-permute-done.11.refs_6_ = bf16[128,512]{1,0:T(8,128)(2,1)S(1)} collective-permute-done((bf16[128,512]{1,0:T(8,128)(2,1)S(1)}, bf16[128,512]{1,0:T(8,128)(2,1)S(1)}, u32[]{:S(2)}, u32[]{:S(2)}) %collective-permute-start.11) | collective-permute-done | bytes 131104 | tf_op jit(solution)/shard_map/ppermute | solution.py:44
  74.4 0.0 collective-permute-start.12
  74.4 1.6 %collective-permute-done.13.refs_8_ = bf16[128,512]{1,0:T(8,128)(2,1)S(1)} collective-permute-done((bf16[128,512]{1,0:T(8,128)(2,1)S(1)}, bf16[128,512]{1,0:T(8,128)(2,1)S(1)}, u32[]{:S(2)}, u32[]{:S(2)}) %collective-permute-start.13) | collective-permute-done | bytes 131104 | tf_op jit(solution)/shard_map/ppermute | solution.py:44
  76.0 0.0 collective-permute-start.14
  76.0 0.0 collective-permute-done.10.refs_4_
  76.0 1.6 %copy-done.1 = bf16[4,2048,128]{2,1,0:T(8,128)(2,1)S(1)} copy-done((bf16[4,2048,128]{2,1,0:T(8,128)(2,1)S(1)}, bf16[4,2048,128]{2,1,0:T(8,128)(2,1)}, u32[]{:S(2)}) %copy-start.1) | copy-done | bytes 2097176
  77.6 0.7 shard_map.198
  78.3 0.0 collective-permute-done.12.refs_7_
  78.3 0.0 collective-permute-done.14.refs_9_
  78.3 0.9 copy-done.2
  79.2 1.4 %shard_map.199 = (bf16[256,512]{1,0:T(8,128)(2,1)S(1)}, bf16[256,256]{1,0:T(8,128)(2,1)S(1)}) custom-call(f32[1,2048]{1,0:T(1,128)S(1)} %get-tuple-element.66.refs_0_, bf16[4,2048,128]{2,1,0:T(8,128)(2,1)S(1)} %get-tuple-element.67.refs_1_, bf16[4,2048,128]{2,1,0:T(8,128)(2,1)S(1)} %copy-done.2, f32[256,128]{1,0:T(8,128)S(1)} %get-tuple-element.65.refs_3_.refs_0_, ...), custom_call_target="tpu_custom_call" | custom-call | tf_op jit(solution)/shard_map/pallas_call | solution.py:411
  80.6 0.6 collective-permute-start.15
  81.1 0.4 shard_map.200
  81.6 0.0 copy-start.8
  81.6 0.0 collective-permute-done.16.refs_4_
  81.6 4.9 %collective-permute-done.15.refs_3_ = bf16[256,256]{1,0:T(8,128)(2,1)S(1)} collective-permute-done((bf16[256,256]{1,0:T(8,128)(2,1)S(1)}, bf16[256,256]{1,0:T(8,128)(2,1)S(1)}, u32[]{:S(2)}, u32[]{:S(2)}) %collective-permute-start.15) | collective-permute-done | bytes 131104 | tf_op jit(solution)/shard_map/ppermute | solution.py:44
  86.5 1.0 shard_map.201
  87.5 0.1 collective-permute-start.18
  87.6 1.5 %collective-permute-done.18 = bf16[256,512]{1,0:T(8,128)(2,1)S(1)} collective-permute-done((bf16[256,512]{1,0:T(8,128)(2,1)S(1)}, bf16[256,512]{1,0:T(8,128)(2,1)S(1)}, u32[]{:S(2)}, u32[]{:S(2)}) %collective-permute-start.18) | collective-permute-done | bytes 262176 | tf_op jit(solution)/shard_map/ppermute | solution.py:44
  89.1 0.1 add_convert_fusion
  89.2 14.7 %all_to_all.10.refs_1_ = bf16[8,32,512]{2,1,0:T(8,128)(2,1)S(1)} all-to-all(bf16[8,32,512]{2,1,0:T(8,128)(2,1)S(1)} %bitcast.28), channel_id=1, replica_groups=mesh['sp'=8,'tp'=4] {'sp'}, dimensions={0} | all-to-all | bytes 524288 | tf_op jit(solution)/shard_map/all_to_all | solution.py:568
  103.9 0.9 shard_map.202
  (20 shorter events, 0.2 us)
Async XLA Ops:
  1.3 8.1 %collective-permute-start = (bf16[64,640]{1,0:T(8,128)(2,1)S(1)}, bf16[64,640]{1,0:T(8,128)(2,1)S(1)}, u32[]{:S(2)}, u32[]{:S(2)}) collective-permute-start(bf16[64,640]{1,0:T(8,128)(2,1)S(1)} %get-tuple-element.43.refs_1_.refs_5_), channel_id=1, source_target_pairs={{0,24},{4,28},{8,16},{12,20},{16,8},{20,12},{24,0},{28,4},{1,25},{... | collective-permute-start | bytes 245768 | tf_op jit(solution)/shard_map/ppermute | solution.py:44
  6.5 6.9 %collective-permute-start.1 = (bf16[64,640]{1,0:T(8,128)(2,1)S(1)}, bf16[64,640]{1,0:T(8,128)(2,1)S(1)}, u32[]{:S(2)}, u32[]{:S(2)}) collective-permute-start(bf16[64,640]{1,0:T(8,128)(2,1)S(1)} %get-tuple-element.43.refs_1_.refs_5_), channel_id=1, source_target_pairs={{0,16},{4,20},{8,24},{12,28},{16,0},{20,4},{24,8},{28,12},{1,17},{... | collective-permute-start | bytes 245768 | tf_op jit(solution)/shard_map/ppermute | solution.py:44
  6.5 8.4 %collective-permute-start.3 = (bf16[64,640]{1,0:T(8,128)(2,1)S(1)}, bf16[64,640]{1,0:T(8,128)(2,1)S(1)}, u32[]{:S(2)}, u32[]{:S(2)}) collective-permute-start(bf16[64,640]{1,0:T(8,128)(2,1)S(1)} %get-tuple-element.43.refs_1_.refs_5_), channel_id=1, source_target_pairs={{0,4},{4,0},{8,12},{12,8},{16,20},{20,16},{24,28},{28,24},{1,5},{5... | collective-permute-start | bytes 245768 | tf_op jit(solution)/shard_map/ppermute | solution.py:44
  13.3 6.0 %collective-permute-start.5 = (bf16[2,64,640]{2,1,0:T(8,128)(2,1)S(1)}, bf16[2,64,640]{2,1,0:T(8,128)(2,1)S(1)}, u32[]{:S(2)}, u32[]{:S(2)}) collective-permute-start(bf16[2,64,640]{2,1,0:T(8,128)(2,1)S(1)} %pad_maximum_fusion.2), channel_id=1, source_target_pairs={{0,4},{4,0},{8,12},{12,8},{16,20},{20,16},{24,28},{28,24},{1,5},{5... | collective-permute-start | bytes 491528 | tf_op jit(solution)/shard_map/ppermute | solution.py:44
  14.9 4.4 %collective-permute-start.4 = (bf16[64,640]{1,0:T(8,128)(2,1)S(1)}, bf16[64,640]{1,0:T(8,128)(2,1)S(1)}, u32[]{:S(2)}, u32[]{:S(2)}) collective-permute-start(bf16[64,640]{1,0:T(8,128)(2,1)S(1)} %collective-permute-done.3), channel_id=1, source_target_pairs={{0,8},{4,12},{8,0},{12,4},{16,24},{20,28},{24,16},{28,20},{1,9},{5... | collective-permute-start | bytes 245768 | tf_op jit(solution)/shard_map/ppermute | solution.py:44
  14.9 5.3 %collective-permute-start.2 = (bf16[64,640]{1,0:T(8,128)(2,1)S(1)}, bf16[64,640]{1,0:T(8,128)(2,1)S(1)}, u32[]{:S(2)}, u32[]{:S(2)}) collective-permute-start(bf16[64,640]{1,0:T(8,128)(2,1)S(1)} %get-tuple-element.43.refs_1_.refs_5_), channel_id=1, source_target_pairs={{0,8},{4,12},{8,0},{12,4},{16,24},{20,28},{24,16},{28,20},{1,9},{5... | collective-permute-start | bytes 245768 | tf_op jit(solution)/shard_map/ppermute | solution.py:44
  19.4 8.6 %collective-permute-start.7 = (bf16[4,64,640]{2,1,0:T(8,128)(2,1)S(1)}, bf16[4,64,640]{2,1,0:T(8,128)(2,1)S(1)}, u32[]{:S(2)}, u32[]{:S(2)}) collective-permute-start(bf16[4,64,640]{2,1,0:T(8,128)(2,1)S(1)} %pad_maximum_fusion.refs_3_.refs_8_), channel_id=1, source_target_pairs={{0,1},{1,0},{2,3},{3,2},{4,5},{5,4},{6,7},{7,6},{8,9},{9,8},{10,11... | collective-permute-start | bytes 983048 | tf_op jit(solution)/shard_map/ppermute | solution.py:44
  20.3 4.2 %collective-permute-start.6 = (bf16[3,64,640]{2,1,0:T(8,128)(2,1)S(1)}, bf16[3,64,640]{2,1,0:T(8,128)(2,1)S(1)}, u32[]{:S(2)}, u32[]{:S(2)}) collective-permute-start(bf16[3,64,640]{2,1,0:T(8,128)(2,1)S(1)} %pad_maximum_fusion.1.refs_2_.refs_6_), channel_id=1, source_target_pairs={{0,1},{1,0},{2,3},{3,2},{4,5},{5,4},{6,7},{7,6},{8,9},{9,8},{10,11... | collective-permute-start | bytes 737288 | tf_op jit(solution)/shard_map/ppermute | solution.py:44
  23.6 0.8 copy-start.10
  28.0 5.4 %copy-start.9 = (s32[128]{0:T(128)S(1)}, s32[128]{0:T(128)}, u32[]{:S(2)}) copy-start(s32[128]{0:T(128)} %param.33) | copy-start | bytes 1540
  30.1 1.7 %collective-permute-start.8 = (bf16[2,128,512]{2,1,0:T(8,128)(2,1)S(1)}, bf16[2,128,512]{2,1,0:T(8,128)(2,1)S(1)}, u32[]{:S(2)}, u32[]{:S(2)}) collective-permute-start(bf16[2,128,512]{2,1,0:T(8,128)(2,1)S(1)} %get-tuple-element.61), channel_id=1, source_target_pairs={{0,1},{1,0},{2,3},{3,2},{4,5},{5,4},{6,7},{7,6},{8,9},{9,8},{10,11... | collective-permute-start | bytes 786440 | tf_op jit(solution)/shard_map/ppermute | solution.py:44
  31.8 7.3 %collective-permute-start.9 = (bf16[128,512]{1,0:T(8,128)(2,1)S(1)}, bf16[128,512]{1,0:T(8,128)(2,1)S(1)}, u32[]{:S(2)}, u32[]{:S(2)}) collective-permute-start(bf16[128,512]{1,0:T(8,128)(2,1)S(1)} %get-tuple-element.63), channel_id=1, source_target_pairs={{0,2},{1,3},{2,0},{3,1},{4,6},{5,7},{6,4},{7,5},{8,10},{9,11},{10,... | collective-permute-start | bytes 393224 | tf_op jit(solution)/shard_map/ppermute | solution.py:44
  36.4 1.4 %copy-start = (bf16[4,2048,128]{2,1,0:T(8,128)(2,1)}, bf16[4,2048,128]{2,1,0:T(8,128)(2,1)S(1)}, u32[]{:S(2)}) copy-start(bf16[4,2048,128]{2,1,0:T(8,128)(2,1)S(1)} %get-tuple-element.68.refs_2_) | copy-start | bytes 6291460
  37.7 1.3 %copy-start.3 = (bf16[512,2048]{1,0:T(8,128)(2,1)}, bf16[512,2048]{1,0:T(8,128)(2,1)S(1)}, u32[]{:S(2)}) copy-start(bf16[512,2048]{1,0:T(8,128)(2,1)S(1)} %get-tuple-element.73.refs_1_) | copy-start | bytes 6291460
  40.1 0.6 copy-start.5
  40.7 0.7 copy-start.7
  41.3 13.1 %all-to-all-start = ((bf16[8,32,512]{2,1,0:T(8,128)(2,1)}), bf16[8,32,512]{2,1,0:T(8,128)(2,1)S(1)}, u32[]{:S(2)}, u32[]{:S(2)}) async-start(bf16[8,32,512]{2,1,0:T(8,128)(2,1)} %get-tuple-element.69), calls=%async_computation | async-start | bytes 524288 | tf_op jit(solution)/shard_map/all_to_all | solution.py:540
  45.3 36.3 %collective-permute-start.16 = (bf16[256,1024]{1,0:T(8,128)(2,1)}, bf16[256,1024]{1,0:T(8,128)(2,1)S(1)}, u32[]{:S(2)}, u32[]{:S(2)}) collective-permute-start(bf16[256,1024]{1,0:T(8,128)(2,1)} %get-tuple-element.77), channel_id=1, source_target_pairs={{0,2},{1,3},{2,0},{3,1},{4,6},{5,7},{6,4},{7,5},{8,10},{9,11},{10,... | collective-permute-start | bytes 1572872 | tf_op jit(solution)/shard_map/ppermute | solution.py:44
  45.8 35.8 %collective-permute-start.17 = (bf16[256,1024]{1,0:T(8,128)(2,1)}, bf16[256,1024]{1,0:T(8,128)(2,1)S(1)}, u32[]{:S(2)}, u32[]{:S(2)}) collective-permute-start(bf16[256,1024]{1,0:T(8,128)(2,1)} %copy-done.10), channel_id=1, source_target_pairs={{0,2},{1,3},{2,0},{3,1},{4,6},{5,7},{6,4},{7,5},{8,10},{9,11},{10,... | collective-permute-start | bytes 1572872 | tf_op jit(solution)/shard_map/ppermute | solution.py:44
  54.5 21.5 %collective-permute-start.10 = (bf16[256,512]{1,0:T(8,128)(2,1)S(1)}, bf16[256,512]{1,0:T(8,128)(2,1)S(1)}, u32[]{:S(2)}, u32[]{:S(2)}) collective-permute-start(bf16[256,512]{1,0:T(8,128)(2,1)S(1)} %bitcast.19), channel_id=1, source_target_pairs={{0,1},{1,0},{2,3},{3,2},{4,5},{5,4},{6,7},{7,6},{8,9},{9,8},{10,11... | collective-permute-start | bytes 786440 | tf_op jit(solution)/shard_map/ppermute | solution.py:44
  54.5 19.9 %collective-permute-start.11 = (bf16[128,512]{1,0:T(8,128)(2,1)S(1)}, bf16[128,512]{1,0:T(8,128)(2,1)S(1)}, u32[]{:S(2)}, u32[]{:S(2)}) collective-permute-start(bf16[128,512]{1,0:T(8,128)(2,1)S(1)} %bitcast.34), channel_id=1, source_target_pairs={{0,2},{1,3},{2,0},{3,1},{4,6},{5,7},{6,4},{7,5},{8,10},{9,11},{10,... | collective-permute-start | bytes 393224 | tf_op jit(solution)/shard_map/ppermute | solution.py:44
  55.1 20.9 %collective-permute-start.13 = (bf16[128,512]{1,0:T(8,128)(2,1)S(1)}, bf16[128,512]{1,0:T(8,128)(2,1)S(1)}, u32[]{:S(2)}, u32[]{:S(2)}) collective-permute-start(bf16[128,512]{1,0:T(8,128)(2,1)S(1)} %bitcast.33), channel_id=1, source_target_pairs={{0,2},{1,3},{2,0},{3,1},{4,6},{5,7},{6,4},{7,5},{8,10},{9,11},{10,... | collective-permute-start | bytes 393224 | tf_op jit(solution)/shard_map/ppermute | solution.py:44
  74.4 4.0 %collective-permute-start.12 = (bf16[128,512]{1,0:T(8,128)(2,1)S(1)}, bf16[128,512]{1,0:T(8,128)(2,1)S(1)}, u32[]{:S(2)}, u32[]{:S(2)}) collective-permute-start(bf16[128,512]{1,0:T(8,128)(2,1)S(1)} %collective-permute-done.11.refs_6_), channel_id=1, source_target_pairs={{0,1},{1,0},{2,3},{3,2},{4,5},{5,4},{6,7},{7,6},{8,9},{9,8},{10,11... | collective-permute-start | bytes 393224 | tf_op jit(solution)/shard_map/ppermute | solution.py:44
  76.0 2.3 %collective-permute-start.14 = (bf16[128,512]{1,0:T(8,128)(2,1)S(1)}, bf16[128,512]{1,0:T(8,128)(2,1)S(1)}, u32[]{:S(2)}, u32[]{:S(2)}) collective-permute-start(bf16[128,512]{1,0:T(8,128)(2,1)S(1)} %collective-permute-done.13.refs_8_), channel_id=1, source_target_pairs={{0,1},{1,0},{2,3},{3,2},{4,5},{5,4},{6,7},{7,6},{8,9},{9,8},{10,11... | collective-permute-start | bytes 393224 | tf_op jit(solution)/shard_map/ppermute | solution.py:44
  76.0 1.6 %copy-start.1 = (bf16[4,2048,128]{2,1,0:T(8,128)(2,1)S(1)}, bf16[4,2048,128]{2,1,0:T(8,128)(2,1)}, u32[]{:S(2)}) copy-start(bf16[4,2048,128]{2,1,0:T(8,128)(2,1)} %copy-done) | copy-start | bytes 6291460
  77.6 1.6 %copy-start.2 = (bf16[4,2048,128]{2,1,0:T(8,128)(2,1)S(1)}, bf16[4,2048,128]{2,1,0:T(8,128)(2,1)}, u32[]{:S(2)}) copy-start(bf16[4,2048,128]{2,1,0:T(8,128)(2,1)} %copy-done) | copy-start | bytes 6291460
  79.2 1.9 %copy-start.4 = (bf16[512,2048]{1,0:T(8,128)(2,1)S(1)}, bf16[512,2048]{1,0:T(8,128)(2,1)}, u32[]{:S(2)}) copy-start(bf16[512,2048]{1,0:T(8,128)(2,1)} %copy-done.3) | copy-start | bytes 6291460
  80.6 6.0 %collective-permute-start.15 = (bf16[256,256]{1,0:T(8,128)(2,1)S(1)}, bf16[256,256]{1,0:T(8,128)(2,1)S(1)}, u32[]{:S(2)}, u32[]{:S(2)}) collective-permute-start(bf16[256,256]{1,0:T(8,128)(2,1)S(1)} %get-tuple-element.76), channel_id=1, source_target_pairs={{0,2},{1,3},{2,0},{3,1},{4,6},{5,7},{6,4},{7,5},{8,10},{9,11},{10,... | collective-permute-start | bytes 393224 | tf_op jit(solution)/shard_map/ppermute | solution.py:44
  81.6 22.3 %copy-start.6 = (bf16[256,128]{1,0:T(8,128)(2,1)S(1)}, bf16[256,128]{1,0:T(8,128)(2,1)}, u32[]{:S(2)}) copy-start(bf16[256,128]{1,0:T(8,128)(2,1)} %copy-done.5) | copy-start | bytes 196612
  81.6 22.3 %copy-start.8 = (bf16[128,512]{1,0:T(8,128)(2,1)S(1)}, bf16[128,512]{1,0:T(8,128)(2,1)}, u32[]{:S(2)}) copy-start(bf16[128,512]{1,0:T(8,128)(2,1)} %copy-done.7) | copy-start | bytes 393220
  87.5 1.6 %collective-permute-start.18 = (bf16[256,512]{1,0:T(8,128)(2,1)S(1)}, bf16[256,512]{1,0:T(8,128)(2,1)S(1)}, u32[]{:S(2)}, u32[]{:S(2)}) collective-permute-start(bf16[256,512]{1,0:T(8,128)(2,1)S(1)} %get-tuple-element.80), channel_id=1, source_target_pairs={{0,1},{1,0},{2,3},{3,2},{4,5},{5,4},{6,7},{7,6},{8,9},{9,8},{10,11... | collective-permute-start | bytes 786440 | tf_op jit(solution)/shard_map/ppermute | solution.py:44

commit v2 on v1

--- a/solution.py
+++ b/solution.py
@@ -201,8 +201,8 @@
 
 
 def third_kernel(masks, q_ref, *refs):
-    lifts, state_refs, (ow_ref, on_ref), blocks = refs[:4], refs[4:7], refs[7:9], refs[9:-2]
-    keep_ref, send_ref = refs[-2:]
+    lifts, state_refs, (ow_ref, on_ref), blocks = refs[:4], refs[4:7], refs[7:9], refs[9:-3]
+    send_ref, att_w_ref, att_n_ref = refs[-3:]
     queries = [q_ref[h] for h in range(q_ref.shape[0])]
     heads = len(queries)
     heads_w = lifts[0].shape[1] // PLAIN_WIDTH_WIDE
@@ -214,9 +214,9 @@
         lane = iota(slim.shape, 1)
         slim = jnp.where(lane >= h * VALUE_WIDTH_SLIM, done[heads_w + h], slim)
     att_n = slim.astype(BF16)
-    core = lax.axis_index("tp") & 1
-    project(att_w, att_n, ow_ref, on_ref, send_ref, 1 - core)
-    project(att_w, att_n, ow_ref, on_ref, keep_ref, core)
+    att_w_ref[...] = att_w
+    att_n_ref[...] = att_n
+    project(att_w, att_n, ow_ref, on_ref, send_ref, 1 - (lax.axis_index("tp") & 1))
 
 
 def project(att_w, att_n, ow_ref, on_ref, out_ref, bit):
@@ -224,6 +224,10 @@
     for piece in range(pieces):
         cols = pl.ds(pl.multiple_of((2 * piece + bit) * quarter, LANES), quarter)
         out_ref[piece] = (dot(att_w, ow_ref[:, cols]) + dot(att_n, on_ref[:, cols])).astype(BF16)
+
+
+def keep_kernel(att_w_ref, att_n_ref, ow_ref, on_ref, keep_ref):
+    project(att_w_ref[...], att_n_ref[...], ow_ref, on_ref, keep_ref, lax.axis_index("tp") & 1)
 
 
 def slots_of(route, groups, capacity):
@@ -316,63 +320,60 @@
     return firsts, seconds
 
 
-def far_kernel(masks, gain_ref, gate_ref, up_ref, weight_ref, act_ref, square_ref, *refs):
+def far_kernel(masks, first, gain_ref, gate_ref, up_ref, weight_ref, act_ref, square_ref, *refs):
     hidden_ref, pair_ref = refs[-2:]
-    halves = (refs[: len(masks)], refs[len(masks) : -2])
     experts, model_width, hidden_width = gate_ref.shape
-    rows = hidden_ref.shape[0] // 2
-    for first, parts in zip((0, rows), halves):
-        span = slice(first, first + rows)
-        acts = [act_ref[e, span, :] for e in range(experts)]
-        square = expand_part(masks, gain_ref, gate_ref, up_ref, parts, acts, square_ref[span, :1])
-        scale = lax.rsqrt(square / model_width + EPSILON)
-        firsts, seconds = places_of(weight_ref, span, experts)
-        pair = [jnp.zeros((rows, hidden_width), F32)] * 2
-        for e in range(experts):
-            gate, up = acts[e][:, :hidden_width] * scale, acts[e][:, hidden_width:] * scale
-            weight = weight_ref[span, ROPE + e : ROPE + e + 1]
-            hidden = gate / (1.0 + jnp.exp(-gate)) * up * weight
-            hidden_ref[span, e * hidden_width : (e + 1) * hidden_width] = hidden.astype(BF16)
-            pair = [jnp.where(firsts[e], hidden, pair[0]), jnp.where(seconds[e], hidden, pair[1])]
-        pair_ref[span, :] = jnp.concatenate(pair, axis=1).astype(BF16)
-
-
-def own_kernel(hidden_ref, down_ref, send_ref, keep_ref):
+    rows = hidden_ref.shape[0]
+    span = slice(first, first + rows)
+    acts = [act_ref[e, span, :] for e in range(experts)]
+    square = expand_part(masks, gain_ref, gate_ref, up_ref, refs[:-2], acts, square_ref[span, :1])
+    scale = lax.rsqrt(square / model_width + EPSILON)
+    firsts, seconds = places_of(weight_ref, span, experts)
+    pair = [jnp.zeros((rows, hidden_width), F32)] * 2
+    for e in range(experts):
+        gate, up = acts[e][:, :hidden_width] * scale, acts[e][:, hidden_width:] * scale
+        weight = weight_ref[span, ROPE + e : ROPE + e + 1]
+        hidden = gate / (1.0 + jnp.exp(-gate)) * up * weight
+        hidden_ref[:, e * hidden_width : (e + 1) * hidden_width] = hidden.astype(BF16)
+        pair = [jnp.where(firsts[e], hidden, pair[0]), jnp.where(seconds[e], hidden, pair[1])]
+    pair_ref[...] = jnp.concatenate(pair, axis=1).astype(BF16)
+
+
+def own_kernel(down_ref, *refs):
+    send_ref, keep_ref = refs[-2:]
     place = lax.axis_index("tp")
     quarter = send_ref.shape[1]
-    hidden = hidden_ref[...]
+    hidden = jnp.concatenate([ref[...] for ref in refs[:-2]], axis=0)
     for ref, mask in ((send_ref, 1), (keep_ref, 0)):
         cols = pl.ds(pl.multiple_of((place ^ mask) * quarter, LANES), quarter)
         ref[...] = dot(hidden, down_ref[:, cols])
 
 
-def join_kernel(weight_ref, part_send_ref, part_keep_ref, *refs):
+def join_kernel(count, first, weight_ref, part_send_ref, part_keep_ref, *refs):
     send_ref, keep_ref = refs[-2:]
-    count = (len(refs) - 2) // 3
-    pairs, lows, highs = refs[:count], refs[count : 2 * count], refs[2 * count : -2]
+    lows, highs, pairs = refs[:count], refs[count : 2 * count], refs[2 * count : -2]
     rows, quarter = send_ref.shape
     width = pairs[0].shape[1] // 2
     half_rows = lows[0].shape[0]
     experts = 2 * half_rows // width
-    firsts, seconds = places_of(weight_ref, slice(0, rows), experts)
-    send, keep = part_send_ref[...], part_keep_ref[...]
+    span = slice(first, first + rows)
+    firsts, seconds = places_of(weight_ref, span, experts)
+    send, keep = part_send_ref[span, :], part_keep_ref[span, :]
     core = lax.axis_index("tp") & 1
-    for pair_ref, low_ref, high_ref in zip(pairs, lows, highs):
-        pair = pair_ref[...]
+    for i in range(count):
+        pair = pairs[i][...]
         zero = jnp.zeros((rows, width), F32)
         one, two = pair[:, :width].astype(F32), pair[:, width:].astype(F32)
         hidden = jnp.concatenate(
             [jnp.where(firsts[e], one, jnp.where(seconds[e], two, zero)) for e in range(experts)], axis=1
         ).astype(BF16)
-        for which, ref in enumerate((low_ref, high_ref)):
-            part = hidden[:, which * half_rows : (which + 1) * half_rows]
-            for bit in range(2):
-                cols = pl.ds(pl.multiple_of((core ^ bit) * quarter, LANES), quarter)
-                product = dot(part, ref[:, cols])
-                if bit:
-                    send = send + product
-                else:
-                    keep = keep + product
+        for bit in range(2):
+            cols = pl.ds(pl.multiple_of((core ^ bit) * quarter, LANES), quarter)
+            product = dot(hidden, jnp.concatenate([lows[i][:, cols], highs[i][:, cols]], axis=0))
+            if bit:
+                send = send + product
+            else:
+                keep = keep + product
     send_ref[...] = send.astype(BF16)
     keep_ref[...] = keep.astype(BF16)
 
@@ -514,10 +515,13 @@
     state = call(
         functools.partial(second_kernel, second_masks), state_shape, [queries, *lifts, *state, across]
     )
-    keep, send = call(
-        functools.partial(third_kernel, second_masks), [held_shape((tp_size // 2, tokens, quarter))] * 2,
+    pieces_shape = held_shape((tp_size // 2, tokens, quarter))
+    send, att_w, att_n = call(
+        functools.partial(third_kernel, second_masks),
+        [pieces_shape, held_shape((tokens, out_wide.shape[0])), held_shape((tokens, out_narrow.shape[0]))],
         [queries, *lifts, *state, *out_weights, across_rest],
     )
+    (keep,) = call(keep_kernel, [pieces_shape], [att_w, att_n, *out_weights], mib=4)
     slot_weights, hot, gate, up, down, gain, resid_cols = call(
         functools.partial(weights_kernel, first_masks + second_masks),
         [held_shape((slots, LANES), F32), held_shape((slots, tokens))],
@@ -550,23 +554,29 @@
         [held_shape((experts, slots, 2 * hidden_width), F32), held_shape((slots, LANES), F32)],
         [gain, gate, up, routed, near],
     )
-    far_near = []
+    hidden, pairs = [], []
     for part in range(2):
-        far_near.append([exchange(rows, "tp", 1) for rows in far[part]])
-    hidden, pair = call(
-        functools.partial(far_kernel, far_masks + [m | 1 for m in far_masks]),
-        [held_shape((slots, experts * hidden_width)), held_shape((slots, 2 * hidden_width))],
-        [gain, gate, up, slot_weights, acts, square, *far[0], *far_near[0], *far[1], *far_near[1]],
-    )
-    pairs = [exchange(pair, "tp", mask) for mask in far_masks]
+        far_near = [exchange(rows, "tp", 1) for rows in far[part]]
+        units, pair = call(
+            functools.partial(far_kernel, far_masks + [m | 1 for m in far_masks], part * part_rows),
+            [held_shape((part_rows, experts * hidden_width)), held_shape((part_rows, 2 * hidden_width))],
+            [gain, gate, up, slot_weights, acts, square, *far[part], *far_near],
+        )
+        hidden.append(units)
+        pairs.append([exchange(pair, "tp", mask) for mask in far_masks])
     wide = held_shape((slots, quarter), F32)
-    thin = held_shape((slots, quarter))
-    part_send, part_keep = call(own_kernel, [wide, wide], [hidden, down])
-    send, keep = call(join_kernel, [thin, thin], [slot_weights, part_send, part_keep, *pairs, *down_low, *down_high])
-    received = exchange(send, "tp", 1)
-    summed = (keep.astype(F32) + received.astype(F32)).astype(BF16)
+    thin = held_shape((part_rows, quarter))
+    part_send, part_keep = call(own_kernel, [wide, wide], [down, *hidden])
+    summed = []
+    for part in range(2):
+        send, keep = call(
+            functools.partial(join_kernel, len(far_masks), part * part_rows), [thin, thin],
+            [slot_weights, part_send, part_keep, *down_low, *down_high, *pairs[part]],
+        )
+        received = exchange(send, "tp", 1)
+        summed.append((keep.astype(F32) + received.astype(F32)).astype(BF16))
     returned = lax.all_to_all(
-        summed.reshape(groups, capacity, quarter), "sp", split_axis=0, concat_axis=0, tiled=True
+        jnp.concatenate(summed).reshape(groups, capacity, quarter), "sp", split_axis=0, concat_axis=0, tiled=True
     )
     return call(final_kernel, [shape((tokens, quarter))], [stream_cols, returned, hot], mib=4)[0]
 

time: 105 us -> 108 us (1.029)
  local copies, waits for them, and re-layouts: 7.26 us -> 8.41 us
    unnamed x22 -> x24, local copies, waits for them, and re-layouts: 7.25 us -> 8.39 us
    ppermute x19 -> x21, waiting for transfers between devices: 35.6 us -> 36.6 us  [exchange(): return lax.ppermute(values, axis, [(i, i ^ mask) for i in range(size)])]
    ppermute x19 -> x21, starting transfers between devices: 17.3 us -> 17.9 us  [exchange(): return lax.ppermute(values, axis, [(i, i ^ mask) for i in range(size)])]
    pallas_call x13 -> x16, Pallas kernels: 18.3 us -> 18 us  [call(): pl.pallas_call(wrapped, out_shape=list(outs) + [held_shape(dims, a.dtype)...]
  transfers between devices with their start and end apart: 20 -> 22, of which waited for: 10 -> 11; matrix products, arithmetic and copies ran while one was open for 0% -> 0% of each run, Pallas kernels for 12% -> 11%
where the time goes in v2:
time: 108 us; the launch traced here: 107 us
  waiting for transfers between devices  43.7 us (40%)
  starting transfers between devices  21.9 us (20%)
  Pallas kernels  18 us (17%)
  blocking collectives  14.7 us (14%)
  local copies, waits for them, and re-layouts  8.41 us (8%)
    ppermute x21, waiting for transfers between devices, exchange(): return lax.ppermute(values, axis, [(i, i ^ mask) for i in range(size)])  36.6 us
    pallas_call x16, Pallas kernels, call(): pl.pallas_call(wrapped, out_shape=list(outs) + [held_shape(dims, a.dtype)...  18 us
    ppermute x21, starting transfers between devices, exchange(): return lax.ppermute(values, axis, [(i, i ^ mask) for i in range(size)])  17.9 us
    all_to_all x1, blocking collectives, body(): lax.all_to_all(jnp.concatenate(summed).reshape(groups, capacity, quarter)...  14.7 us
    unnamed x24, local copies, waits for them, and re-layouts  8.39 us
    all_to_all x1, waiting for transfers between devices, body(): lax.all_to_all(placed, 'sp', split_axis=0, concat_axis=0, tiled=True)  7.15 us
    all_to_all x1, starting transfers between devices, body(): lax.all_to_all(placed, 'sp', split_axis=0, concat_axis=0, tiled=True)  3.96 us
  transfers between devices with their start and end apart: 22, of which 11 were waited for; matrix products, arithmetic and copies ran while one was open for 0% of the time, Pallas kernels for 11%

profile of v2, /device:TPU:0, one launch (start us, length us, event | category | flops | bytes accessed | tf_op | source)
XLA Modules:
  0.0 107.4 jit_solution(9060833157489229991)
XLA Ops:
  0.0 0.1 multiply_sine_fusion
  0.2 1.1 %shard_map.190 = (bf16[64,640]{1,0:T(8,128)(2,1)S(1)}, bf16[64,640]{1,0:T(8,128)(2,1)S(1)}) custom-call(f32[32,128]{1,0:T(8,128)S(1)} %get-tuple-element.94.refs_0_, f32[32,128]{1,0:T(8,128)S(1)} %get-tuple-element.93.refs_1_, bf16[128,512]{1,0:T(8,128)(2,1)} %refs_2_.2, bf16[64,128]{1,0:T(8,128)(2,1)} %bitcast.38, f32[1,512]{1,0:T(1,128)} %bitcast.40, ...), custom_call_target="tpu_custom_call" | custom-call | tf_op jit(solution)/shard_map/pallas_call | solution.py:412
  1.3 5.1 %collective-permute-start = (bf16[64,640]{1,0:T(8,128)(2,1)S(1)}, bf16[64,640]{1,0:T(8,128)(2,1)S(1)}, u32[]{:S(2)}, u32[]{:S(2)}) collective-permute-start(bf16[64,640]{1,0:T(8,128)(2,1)S(1)} %get-tuple-element.48.refs_1_.refs_5_), channel_id=1, source_target_pairs={{0,24},{4,28},{8,16},{12,20},{16,8},{20,12},{24,0},{28,4},{1,25},{... | collective-permute-start | bytes 245768 | tf_op jit(solution)/shard_map/ppermute | solution.py:44
  6.5 1.5 %collective-permute-start.3 = (bf16[64,640]{1,0:T(8,128)(2,1)S(1)}, bf16[64,640]{1,0:T(8,128)(2,1)S(1)}, u32[]{:S(2)}, u32[]{:S(2)}) collective-permute-start(bf16[64,640]{1,0:T(8,128)(2,1)S(1)} %get-tuple-element.48.refs_1_.refs_5_), channel_id=1, source_target_pairs={{0,4},{4,0},{8,12},{12,8},{16,20},{20,16},{24,28},{28,24},{1,5},{5... | collective-permute-start | bytes 245768 | tf_op jit(solution)/shard_map/ppermute | solution.py:44
  8.0 1.5 %collective-permute-done = bf16[64,640]{1,0:T(8,128)(2,1)S(1)} collective-permute-done((bf16[64,640]{1,0:T(8,128)(2,1)S(1)}, bf16[64,640]{1,0:T(8,128)(2,1)S(1)}, u32[]{:S(2)}, u32[]{:S(2)}) %collective-permute-start) | collective-permute-done | bytes 81952 | tf_op jit(solution)/shard_map/ppermute | solution.py:44
  9.4 3.9 %collective-permute-done.1 = bf16[64,640]{1,0:T(8,128)(2,1)S(1)} collective-permute-done((bf16[64,640]{1,0:T(8,128)(2,1)S(1)}, bf16[64,640]{1,0:T(8,128)(2,1)S(1)}, u32[]{:S(2)}, u32[]{:S(2)}) %collective-permute-start.1) | collective-permute-done | bytes 81952 | tf_op jit(solution)/shard_map/ppermute | solution.py:44
  13.3 1.6 %collective-permute-start.5 = (bf16[2,64,640]{2,1,0:T(8,128)(2,1)S(1)}, bf16[2,64,640]{2,1,0:T(8,128)(2,1)S(1)}, u32[]{:S(2)}, u32[]{:S(2)}) collective-permute-start(bf16[2,64,640]{2,1,0:T(8,128)(2,1)S(1)} %pad_maximum_fusion.3), channel_id=1, source_target_pairs={{0,4},{4,0},{8,12},{12,8},{16,20},{20,16},{24,28},{28,24},{1,5},{5... | collective-permute-start | bytes 491528 | tf_op jit(solution)/shard_map/ppermute | solution.py:44
  14.9 0.0 collective-permute-done.3
  14.9 0.0 collective-permute-start.4
  14.9 2.0 %collective-permute-start.2 = (bf16[64,640]{1,0:T(8,128)(2,1)S(1)}, bf16[64,640]{1,0:T(8,128)(2,1)S(1)}, u32[]{:S(2)}, u32[]{:S(2)}) collective-permute-start(bf16[64,640]{1,0:T(8,128)(2,1)S(1)} %get-tuple-element.48.refs_1_.refs_5_), channel_id=1, source_target_pairs={{0,8},{4,12},{8,0},{12,4},{16,24},{20,28},{24,16},{28,20},{1,9},{5... | collective-permute-start | bytes 245768 | tf_op jit(solution)/shard_map/ppermute | solution.py:44
  16.9 2.4 %collective-permute-done.4 = bf16[64,640]{1,0:T(8,128)(2,1)S(1)} collective-permute-done((bf16[64,640]{1,0:T(8,128)(2,1)S(1)}, bf16[64,640]{1,0:T(8,128)(2,1)S(1)}, u32[]{:S(2)}, u32[]{:S(2)}) %collective-permute-start.4) | collective-permute-done | bytes 81952 | tf_op jit(solution)/shard_map/ppermute | solution.py:44
  19.3 0.0 collective-permute-done.5
  19.4 0.1 collective-permute-start.7
  19.5 0.7 collective-permute-done.2
  20.3 0.1 collective-permute-start.6
  20.3 2.4 %shard_map.192 = (bf16[4,128,256]{2,1,0:T(8,128)(2,1)S(1)}, bf16[512,256]{1,0:T(8,128)(2,1)S(1)}, bf16[512,256]{1,0:T(8,128)(2,1)S(1)}, bf16[512,128]{1,0:T(8,12...) custom-call(f32[32,128]{1,0:T(8,128)S(1)} %get-tuple-element.94.refs, ...), custom_call_target="tpu_custom_call" | custom-call | tf_op jit(solution)/shard_map/pallas_call | solution.py:412
  22.8 0.8 copy-done.10
  23.6 0.8 copy-done.11
  24.4 0.0 collective-permute-done.6.refs_5_.refs_8_
  24.4 1.9 %shard_map.193 = (f32[4,128,128]{2,1,0:T(8,128)S(1)}, f32[4,128,128]{2,1,0:T(8,128)S(1)}, f32[4,128,128]{2,1,0:T(8,128)S(1)}) custom-call(bf16[4,128,256]{2,1,0:T(8,128)(2,1)S(1)} %get-tuple-element.52.refs_0_, bf16[512,256]{1,0:T(8,128)(2,1)S(1)} %get-tuple-element.53.refs_1_, bf16[512,256]{1,0:T(8,128)(2,1)S(1)} %get-tuple-element.54.refs_2_, ...), custom_call_target="tpu_custom_call" | custom-call | tf_op jit(solution)/shard_map/pallas_call | solution.py:412
  26.3 1.6 %shard_map.194 = (f32[4,128,128]{2,1,0:T(8,128)S(1)}, f32[4,128,128]{2,1,0:T(8,128)S(1)}, f32[4,128,128]{2,1,0:T(8,128)S(1)}) custom-call(bf16[4,128,256]{2,1,0:T(8,128)(2,1)S(1)} %get-tuple-element.52.refs_0_, bf16[512,256]{1,0:T(8,128)(2,1)S(1)} %get-tuple-element.53.refs_1_, bf16[512,256]{1,0:T(8,128)(2,1)S(1)} %get-tuple-element.54.refs_2_, ...), custom_call_target="tpu_custom_call" | custom-call | tf_op jit(solution)/shard_map/pallas_call | solution.py:412
  28.0 2.0 %shard_map.195 = (bf16[2,128,512]{2,1,0:T(8,128)(2,1)S(1)}, bf16[128,256]{1,0:T(8,128)(2,1)S(1)}, bf16[128,128]{1,0:T(8,128)(2,1)S(1)}) custom-call(bf16[4,128,256]{2,1,0:T(8,128)(2,1)S(1)} %get-tuple-element.52.refs_0_, bf16[512,256]{1,0:T(8,128)(2,1)S(1)} %get-tuple-element.53.refs_1_, bf16[512,256]{1,0:T(8,128)(2,1)S(1)} %get-tuple-element.54.refs_2_, ...), custom_call_target="tpu_custom_call" | custom-call | tf_op jit(solution)/shard_map/pallas_call | solution.py:412
  29.9 0.0 copy-start.9
  29.9 0.6 collective-permute-start.8
  30.5 0.3 shard_map.196.refs_0_
  30.8 0.9 collective-permute-done.8.refs_1_
  31.7 0.1 shard_map.197
  31.7 1.6 %collective-permute-start.9 = (bf16[128,512]{1,0:T(8,128)(2,1)S(1)}, bf16[128,512]{1,0:T(8,128)(2,1)S(1)}, u32[]{:S(2)}, u32[]{:S(2)}) collective-permute-start(bf16[128,512]{1,0:T(8,128)(2,1)S(1)} %get-tuple-element.69), channel_id=1, source_target_pairs={{0,2},{1,3},{2,0},{3,1},{4,6},{5,7},{6,4},{7,5},{8,10},{9,11},{10,... | collective-permute-start | bytes 393224 | tf_op jit(solution)/shard_map/ppermute | solution.py:44
  33.3 3.0 %shard_map.191 = (f32[256,128]{1,0:T(8,128)S(1)}, bf16[256,128]{1,0:T(8,128)(2,1)S(1)}, bf16[4,2048,128]{2,1,0:T(8,128)(2,1)S(1)}, bf16[4,2048,128]{2,1,0:T(8,12...) custom-call(s32[1,128]{1,0:T(1,128)S(1)} %bitcast.22, ...), custom_call_target="tpu_custom_call" | custom-call | tf_op jit(solution)/shard_map/pallas_call | solution.py:412
  36.3 1.3 %copy-done = bf16[4,2048,128]{2,1,0:T(8,128)(2,1)} copy-done((bf16[4,2048,128]{2,1,0:T(8,128)(2,1)}, bf16[4,2048,128]{2,1,0:T(8,128)(2,1)S(1)}, u32[]{:S(2)}) %copy-start) | copy-done | bytes 2097176
  37.6 1.3 %copy-done.3 = bf16[512,2048]{1,0:T(8,128)(2,1)} copy-done((bf16[512,2048]{1,0:T(8,128)(2,1)}, bf16[512,2048]{1,0:T(8,128)(2,1)S(1)}, u32[]{:S(2)}) %copy-start.3) | copy-done | bytes 2097176
  39.0 0.0 collective-permute-done.9.refs_3_
  39.0 1.0 shard_map.198
  39.9 0.6 copy-done.5
  40.6 0.7 copy-done.7
  41.2 4.0 %all-to-all-start = ((bf16[8,32,512]{2,1,0:T(8,128)(2,1)}), bf16[8,32,512]{2,1,0:T(8,128)(2,1)S(1)}, u32[]{:S(2)}, u32[]{:S(2)}) async-start(bf16[8,32,512]{2,1,0:T(8,128)(2,1)} %get-tuple-element.76), calls=%async_computation | async-start | bytes 524288 | tf_op jit(solution)/shard_map/all_to_all | solution.py:544
  45.2 0.5 collective-permute-start.15
  45.7 1.5 %collective-permute-start.16 = (bf16[256,1024]{1,0:T(8,128)(2,1)}, bf16[256,1024]{1,0:T(8,128)(2,1)S(1)}, u32[]{:S(2)}, u32[]{:S(2)}) collective-permute-start(bf16[256,1024]{1,0:T(8,128)(2,1)} %copy-done.10), channel_id=1, source_target_pairs={{0,2},{1,3},{2,0},{3,1},{4,6},{5,7},{6,4},{7,5},{8,10},{9,11},{10,... | collective-permute-start | bytes 1572872 | tf_op jit(solution)/shard_map/ppermute | solution.py:44
  47.2 7.1 %all-to-all-done = bf16[8,32,512]{2,1,0:T(8,128)(2,1)S(1)} async-done(((bf16[8,32,512]{2,1,0:T(8,128)(2,1)}), bf16[8,32,512]{2,1,0:T(8,128)(2,1)S(1)}, u32[]{:S(2)}, u32[]{:S(2)}) %all-to-all-start) | async-done | bytes 262176 | tf_op jit(solution)/shard_map/all_to_all | solution.py:544
  54.4 0.0 collective-permute-start.10
  54.4 0.6 collective-permute-start.11
  55.0 1.5 %collective-permute-start.13 = (bf16[128,512]{1,0:T(8,128)(2,1)S(1)}, bf16[128,512]{1,0:T(8,128)(2,1)S(1)}, u32[]{:S(2)}, u32[]{:S(2)}) collective-permute-start(bf16[128,512]{1,0:T(8,128)(2,1)S(1)} %bitcast.33), channel_id=1, source_target_pairs={{0,2},{1,3},{2,0},{3,1},{4,6},{5,7},{6,4},{7,5},{8,10},{9,11},{10,... | collective-permute-start | bytes 393224 | tf_op jit(solution)/shard_map/ppermute | solution.py:44
  56.5 17.8 %collective-permute-done.11.refs_6_ = bf16[128,512]{1,0:T(8,128)(2,1)S(1)} collective-permute-done((bf16[128,512]{1,0:T(8,128)(2,1)S(1)}, bf16[128,512]{1,0:T(8,128)(2,1)S(1)}, u32[]{:S(2)}, u32[]{:S(2)}) %collective-permute-start.11) | collective-permute-done | bytes 131104 | tf_op jit(solution)/shard_map/ppermute | solution.py:44
  74.2 0.0 collective-permute-start.12
  74.2 1.6 %collective-permute-done.13.refs_6_ = bf16[128,512]{1,0:T(8,128)(2,1)S(1)} collective-permute-done((bf16[128,512]{1,0:T(8,128)(2,1)S(1)}, bf16[128,512]{1,0:T(8,128)(2,1)S(1)}, u32[]{:S(2)}, u32[]{:S(2)}) %collective-permute-start.13) | collective-permute-done | bytes 131104 | tf_op jit(solution)/shard_map/ppermute | solution.py:44
  75.9 1.6 %copy-done.1 = bf16[4,2048,128]{2,1,0:T(8,128)(2,1)S(1)} copy-done((bf16[4,2048,128]{2,1,0:T(8,128)(2,1)S(1)}, bf16[4,2048,128]{2,1,0:T(8,128)(2,1)}, u32[]{:S(2)}) %copy-start.1) | copy-done | bytes 2097176
  77.5 0.7 shard_map.199
  78.2 0.9 copy-done.2
  79.1 0.6 shard_map.200
  79.7 0.6 collective-permute-start.17
  80.3 0.7 shard_map.201
  81.0 0.3 copy-done.4
  81.3 0.4 shard_map.202
  81.8 2.5 %collective-permute-done.17.refs_5_ = bf16[128,256]{1,0:T(8,128)(2,1)S(1)} collective-permute-done((bf16[128,256]{1,0:T(8,128)(2,1)S(1)}, bf16[128,256]{1,0:T(8,128)(2,1)S(1)}, u32[]{:S(2)}, u32[]{:S(2)}) %collective-permute-start.17) | collective-permute-done | bytes 65568 | tf_op jit(solution)/shard_map/ppermute | solution.py:44
  84.3 0.7 shard_map.203
  85.0 0.0 copy-start.8
  85.0 0.1 collective-permute-start.18
  85.1 0.6 collective-permute-start.19
  85.7 3.9 %collective-permute-done.19.refs_5_ = bf16[128,256]{1,0:T(8,128)(2,1)S(1)} collective-permute-done((bf16[128,256]{1,0:T(8,128)(2,1)S(1)}, bf16[128,256]{1,0:T(8,128)(2,1)S(1)}, u32[]{:S(2)}, u32[]{:S(2)}) %collective-permute-start.19) | collective-permute-done | bytes 65568 | tf_op jit(solution)/shard_map/ppermute | solution.py:44
  89.6 0.7 shard_map.204
  90.3 0.1 collective-permute-start.20
  90.4 1.3 %collective-permute-done.20 = bf16[128,512]{1,0:T(8,128)(2,1)S(1)} collective-permute-done((bf16[128,512]{1,0:T(8,128)(2,1)S(1)}, bf16[128,512]{1,0:T(8,128)(2,1)S(1)}, u32[]{:S(2)}, u32[]{:S(2)}) %collective-permute-start.20) | collective-permute-done | bytes 131104 | tf_op jit(solution)/shard_map/ppermute | solution.py:44
  91.7 14.7 %all_to_all.10.refs_1_ = bf16[8,32,512]{2,1,0:T(8,128)(2,1)S(1)} all-to-all(bf16[8,32,512]{2,1,0:T(8,128)(2,1)S(1)} %bitcast.28), channel_id=1, replica_groups=mesh['sp'=8,'tp'=4] {'sp'}, dimensions={0} | all-to-all | bytes 524288 | tf_op jit(solution)/shard_map/all_to_all | solution.py:578
  106.5 0.9 shard_map.205
  (31 shorter events, 0.3 us)
Async XLA Ops:
  1.3 8.1 %collective-permute-start = (bf16[64,640]{1,0:T(8,128)(2,1)S(1)}, bf16[64,640]{1,0:T(8,128)(2,1)S(1)}, u32[]{:S(2)}, u32[]{:S(2)}) collective-permute-start(bf16[64,640]{1,0:T(8,128)(2,1)S(1)} %get-tuple-element.48.refs_1_.refs_5_), channel_id=1, source_target_pairs={{0,24},{4,28},{8,16},{12,20},{16,8},{20,12},{24,0},{28,4},{1,25},{... | collective-permute-start | bytes 245768 | tf_op jit(solution)/shard_map/ppermute | solution.py:44
  6.5 6.9 %collective-permute-start.1 = (bf16[64,640]{1,0:T(8,128)(2,1)S(1)}, bf16[64,640]{1,0:T(8,128)(2,1)S(1)}, u32[]{:S(2)}, u32[]{:S(2)}) collective-permute-start(bf16[64,640]{1,0:T(8,128)(2,1)S(1)} %get-tuple-element.48.refs_1_.refs_5_), channel_id=1, source_target_pairs={{0,16},{4,20},{8,24},{12,28},{16,0},{20,4},{24,8},{28,12},{1,17},{... | collective-permute-start | bytes 245768 | tf_op jit(solution)/shard_map/ppermute | solution.py:44
  6.5 8.4 %collective-permute-start.3 = (bf16[64,640]{1,0:T(8,128)(2,1)S(1)}, bf16[64,640]{1,0:T(8,128)(2,1)S(1)}, u32[]{:S(2)}, u32[]{:S(2)}) collective-permute-start(bf16[64,640]{1,0:T(8,128)(2,1)S(1)} %get-tuple-element.48.refs_1_.refs_5_), channel_id=1, source_target_pairs={{0,4},{4,0},{8,12},{12,8},{16,20},{20,16},{24,28},{28,24},{1,5},{5... | collective-permute-start | bytes 245768 | tf_op jit(solution)/shard_map/ppermute | solution.py:44
  13.3 6.0 %collective-permute-start.5 = (bf16[2,64,640]{2,1,0:T(8,128)(2,1)S(1)}, bf16[2,64,640]{2,1,0:T(8,128)(2,1)S(1)}, u32[]{:S(2)}, u32[]{:S(2)}) collective-permute-start(bf16[2,64,640]{2,1,0:T(8,128)(2,1)S(1)} %pad_maximum_fusion.3), channel_id=1, source_target_pairs={{0,4},{4,0},{8,12},{12,8},{16,20},{20,16},{24,28},{28,24},{1,5},{5... | collective-permute-start | bytes 491528 | tf_op jit(solution)/shard_map/ppermute | solution.py:44
  14.9 4.4 %collective-permute-start.4 = (bf16[64,640]{1,0:T(8,128)(2,1)S(1)}, bf16[64,640]{1,0:T(8,128)(2,1)S(1)}, u32[]{:S(2)}, u32[]{:S(2)}) collective-permute-start(bf16[64,640]{1,0:T(8,128)(2,1)S(1)} %collective-permute-done.3), channel_id=1, source_target_pairs={{0,8},{4,12},{8,0},{12,4},{16,24},{20,28},{24,16},{28,20},{1,9},{5... | collective-permute-start | bytes 245768 | tf_op jit(solution)/shard_map/ppermute | solution.py:44
  14.9 5.3 %collective-permute-start.2 = (bf16[64,640]{1,0:T(8,128)(2,1)S(1)}, bf16[64,640]{1,0:T(8,128)(2,1)S(1)}, u32[]{:S(2)}, u32[]{:S(2)}) collective-permute-start(bf16[64,640]{1,0:T(8,128)(2,1)S(1)} %get-tuple-element.48.refs_1_.refs_5_), channel_id=1, source_target_pairs={{0,8},{4,12},{8,0},{12,4},{16,24},{20,28},{24,16},{28,20},{1,9},{5... | collective-permute-start | bytes 245768 | tf_op jit(solution)/shard_map/ppermute | solution.py:44
  19.4 8.6 %collective-permute-start.7 = (bf16[4,64,640]{2,1,0:T(8,128)(2,1)S(1)}, bf16[4,64,640]{2,1,0:T(8,128)(2,1)S(1)}, u32[]{:S(2)}, u32[]{:S(2)}) collective-permute-start(bf16[4,64,640]{2,1,0:T(8,128)(2,1)S(1)} %pad_maximum_fusion.refs_3_.refs_8_), channel_id=1, source_target_pairs={{0,1},{1,0},{2,3},{3,2},{4,5},{5,4},{6,7},{7,6},{8,9},{9,8},{10,11... | collective-permute-start | bytes 983048 | tf_op jit(solution)/shard_map/ppermute | solution.py:44
  20.3 4.2 %collective-permute-start.6 = (bf16[3,64,640]{2,1,0:T(8,128)(2,1)S(1)}, bf16[3,64,640]{2,1,0:T(8,128)(2,1)S(1)}, u32[]{:S(2)}, u32[]{:S(2)}) collective-permute-start(bf16[3,64,640]{2,1,0:T(8,128)(2,1)S(1)} %pad_maximum_fusion.2.refs_2_.refs_6_), channel_id=1, source_target_pairs={{0,1},{1,0},{2,3},{3,2},{4,5},{5,4},{6,7},{7,6},{8,9},{9,8},{10,11... | collective-permute-start | bytes 737288 | tf_op jit(solution)/shard_map/ppermute | solution.py:44
  22.8 0.8 copy-start.10
  23.6 0.8 copy-start.11
  29.9 3.4 %copy-start.9 = (s32[128]{0:T(128)S(1)}, s32[128]{0:T(128)}, u32[]{:S(2)}) copy-start(s32[128]{0:T(128)} %param.33) | copy-start | bytes 1540
  29.9 1.7 %collective-permute-start.8 = (bf16[2,128,512]{2,1,0:T(8,128)(2,1)S(1)}, bf16[2,128,512]{2,1,0:T(8,128)(2,1)S(1)}, u32[]{:S(2)}, u32[]{:S(2)}) collective-permute-start(bf16[2,128,512]{2,1,0:T(8,128)(2,1)S(1)} %get-tuple-element.67), channel_id=1, source_target_pairs={{0,1},{1,0},{2,3},{3,2},{4,5},{5,4},{6,7},{7,6},{8,9},{9,8},{10,11... | collective-permute-start | bytes 786440 | tf_op jit(solution)/shard_map/ppermute | solution.py:44
  31.7 7.2 %collective-permute-start.9 = (bf16[128,512]{1,0:T(8,128)(2,1)S(1)}, bf16[128,512]{1,0:T(8,128)(2,1)S(1)}, u32[]{:S(2)}, u32[]{:S(2)}) collective-permute-start(bf16[128,512]{1,0:T(8,128)(2,1)S(1)} %get-tuple-element.69), channel_id=1, source_target_pairs={{0,2},{1,3},{2,0},{3,1},{4,6},{5,7},{6,4},{7,5},{8,10},{9,11},{10,... | collective-permute-start | bytes 393224 | tf_op jit(solution)/shard_map/ppermute | solution.py:44
  36.3 1.3 %copy-start = (bf16[4,2048,128]{2,1,0:T(8,128)(2,1)}, bf16[4,2048,128]{2,1,0:T(8,128)(2,1)S(1)}, u32[]{:S(2)}) copy-start(bf16[4,2048,128]{2,1,0:T(8,128)(2,1)S(1)} %get-tuple-element.75.refs_2_) | copy-start | bytes 6291460
  37.6 1.3 %copy-start.3 = (bf16[512,2048]{1,0:T(8,128)(2,1)}, bf16[512,2048]{1,0:T(8,128)(2,1)S(1)}, u32[]{:S(2)}) copy-start(bf16[512,2048]{1,0:T(8,128)(2,1)S(1)} %get-tuple-element.72.refs_0_) | copy-start | bytes 6291460
  39.9 0.6 copy-start.5
  40.6 0.7 copy-start.7
  41.2 13.1 %all-to-all-start = ((bf16[8,32,512]{2,1,0:T(8,128)(2,1)}), bf16[8,32,512]{2,1,0:T(8,128)(2,1)S(1)}, u32[]{:S(2)}, u32[]{:S(2)}) async-start(bf16[8,32,512]{2,1,0:T(8,128)(2,1)} %get-tuple-element.76), calls=%async_computation | async-start | bytes 524288 | tf_op jit(solution)/shard_map/all_to_all | solution.py:544
  45.2 36.6 %collective-permute-start.15 = (bf16[256,1024]{1,0:T(8,128)(2,1)}, bf16[256,1024]{1,0:T(8,128)(2,1)S(1)}, u32[]{:S(2)}, u32[]{:S(2)}) collective-permute-start(bf16[256,1024]{1,0:T(8,128)(2,1)} %copy-done.11), channel_id=1, source_target_pairs={{0,2},{1,3},{2,0},{3,1},{4,6},{5,7},{6,4},{7,5},{8,10},{9,11},{10,... | collective-permute-start | bytes 1572872 | tf_op jit(solution)/shard_map/ppermute | solution.py:44
  45.7 36.1 %collective-permute-start.16 = (bf16[256,1024]{1,0:T(8,128)(2,1)}, bf16[256,1024]{1,0:T(8,128)(2,1)S(1)}, u32[]{:S(2)}, u32[]{:S(2)}) collective-permute-start(bf16[256,1024]{1,0:T(8,128)(2,1)} %copy-done.10), channel_id=1, source_target_pairs={{0,2},{1,3},{2,0},{3,1},{4,6},{5,7},{6,4},{7,5},{8,10},{9,11},{10,... | collective-permute-start | bytes 1572872 | tf_op jit(solution)/shard_map/ppermute | solution.py:44
  54.4 21.5 %collective-permute-start.10 = (bf16[256,512]{1,0:T(8,128)(2,1)S(1)}, bf16[256,512]{1,0:T(8,128)(2,1)S(1)}, u32[]{:S(2)}, u32[]{:S(2)}) collective-permute-start(bf16[256,512]{1,0:T(8,128)(2,1)S(1)} %bitcast.19), channel_id=1, source_target_pairs={{0,1},{1,0},{2,3},{3,2},{4,5},{5,4},{6,7},{7,6},{8,9},{9,8},{10,11... | collective-permute-start | bytes 786440 | tf_op jit(solution)/shard_map/ppermute | solution.py:44
  54.4 19.9 %collective-permute-start.11 = (bf16[128,512]{1,0:T(8,128)(2,1)S(1)}, bf16[128,512]{1,0:T(8,128)(2,1)S(1)}, u32[]{:S(2)}, u32[]{:S(2)}) collective-permute-start(bf16[128,512]{1,0:T(8,128)(2,1)S(1)} %bitcast.34), channel_id=1, source_target_pairs={{0,2},{1,3},{2,0},{3,1},{4,6},{5,7},{6,4},{7,5},{8,10},{9,11},{10,... | collective-permute-start | bytes 393224 | tf_op jit(solution)/shard_map/ppermute | solution.py:44
  55.0 20.9 %collective-permute-start.13 = (bf16[128,512]{1,0:T(8,128)(2,1)S(1)}, bf16[128,512]{1,0:T(8,128)(2,1)S(1)}, u32[]{:S(2)}, u32[]{:S(2)}) collective-permute-start(bf16[128,512]{1,0:T(8,128)(2,1)S(1)} %bitcast.33), channel_id=1, source_target_pairs={{0,2},{1,3},{2,0},{3,1},{4,6},{5,7},{6,4},{7,5},{8,10},{9,11},{10,... | collective-permute-start | bytes 393224 | tf_op jit(solution)/shard_map/ppermute | solution.py:44
  74.2 4.0 %collective-permute-start.12 = (bf16[128,512]{1,0:T(8,128)(2,1)S(1)}, bf16[128,512]{1,0:T(8,128)(2,1)S(1)}, u32[]{:S(2)}, u32[]{:S(2)}) collective-permute-start(bf16[128,512]{1,0:T(8,128)(2,1)S(1)} %collective-permute-done.11.refs_6_), channel_id=1, source_target_pairs={{0,1},{1,0},{2,3},{3,2},{4,5},{5,4},{6,7},{7,6},{8,9},{9,8},{10,11... | collective-permute-start | bytes 393224 | tf_op jit(solution)/shard_map/ppermute | solution.py:44
  75.9 4.4 %collective-permute-start.14 = (bf16[128,512]{1,0:T(8,128)(2,1)S(1)}, bf16[128,512]{1,0:T(8,128)(2,1)S(1)}, u32[]{:S(2)}, u32[]{:S(2)}) collective-permute-start(bf16[128,512]{1,0:T(8,128)(2,1)S(1)} %collective-permute-done.13.refs_6_), channel_id=1, source_target_pairs={{0,1},{1,0},{2,3},{3,2},{4,5},{5,4},{6,7},{7,6},{8,9},{9,8},{10,11... | collective-permute-start | bytes 393224 | tf_op jit(solution)/shard_map/ppermute | solution.py:44
  75.9 1.6 %copy-start.1 = (bf16[4,2048,128]{2,1,0:T(8,128)(2,1)S(1)}, bf16[4,2048,128]{2,1,0:T(8,128)(2,1)}, u32[]{:S(2)}) copy-start(bf16[4,2048,128]{2,1,0:T(8,128)(2,1)} %copy-done) | copy-start | bytes 6291460
  77.5 1.6 %copy-start.2 = (bf16[4,2048,128]{2,1,0:T(8,128)(2,1)S(1)}, bf16[4,2048,128]{2,1,0:T(8,128)(2,1)}, u32[]{:S(2)}) copy-start(bf16[4,2048,128]{2,1,0:T(8,128)(2,1)} %copy-done) | copy-start | bytes 6291460
  79.7 1.6 %copy-start.4 = (bf16[512,2048]{1,0:T(8,128)(2,1)S(1)}, bf16[512,2048]{1,0:T(8,128)(2,1)}, u32[]{:S(2)}) copy-start(bf16[512,2048]{1,0:T(8,128)(2,1)} %copy-done.3) | copy-start | bytes 6291460
  79.7 4.6 %collective-permute-start.17 = (bf16[128,256]{1,0:T(8,128)(2,1)S(1)}, bf16[128,256]{1,0:T(8,128)(2,1)S(1)}, u32[]{:S(2)}, u32[]{:S(2)}) collective-permute-start(bf16[128,256]{1,0:T(8,128)(2,1)S(1)} %get-tuple-element.85), channel_id=1, source_target_pairs={{0,2},{1,3},{2,0},{3,1},{4,6},{5,7},{6,4},{7,5},{8,10},{9,11},{10,... | collective-permute-start | bytes 196616 | tf_op jit(solution)/shard_map/ppermute | solution.py:44
  85.0 21.5 %copy-start.6 = (bf16[256,128]{1,0:T(8,128)(2,1)S(1)}, bf16[256,128]{1,0:T(8,128)(2,1)}, u32[]{:S(2)}) copy-start(bf16[256,128]{1,0:T(8,128)(2,1)} %copy-done.5) | copy-start | bytes 196612
  85.0 21.5 %copy-start.8 = (bf16[128,512]{1,0:T(8,128)(2,1)S(1)}, bf16[128,512]{1,0:T(8,128)(2,1)}, u32[]{:S(2)}) copy-start(bf16[128,512]{1,0:T(8,128)(2,1)} %copy-done.7) | copy-start | bytes 393220
  85.0 5.3 %collective-permute-start.18 = (bf16[128,512]{1,0:T(8,128)(2,1)S(1)}, bf16[128,512]{1,0:T(8,128)(2,1)S(1)}, u32[]{:S(2)}, u32[]{:S(2)}) collective-permute-start(bf16[128,512]{1,0:T(8,128)(2,1)S(1)} %get-tuple-element.87), channel_id=1, source_target_pairs={{0,1},{1,0},{2,3},{3,2},{4,5},{5,4},{6,7},{7,6},{8,9},{9,8},{10,11... | collective-permute-start | bytes 393224 | tf_op jit(solution)/shard_map/ppermute | solution.py:44
  85.1 4.5 %collective-permute-start.19 = (bf16[128,256]{1,0:T(8,128)(2,1)S(1)}, bf16[128,256]{1,0:T(8,128)(2,1)S(1)}, u32[]{:S(2)}, u32[]{:S(2)}) collective-permute-start(bf16[128,256]{1,0:T(8,128)(2,1)S(1)} %get-tuple-element.88), channel_id=1, source_target_pairs={{0,2},{1,3},{2,0},{3,1},{4,6},{5,7},{6,4},{7,5},{8,10},{9,11},{10,... | collective-permute-start | bytes 196616 | tf_op jit(solution)/shard_map/ppermute | solution.py:44
  90.3 1.4 %collective-permute-start.20 = (bf16[128,512]{1,0:T(8,128)(2,1)S(1)}, bf16[128,512]{1,0:T(8,128)(2,1)S(1)}, u32[]{:S(2)}, u32[]{:S(2)}) collective-permute-start(bf16[128,512]{1,0:T(8,128)(2,1)S(1)} %get-tuple-element.90), channel_id=1, source_target_pairs={{0,1},{1,0},{2,3},{3,2},{4,5},{5,4},{6,7},{7,6},{8,9},{9,8},{10,11... | collective-permute-start | bytes 393224 | tf_op jit(solution)/shard_map/ppermute | solution.py:44

commit v3 on v2

--- a/solution.py
+++ b/solution.py
@@ -146,30 +146,30 @@
             offset = jnp.where(index == i, core if mine[start + i] else 1 - core, offset)
         key_pos = ((place ^ mask) * 2 + offset) * half + (lane & (half - 1))
         visible = iota((tokens, 1), 0) + place * tokens >= key_pos
-        new_state = []
+        scored = []
         for h in range(heads_w + heads_n):
             if h < heads_w:
                 keys = key_w[:, h * PLAIN_WIDTH_WIDE : (h + 1) * PLAIN_WIDTH_WIDE]
-                values = val_w[:, h * VALUE_WIDTH_WIDE : (h + 1) * VALUE_WIDTH_WIDE]
                 scale = (PLAIN_WIDTH_WIDE + ROPE) ** (-0.5)
             else:
                 keys = key_n
-                values = val_n
                 scale = (PLAIN_WIDTH_SLIM + ROPE) ** (-0.5)
             scores = dot_t(queries[h], jnp.concatenate([keys, rot], axis=1)) * scale
-            scores = jnp.where(visible, scores, MASKED)
-            peak = jnp.max(scores, axis=-1, keepdims=True)
-            if state is not None:
-                peak = jnp.maximum(peak, state[h][0])
-            weights = jnp.exp(scores - peak)
-            total = jnp.sum(weights, axis=-1, keepdims=True)
-            acc = dot(weights.astype(BF16), values)
-            if state is not None:
-                keep = jnp.exp(state[h][0] - peak)
-                total = total + state[h][1] * keep
-                acc = acc + state[h][2] * keep
-            new_state.append((peak, total, acc))
-        state = new_state
+            scored.append(jnp.where(visible, scores, MASKED))
+        peaks = [jnp.max(scores, axis=-1, keepdims=True) for scores in scored]
+        if state is not None:
+            peaks = [jnp.maximum(peak, state[h][0]) for h, peak in enumerate(peaks)]
+        weighed = [jnp.exp(scores - peak) for scores, peak in zip(scored, peaks)]
+        totals = [jnp.sum(weights, axis=-1, keepdims=True) for weights in weighed]
+        accs = []
+        for h, weights in enumerate(weighed):
+            values = val_w[:, h * VALUE_WIDTH_WIDE : (h + 1) * VALUE_WIDTH_WIDE] if h < heads_w else val_n
+            accs.append(dot(weights.astype(BF16), values))
+        if state is not None:
+            keeps = [jnp.exp(state[h][0] - peak) for h, peak in enumerate(peaks)]
+            totals = [total + state[h][1] * keeps[h] for h, total in enumerate(totals)]
+            accs = [acc + state[h][2] * keeps[h] for h, acc in enumerate(accs)]
+        state = list(zip(peaks, totals, accs))
     return state
 
 
@@ -181,9 +181,11 @@
         acc_ref[h] = acc
 
 
-def load_state(refs):
-    peak_ref, total_ref, acc_ref = refs
-    return [(peak_ref[h, :, :1], total_ref[h, :, :1], acc_ref[h]) for h in range(peak_ref.shape[0])]
+def merged(states):
+    peak = functools.reduce(jnp.maximum, [part[0] for part in states])
+    factors = [jnp.exp(part[0] - peak) for part in states]
+    total = sum(part[1] * factor for part, factor in zip(states, factors))
+    return sum(part[2] * factor for part, factor in zip(states, factors)) / total
 
 
 def first_kernel(masks, q_ref, *refs):
@@ -194,20 +196,23 @@
 
 
 def second_kernel(masks, q_ref, *refs):
-    lifts, state_refs, blocks = refs[:4], refs[4:7], refs[7:-3]
+    lifts, blocks = refs[:4], refs[4:-3]
     queries = [q_ref[h] for h in range(q_ref.shape[0])]
-    state = attend_body(queries, pieces_of(blocks), masks, [True] * len(masks), *lifts, load_state(state_refs))
+    state = attend_body(queries, pieces_of(blocks), masks, [True] * len(masks), *lifts, None)
     store_state(state, refs[-3:])
 
 
 def third_kernel(masks, q_ref, *refs):
-    lifts, state_refs, (ow_ref, on_ref), blocks = refs[:4], refs[4:7], refs[7:9], refs[9:-3]
+    lifts, state_refs, (ow_ref, on_ref), blocks = refs[:4], (refs[4:7], refs[7:10]), refs[10:12], refs[12:-3]
     send_ref, att_w_ref, att_n_ref = refs[-3:]
     queries = [q_ref[h] for h in range(q_ref.shape[0])]
     heads = len(queries)
     heads_w = lifts[0].shape[1] // PLAIN_WIDTH_WIDE
-    state = attend_body(queries, pieces_of(blocks), masks, [False] * len(masks), *lifts, load_state(state_refs))
-    done = [acc / total for _, total, acc in state]
+    state = attend_body(queries, pieces_of(blocks), masks, [False] * len(masks), *lifts, None)
+    done = []
+    for h, (peak, total, acc) in enumerate(state):
+        fresh = (jnp.broadcast_to(peak, acc.shape), jnp.broadcast_to(total, acc.shape), acc)
+        done.append(merged([fresh] + [tuple(ref[h] for ref in held) for held in state_refs]))
     att_w = jnp.concatenate(done[:heads_w], axis=1).astype(BF16)
     slim = done[heads_w]
     for h in range(1, heads - heads_w):
@@ -512,9 +517,7 @@
     down_high = [exchange(down_cuts[2 * i + 1], "tp", mask) for i, mask in enumerate(far_masks)]
     state_shape = [held_shape((heads, tokens, LANES), F32)] * 3
     state = call(functools.partial(first_kernel, first_masks), state_shape, [queries, *lifts, *column, *column_rest])
-    state = call(
-        functools.partial(second_kernel, second_masks), state_shape, [queries, *lifts, *state, across]
-    )
+    state += call(functools.partial(second_kernel, second_masks), state_shape, [queries, *lifts, across])
     pieces_shape = held_shape((tp_size // 2, tokens, quarter))
     send, att_w, att_n = call(
         functools.partial(third_kernel, second_masks),

time: 108 us -> 106 us (0.981)
  Pallas kernels: 18 us -> 15.8 us
    pallas_call x16, Pallas kernels: 18 us -> 15.8 us  [call(): pl.pallas_call(wrapped, out_shape=list(outs) + [held_shape(dims, a.dtype)...]
  transfers between devices with their start and end apart: 22 -> 22, of which waited for: 11 -> 11; matrix products, arithmetic and copies ran while one was open for 0% -> 0% of each run, Pallas kernels for 11% -> 10%
where the time goes in v3:
time: 106 us; the launch traced here: 105 us
  waiting for transfers between devices  43.7 us (41%)
  starting transfers between devices  21.8 us (21%)
  Pallas kernels  15.8 us (15%)
  blocking collectives  14.7 us (14%)
  local copies, waits for them, and re-layouts  8.42 us (8%)
    ppermute x21, waiting for transfers between devices, exchange(): return lax.ppermute(values, axis, [(i, i ^ mask) for i in range(size)])  36.6 us
    ppermute x21, starting transfers between devices, exchange(): return lax.ppermute(values, axis, [(i, i ^ mask) for i in range(size)])  17.9 us
    pallas_call x16, Pallas kernels, call(): pl.pallas_call(wrapped, out_shape=list(outs) + [held_shape(dims, a.dtype)...  15.8 us
    all_to_all x1, blocking collectives, body(): lax.all_to_all(jnp.concatenate(summed).reshape(groups, capacity, quarter)...  14.7 us
    unnamed x24, local copies, waits for them, and re-layouts  8.4 us
    all_to_all x1, waiting for transfers between devices, body(): lax.all_to_all(placed, 'sp', split_axis=0, concat_axis=0, tiled=True)  7.15 us
    all_to_all x1, starting transfers between devices, body(): lax.all_to_all(placed, 'sp', split_axis=0, concat_axis=0, tiled=True)  3.97 us
  transfers between devices with their start and end apart: 22, of which 11 were waited for; matrix products, arithmetic and copies ran while one was open for 0% of the time, Pallas kernels for 10%

profile of v3, /device:TPU:0, one launch (start us, length us, event | category | flops | bytes accessed | tf_op | source)
XLA Modules:
  0.0 105.1 jit_solution(8454369510898866930)
XLA Ops:
  0.0 0.1 multiply_sine_fusion
  0.2 1.1 %shard_map.190 = (bf16[64,640]{1,0:T(8,128)(2,1)S(1)}, bf16[64,640]{1,0:T(8,128)(2,1)S(1)}) custom-call(f32[32,128]{1,0:T(8,128)S(1)} %get-tuple-element.94.refs_0_, f32[32,128]{1,0:T(8,128)S(1)} %get-tuple-element.93.refs_1_, bf16[128,512]{1,0:T(8,128)(2,1)} %refs_2_.2, bf16[64,128]{1,0:T(8,128)(2,1)} %bitcast.38, f32[1,512]{1,0:T(1,128)} %bitcast.40, ...), custom_call_target="tpu_custom_call" | custom-call | tf_op jit(solution)/shard_map/pallas_call | solution.py:417
  1.3 5.1 %collective-permute-start = (bf16[64,640]{1,0:T(8,128)(2,1)S(1)}, bf16[64,640]{1,0:T(8,128)(2,1)S(1)}, u32[]{:S(2)}, u32[]{:S(2)}) collective-permute-start(bf16[64,640]{1,0:T(8,128)(2,1)S(1)} %get-tuple-element.48.refs_1_.refs_5_), channel_id=1, source_target_pairs={{0,24},{4,28},{8,16},{12,20},{16,8},{20,12},{24,0},{28,4},{1,25},{... | collective-permute-start | bytes 245768 | tf_op jit(solution)/shard_map/ppermute | solution.py:44
  6.5 1.5 %collective-permute-start.3 = (bf16[64,640]{1,0:T(8,128)(2,1)S(1)}, bf16[64,640]{1,0:T(8,128)(2,1)S(1)}, u32[]{:S(2)}, u32[]{:S(2)}) collective-permute-start(bf16[64,640]{1,0:T(8,128)(2,1)S(1)} %get-tuple-element.48.refs_1_.refs_5_), channel_id=1, source_target_pairs={{0,4},{4,0},{8,12},{12,8},{16,20},{20,16},{24,28},{28,24},{1,5},{5... | collective-permute-start | bytes 245768 | tf_op jit(solution)/shard_map/ppermute | solution.py:44
  8.0 1.5 %collective-permute-done = bf16[64,640]{1,0:T(8,128)(2,1)S(1)} collective-permute-done((bf16[64,640]{1,0:T(8,128)(2,1)S(1)}, bf16[64,640]{1,0:T(8,128)(2,1)S(1)}, u32[]{:S(2)}, u32[]{:S(2)}) %collective-permute-start) | collective-permute-done | bytes 81952 | tf_op jit(solution)/shard_map/ppermute | solution.py:44
  9.4 3.9 %collective-permute-done.1 = bf16[64,640]{1,0:T(8,128)(2,1)S(1)} collective-permute-done((bf16[64,640]{1,0:T(8,128)(2,1)S(1)}, bf16[64,640]{1,0:T(8,128)(2,1)S(1)}, u32[]{:S(2)}, u32[]{:S(2)}) %collective-permute-start.1) | collective-permute-done | bytes 81952 | tf_op jit(solution)/shard_map/ppermute | solution.py:44
  13.3 1.6 %collective-permute-start.5 = (bf16[2,64,640]{2,1,0:T(8,128)(2,1)S(1)}, bf16[2,64,640]{2,1,0:T(8,128)(2,1)S(1)}, u32[]{:S(2)}, u32[]{:S(2)}) collective-permute-start(bf16[2,64,640]{2,1,0:T(8,128)(2,1)S(1)} %pad_maximum_fusion.3), channel_id=1, source_target_pairs={{0,4},{4,0},{8,12},{12,8},{16,20},{20,16},{24,28},{28,24},{1,5},{5... | collective-permute-start | bytes 491528 | tf_op jit(solution)/shard_map/ppermute | solution.py:44
  14.9 0.0 collective-permute-done.3
  14.9 0.0 collective-permute-start.4
  14.9 2.0 %collective-permute-start.2 = (bf16[64,640]{1,0:T(8,128)(2,1)S(1)}, bf16[64,640]{1,0:T(8,128)(2,1)S(1)}, u32[]{:S(2)}, u32[]{:S(2)}) collective-permute-start(bf16[64,640]{1,0:T(8,128)(2,1)S(1)} %get-tuple-element.48.refs_1_.refs_5_), channel_id=1, source_target_pairs={{0,8},{4,12},{8,0},{12,4},{16,24},{20,28},{24,16},{28,20},{1,9},{5... | collective-permute-start | bytes 245768 | tf_op jit(solution)/shard_map/ppermute | solution.py:44
  16.9 2.4 %collective-permute-done.4 = bf16[64,640]{1,0:T(8,128)(2,1)S(1)} collective-permute-done((bf16[64,640]{1,0:T(8,128)(2,1)S(1)}, bf16[64,640]{1,0:T(8,128)(2,1)S(1)}, u32[]{:S(2)}, u32[]{:S(2)}) %collective-permute-start.4) | collective-permute-done | bytes 81952 | tf_op jit(solution)/shard_map/ppermute | solution.py:44
  19.3 0.0 collective-permute-done.5
  19.4 0.1 collective-permute-start.7
  19.5 0.7 collective-permute-done.2
  20.3 0.1 collective-permute-start.6
  20.3 2.4 %shard_map.192 = (bf16[4,128,256]{2,1,0:T(8,128)(2,1)S(1)}, bf16[512,256]{1,0:T(8,128)(2,1)S(1)}, bf16[512,256]{1,0:T(8,128)(2,1)S(1)}, bf16[512,128]{1,0:T(8,12...) custom-call(f32[32,128]{1,0:T(8,128)S(1)} %get-tuple-element.94.refs, ...), custom_call_target="tpu_custom_call" | custom-call | tf_op jit(solution)/shard_map/pallas_call | solution.py:417
  22.8 0.8 copy-done.10
  23.6 0.8 copy-done.11
  24.4 0.8 shard_map.194
  25.2 1.3 %shard_map.193 = (f32[4,128,128]{2,1,0:T(8,128)S(1)}, f32[4,128,128]{2,1,0:T(8,128)S(1)}, f32[4,128,128]{2,1,0:T(8,128)S(1)}) custom-call(bf16[4,128,256]{2,1,0:T(8,128)(2,1)S(1)} %get-tuple-element.52.refs_0_, bf16[512,256]{1,0:T(8,128)(2,1)S(1)} %get-tuple-element.53.refs_1_, bf16[512,256]{1,0:T(8,128)(2,1)S(1)} %get-tuple-element.54.refs_2_, ...), custom_call_target="tpu_custom_call" | custom-call | tf_op jit(solution)/shard_map/pallas_call | solution.py:417
  26.5 0.0 collective-permute-done.7.refs_6_.refs_13_
  26.5 1.2 %shard_map.195 = (bf16[2,128,512]{2,1,0:T(8,128)(2,1)S(1)}, bf16[128,256]{1,0:T(8,128)(2,1)S(1)}, bf16[128,128]{1,0:T(8,128)(2,1)S(1)}) custom-call(bf16[4,128,256]{2,1,0:T(8,128)(2,1)S(1)} %get-tuple-element.52.refs_0_, bf16[512,256]{1,0:T(8,128)(2,1)S(1)} %get-tuple-element.53.refs_1_, bf16[512,256]{1,0:T(8,128)(2,1)S(1)} %get-tuple-element.54.refs_2_, ...), custom_call_target="tpu_custom_call" | custom-call | tf_op jit(solution)/shard_map/pallas_call | solution.py:417
  27.7 0.0 copy-start.9
  27.7 0.5 collective-permute-start.8
  28.3 0.3 shard_map.196.refs_0_
  28.5 0.9 collective-permute-done.8.refs_1_
  29.4 0.1 shard_map.197
  29.5 1.6 %collective-permute-start.9 = (bf16[128,512]{1,0:T(8,128)(2,1)S(1)}, bf16[128,512]{1,0:T(8,128)(2,1)S(1)}, u32[]{:S(2)}, u32[]{:S(2)}) collective-permute-start(bf16[128,512]{1,0:T(8,128)(2,1)S(1)} %get-tuple-element.69), channel_id=1, source_target_pairs={{0,2},{1,3},{2,0},{3,1},{4,6},{5,7},{6,4},{7,5},{8,10},{9,11},{10,... | collective-permute-start | bytes 393224 | tf_op jit(solution)/shard_map/ppermute | solution.py:44
  31.1 3.0 %shard_map.191 = (f32[256,128]{1,0:T(8,128)S(1)}, bf16[256,128]{1,0:T(8,128)(2,1)S(1)}, bf16[4,2048,128]{2,1,0:T(8,128)(2,1)S(1)}, bf16[4,2048,128]{2,1,0:T(8,12...) custom-call(s32[1,128]{1,0:T(1,128)S(1)} %bitcast.22, ...), custom_call_target="tpu_custom_call" | custom-call | tf_op jit(solution)/shard_map/pallas_call | solution.py:417
  34.1 1.3 %copy-done = bf16[4,2048,128]{2,1,0:T(8,128)(2,1)} copy-done((bf16[4,2048,128]{2,1,0:T(8,128)(2,1)}, bf16[4,2048,128]{2,1,0:T(8,128)(2,1)S(1)}, u32[]{:S(2)}) %copy-start) | copy-done | bytes 2097176
  35.4 1.3 %copy-done.3 = bf16[512,2048]{1,0:T(8,128)(2,1)} copy-done((bf16[512,2048]{1,0:T(8,128)(2,1)}, bf16[512,2048]{1,0:T(8,128)(2,1)S(1)}, u32[]{:S(2)}) %copy-start.3) | copy-done | bytes 2097176
  36.7 0.0 collective-permute-done.9.refs_3_
  36.7 1.0 shard_map.198
  37.7 0.6 copy-done.5
  38.3 0.7 copy-done.7
  39.0 4.0 %all-to-all-start = ((bf16[8,32,512]{2,1,0:T(8,128)(2,1)}), bf16[8,32,512]{2,1,0:T(8,128)(2,1)S(1)}, u32[]{:S(2)}, u32[]{:S(2)}) async-start(bf16[8,32,512]{2,1,0:T(8,128)(2,1)} %get-tuple-element.76), calls=%async_computation | async-start | bytes 524288 | tf_op jit(solution)/shard_map/all_to_all | solution.py:547
  42.9 0.5 collective-permute-start.15
  43.4 1.5 %collective-permute-start.16 = (bf16[256,1024]{1,0:T(8,128)(2,1)}, bf16[256,1024]{1,0:T(8,128)(2,1)S(1)}, u32[]{:S(2)}, u32[]{:S(2)}) collective-permute-start(bf16[256,1024]{1,0:T(8,128)(2,1)} %copy-done.10), channel_id=1, source_target_pairs={{0,2},{1,3},{2,0},{3,1},{4,6},{5,7},{6,4},{7,5},{8,10},{9,11},{10,... | collective-permute-start | bytes 1572872 | tf_op jit(solution)/shard_map/ppermute | solution.py:44
  45.0 7.2 %all-to-all-done = bf16[8,32,512]{2,1,0:T(8,128)(2,1)S(1)} async-done(((bf16[8,32,512]{2,1,0:T(8,128)(2,1)}), bf16[8,32,512]{2,1,0:T(8,128)(2,1)S(1)}, u32[]{:S(2)}, u32[]{:S(2)}) %all-to-all-start) | async-done | bytes 262176 | tf_op jit(solution)/shard_map/all_to_all | solution.py:547
  52.1 0.6 collective-permute-start.11
  52.7 1.5 %collective-permute-start.13 = (bf16[128,512]{1,0:T(8,128)(2,1)S(1)}, bf16[128,512]{1,0:T(8,128)(2,1)S(1)}, u32[]{:S(2)}, u32[]{:S(2)}) collective-permute-start(bf16[128,512]{1,0:T(8,128)(2,1)S(1)} %bitcast.33), channel_id=1, source_target_pairs={{0,2},{1,3},{2,0},{3,1},{4,6},{5,7},{6,4},{7,5},{8,10},{9,11},{10,... | collective-permute-start | bytes 393224 | tf_op jit(solution)/shard_map/ppermute | solution.py:44
  54.2 17.8 %collective-permute-done.11.refs_6_ = bf16[128,512]{1,0:T(8,128)(2,1)S(1)} collective-permute-done((bf16[128,512]{1,0:T(8,128)(2,1)S(1)}, bf16[128,512]{1,0:T(8,128)(2,1)S(1)}, u32[]{:S(2)}, u32[]{:S(2)}) %collective-permute-start.11) | collective-permute-done | bytes 131104 | tf_op jit(solution)/shard_map/ppermute | solution.py:44
  72.0 0.0 collective-permute-start.12
  72.0 1.7 %collective-permute-done.13.refs_6_ = bf16[128,512]{1,0:T(8,128)(2,1)S(1)} collective-permute-done((bf16[128,512]{1,0:T(8,128)(2,1)S(1)}, bf16[128,512]{1,0:T(8,128)(2,1)S(1)}, u32[]{:S(2)}, u32[]{:S(2)}) %collective-permute-start.13) | collective-permute-done | bytes 131104 | tf_op jit(solution)/shard_map/ppermute | solution.py:44
  73.6 0.0 collective-permute-start.14
  73.7 1.6 %copy-done.1 = bf16[4,2048,128]{2,1,0:T(8,128)(2,1)S(1)} copy-done((bf16[4,2048,128]{2,1,0:T(8,128)(2,1)S(1)}, bf16[4,2048,128]{2,1,0:T(8,128)(2,1)}, u32[]{:S(2)}) %copy-start.1) | copy-done | bytes 2097176
  75.3 0.7 shard_map.199
  76.0 0.9 copy-done.2
  76.8 0.7 shard_map.200
  77.5 0.6 collective-permute-start.17
  78.1 0.6 shard_map.201
  78.7 0.4 copy-done.4
  79.1 0.4 shard_map.202
  79.5 2.5 %collective-permute-done.17.refs_5_ = bf16[128,256]{1,0:T(8,128)(2,1)S(1)} collective-permute-done((bf16[128,256]{1,0:T(8,128)(2,1)S(1)}, bf16[128,256]{1,0:T(8,128)(2,1)S(1)}, u32[]{:S(2)}, u32[]{:S(2)}) %collective-permute-start.17) | collective-permute-done | bytes 65568 | tf_op jit(solution)/shard_map/ppermute | solution.py:44
  82.1 0.7 shard_map.203
  82.8 0.0 copy-start.8
  82.8 0.1 collective-permute-start.18
  82.9 0.6 collective-permute-start.19
  83.4 3.9 %collective-permute-done.19.refs_5_ = bf16[128,256]{1,0:T(8,128)(2,1)S(1)} collective-permute-done((bf16[128,256]{1,0:T(8,128)(2,1)S(1)}, bf16[128,256]{1,0:T(8,128)(2,1)S(1)}, u32[]{:S(2)}, u32[]{:S(2)}) %collective-permute-start.19) | collective-permute-done | bytes 65568 | tf_op jit(solution)/shard_map/ppermute | solution.py:44
  87.3 0.7 shard_map.204
  88.0 0.1 collective-permute-start.20
  88.2 1.3 %collective-permute-done.20 = bf16[128,512]{1,0:T(8,128)(2,1)S(1)} collective-permute-done((bf16[128,512]{1,0:T(8,128)(2,1)S(1)}, bf16[128,512]{1,0:T(8,128)(2,1)S(1)}, u32[]{:S(2)}, u32[]{:S(2)}) %collective-permute-start.20) | collective-permute-done | bytes 131104 | tf_op jit(solution)/shard_map/ppermute | solution.py:44
  89.5 14.7 %all_to_all.10.refs_1_ = bf16[8,32,512]{2,1,0:T(8,128)(2,1)S(1)} all-to-all(bf16[8,32,512]{2,1,0:T(8,128)(2,1)S(1)} %bitcast.28), channel_id=1, replica_groups=mesh['sp'=8,'tp'=4] {'sp'}, dimensions={0} | all-to-all | bytes 524288 | tf_op jit(solution)/shard_map/all_to_all | solution.py:581
  104.3 0.9 shard_map.205
  (31 shorter events, 0.3 us)
Async XLA Ops:
  1.3 8.1 %collective-permute-start = (bf16[64,640]{1,0:T(8,128)(2,1)S(1)}, bf16[64,640]{1,0:T(8,128)(2,1)S(1)}, u32[]{:S(2)}, u32[]{:S(2)}) collective-permute-start(bf16[64,640]{1,0:T(8,128)(2,1)S(1)} %get-tuple-element.48.refs_1_.refs_5_), channel_id=1, source_target_pairs={{0,24},{4,28},{8,16},{12,20},{16,8},{20,12},{24,0},{28,4},{1,25},{... | collective-permute-start | bytes 245768 | tf_op jit(solution)/shard_map/ppermute | solution.py:44
  6.5 6.9 %collective-permute-start.1 = (bf16[64,640]{1,0:T(8,128)(2,1)S(1)}, bf16[64,640]{1,0:T(8,128)(2,1)S(1)}, u32[]{:S(2)}, u32[]{:S(2)}) collective-permute-start(bf16[64,640]{1,0:T(8,128)(2,1)S(1)} %get-tuple-element.48.refs_1_.refs_5_), channel_id=1, source_target_pairs={{0,16},{4,20},{8,24},{12,28},{16,0},{20,4},{24,8},{28,12},{1,17},{... | collective-permute-start | bytes 245768 | tf_op jit(solution)/shard_map/ppermute | solution.py:44
  6.5 8.4 %collective-permute-start.3 = (bf16[64,640]{1,0:T(8,128)(2,1)S(1)}, bf16[64,640]{1,0:T(8,128)(2,1)S(1)}, u32[]{:S(2)}, u32[]{:S(2)}) collective-permute-start(bf16[64,640]{1,0:T(8,128)(2,1)S(1)} %get-tuple-element.48.refs_1_.refs_5_), channel_id=1, source_target_pairs={{0,4},{4,0},{8,12},{12,8},{16,20},{20,16},{24,28},{28,24},{1,5},{5... | collective-permute-start | bytes 245768 | tf_op jit(solution)/shard_map/ppermute | solution.py:44
  13.3 6.0 %collective-permute-start.5 = (bf16[2,64,640]{2,1,0:T(8,128)(2,1)S(1)}, bf16[2,64,640]{2,1,0:T(8,128)(2,1)S(1)}, u32[]{:S(2)}, u32[]{:S(2)}) collective-permute-start(bf16[2,64,640]{2,1,0:T(8,128)(2,1)S(1)} %pad_maximum_fusion.3), channel_id=1, source_target_pairs={{0,4},{4,0},{8,12},{12,8},{16,20},{20,16},{24,28},{28,24},{1,5},{5... | collective-permute-start | bytes 491528 | tf_op jit(solution)/shard_map/ppermute | solution.py:44
  14.9 4.4 %collective-permute-start.4 = (bf16[64,640]{1,0:T(8,128)(2,1)S(1)}, bf16[64,640]{1,0:T(8,128)(2,1)S(1)}, u32[]{:S(2)}, u32[]{:S(2)}) collective-permute-start(bf16[64,640]{1,0:T(8,128)(2,1)S(1)} %collective-permute-done.3), channel_id=1, source_target_pairs={{0,8},{4,12},{8,0},{12,4},{16,24},{20,28},{24,16},{28,20},{1,9},{5... | collective-permute-start | bytes 245768 | tf_op jit(solution)/shard_map/ppermute | solution.py:44
  14.9 5.3 %collective-permute-start.2 = (bf16[64,640]{1,0:T(8,128)(2,1)S(1)}, bf16[64,640]{1,0:T(8,128)(2,1)S(1)}, u32[]{:S(2)}, u32[]{:S(2)}) collective-permute-start(bf16[64,640]{1,0:T(8,128)(2,1)S(1)} %get-tuple-element.48.refs_1_.refs_5_), channel_id=1, source_target_pairs={{0,8},{4,12},{8,0},{12,4},{16,24},{20,28},{24,16},{28,20},{1,9},{5... | collective-permute-start | bytes 245768 | tf_op jit(solution)/shard_map/ppermute | solution.py:44
  19.4 7.1 %collective-permute-start.7 = (bf16[4,64,640]{2,1,0:T(8,128)(2,1)S(1)}, bf16[4,64,640]{2,1,0:T(8,128)(2,1)S(1)}, u32[]{:S(2)}, u32[]{:S(2)}) collective-permute-start(bf16[4,64,640]{2,1,0:T(8,128)(2,1)S(1)} %pad_maximum_fusion.refs_3_.refs_5_), channel_id=1, source_target_pairs={{0,1},{1,0},{2,3},{3,2},{4,5},{5,4},{6,7},{7,6},{8,9},{9,8},{10,11... | collective-permute-start | bytes 983048 | tf_op jit(solution)/shard_map/ppermute | solution.py:44
  20.3 4.9 %collective-permute-start.6 = (bf16[3,64,640]{2,1,0:T(8,128)(2,1)S(1)}, bf16[3,64,640]{2,1,0:T(8,128)(2,1)S(1)}, u32[]{:S(2)}, u32[]{:S(2)}) collective-permute-start(bf16[3,64,640]{2,1,0:T(8,128)(2,1)S(1)} %pad_maximum_fusion.2.refs_2_.refs_6_), channel_id=1, source_target_pairs={{0,1},{1,0},{2,3},{3,2},{4,5},{5,4},{6,7},{7,6},{8,9},{9,8},{10,11... | collective-permute-start | bytes 737288 | tf_op jit(solution)/shard_map/ppermute | solution.py:44
  22.8 0.8 copy-start.10
  23.6 0.8 copy-start.11
  27.7 3.4 %copy-start.9 = (s32[128]{0:T(128)S(1)}, s32[128]{0:T(128)}, u32[]{:S(2)}) copy-start(s32[128]{0:T(128)} %param.33) | copy-start | bytes 1540
  27.7 1.7 %collective-permute-start.8 = (bf16[2,128,512]{2,1,0:T(8,128)(2,1)S(1)}, bf16[2,128,512]{2,1,0:T(8,128)(2,1)S(1)}, u32[]{:S(2)}, u32[]{:S(2)}) collective-permute-start(bf16[2,128,512]{2,1,0:T(8,128)(2,1)S(1)} %get-tuple-element.67), channel_id=1, source_target_pairs={{0,1},{1,0},{2,3},{3,2},{4,5},{5,4},{6,7},{7,6},{8,9},{9,8},{10,11... | collective-permute-start | bytes 786440 | tf_op jit(solution)/shard_map/ppermute | solution.py:44
  29.5 7.2 %collective-permute-start.9 = (bf16[128,512]{1,0:T(8,128)(2,1)S(1)}, bf16[128,512]{1,0:T(8,128)(2,1)S(1)}, u32[]{:S(2)}, u32[]{:S(2)}) collective-permute-start(bf16[128,512]{1,0:T(8,128)(2,1)S(1)} %get-tuple-element.69), channel_id=1, source_target_pairs={{0,2},{1,3},{2,0},{3,1},{4,6},{5,7},{6,4},{7,5},{8,10},{9,11},{10,... | collective-permute-start | bytes 393224 | tf_op jit(solution)/shard_map/ppermute | solution.py:44
  34.0 1.3 %copy-start = (bf16[4,2048,128]{2,1,0:T(8,128)(2,1)}, bf16[4,2048,128]{2,1,0:T(8,128)(2,1)S(1)}, u32[]{:S(2)}) copy-start(bf16[4,2048,128]{2,1,0:T(8,128)(2,1)S(1)} %get-tuple-element.75.refs_2_) | copy-start | bytes 6291460
  35.4 1.3 %copy-start.3 = (bf16[512,2048]{1,0:T(8,128)(2,1)}, bf16[512,2048]{1,0:T(8,128)(2,1)S(1)}, u32[]{:S(2)}) copy-start(bf16[512,2048]{1,0:T(8,128)(2,1)S(1)} %get-tuple-element.72.refs_0_) | copy-start | bytes 6291460
  37.7 0.6 copy-start.5
  38.3 0.7 copy-start.7
  39.0 13.2 %all-to-all-start = ((bf16[8,32,512]{2,1,0:T(8,128)(2,1)}), bf16[8,32,512]{2,1,0:T(8,128)(2,1)S(1)}, u32[]{:S(2)}, u32[]{:S(2)}) async-start(bf16[8,32,512]{2,1,0:T(8,128)(2,1)} %get-tuple-element.76), calls=%async_computation | async-start | bytes 524288 | tf_op jit(solution)/shard_map/all_to_all | solution.py:547
  42.9 36.6 %collective-permute-start.15 = (bf16[256,1024]{1,0:T(8,128)(2,1)}, bf16[256,1024]{1,0:T(8,128)(2,1)S(1)}, u32[]{:S(2)}, u32[]{:S(2)}) collective-permute-start(bf16[256,1024]{1,0:T(8,128)(2,1)} %copy-done.11), channel_id=1, source_target_pairs={{0,2},{1,3},{2,0},{3,1},{4,6},{5,7},{6,4},{7,5},{8,10},{9,11},{10,... | collective-permute-start | bytes 1572872 | tf_op jit(solution)/shard_map/ppermute | solution.py:44
  43.4 36.1 %collective-permute-start.16 = (bf16[256,1024]{1,0:T(8,128)(2,1)}, bf16[256,1024]{1,0:T(8,128)(2,1)S(1)}, u32[]{:S(2)}, u32[]{:S(2)}) collective-permute-start(bf16[256,1024]{1,0:T(8,128)(2,1)} %copy-done.10), channel_id=1, source_target_pairs={{0,2},{1,3},{2,0},{3,1},{4,6},{5,7},{6,4},{7,5},{8,10},{9,11},{10,... | collective-permute-start | bytes 1572872 | tf_op jit(solution)/shard_map/ppermute | solution.py:44
  52.1 21.5 %collective-permute-start.10 = (bf16[256,512]{1,0:T(8,128)(2,1)S(1)}, bf16[256,512]{1,0:T(8,128)(2,1)S(1)}, u32[]{:S(2)}, u32[]{:S(2)}) collective-permute-start(bf16[256,512]{1,0:T(8,128)(2,1)S(1)} %bitcast.19), channel_id=1, source_target_pairs={{0,1},{1,0},{2,3},{3,2},{4,5},{5,4},{6,7},{7,6},{8,9},{9,8},{10,11... | collective-permute-start | bytes 786440 | tf_op jit(solution)/shard_map/ppermute | solution.py:44
  52.1 19.8 %collective-permute-start.11 = (bf16[128,512]{1,0:T(8,128)(2,1)S(1)}, bf16[128,512]{1,0:T(8,128)(2,1)S(1)}, u32[]{:S(2)}, u32[]{:S(2)}) collective-permute-start(bf16[128,512]{1,0:T(8,128)(2,1)S(1)} %bitcast.34), channel_id=1, source_target_pairs={{0,2},{1,3},{2,0},{3,1},{4,6},{5,7},{6,4},{7,5},{8,10},{9,11},{10,... | collective-permute-start | bytes 393224 | tf_op jit(solution)/shard_map/ppermute | solution.py:44
  52.7 20.9 %collective-permute-start.13 = (bf16[128,512]{1,0:T(8,128)(2,1)S(1)}, bf16[128,512]{1,0:T(8,128)(2,1)S(1)}, u32[]{:S(2)}, u32[]{:S(2)}) collective-permute-start(bf16[128,512]{1,0:T(8,128)(2,1)S(1)} %bitcast.33), channel_id=1, source_target_pairs={{0,2},{1,3},{2,0},{3,1},{4,6},{5,7},{6,4},{7,5},{8,10},{9,11},{10,... | collective-permute-start | bytes 393224 | tf_op jit(solution)/shard_map/ppermute | solution.py:44
  72.0 4.0 %collective-permute-start.12 = (bf16[128,512]{1,0:T(8,128)(2,1)S(1)}, bf16[128,512]{1,0:T(8,128)(2,1)S(1)}, u32[]{:S(2)}, u32[]{:S(2)}) collective-permute-start(bf16[128,512]{1,0:T(8,128)(2,1)S(1)} %collective-permute-done.11.refs_6_), channel_id=1, source_target_pairs={{0,1},{1,0},{2,3},{3,2},{4,5},{5,4},{6,7},{7,6},{8,9},{9,8},{10,11... | collective-permute-start | bytes 393224 | tf_op jit(solution)/shard_map/ppermute | solution.py:44
  73.6 4.4 %collective-permute-start.14 = (bf16[128,512]{1,0:T(8,128)(2,1)S(1)}, bf16[128,512]{1,0:T(8,128)(2,1)S(1)}, u32[]{:S(2)}, u32[]{:S(2)}) collective-permute-start(bf16[128,512]{1,0:T(8,128)(2,1)S(1)} %collective-permute-done.13.refs_6_), channel_id=1, source_target_pairs={{0,1},{1,0},{2,3},{3,2},{4,5},{5,4},{6,7},{7,6},{8,9},{9,8},{10,11... | collective-permute-start | bytes 393224 | tf_op jit(solution)/shard_map/ppermute | solution.py:44
  73.7 1.6 %copy-start.1 = (bf16[4,2048,128]{2,1,0:T(8,128)(2,1)S(1)}, bf16[4,2048,128]{2,1,0:T(8,128)(2,1)}, u32[]{:S(2)}) copy-start(bf16[4,2048,128]{2,1,0:T(8,128)(2,1)} %copy-done) | copy-start | bytes 6291460
  75.2 1.6 %copy-start.2 = (bf16[4,2048,128]{2,1,0:T(8,128)(2,1)S(1)}, bf16[4,2048,128]{2,1,0:T(8,128)(2,1)}, u32[]{:S(2)}) copy-start(bf16[4,2048,128]{2,1,0:T(8,128)(2,1)} %copy-done) | copy-start | bytes 6291460
  77.5 1.6 %copy-start.4 = (bf16[512,2048]{1,0:T(8,128)(2,1)S(1)}, bf16[512,2048]{1,0:T(8,128)(2,1)}, u32[]{:S(2)}) copy-start(bf16[512,2048]{1,0:T(8,128)(2,1)} %copy-done.3) | copy-start | bytes 6291460
  77.5 4.6 %collective-permute-start.17 = (bf16[128,256]{1,0:T(8,128)(2,1)S(1)}, bf16[128,256]{1,0:T(8,128)(2,1)S(1)}, u32[]{:S(2)}, u32[]{:S(2)}) collective-permute-start(bf16[128,256]{1,0:T(8,128)(2,1)S(1)} %get-tuple-element.85), channel_id=1, source_target_pairs={{0,2},{1,3},{2,0},{3,1},{4,6},{5,7},{6,4},{7,5},{8,10},{9,11},{10,... | collective-permute-start | bytes 196616 | tf_op jit(solution)/shard_map/ppermute | solution.py:44
  82.8 21.5 %copy-start.6 = (bf16[256,128]{1,0:T(8,128)(2,1)S(1)}, bf16[256,128]{1,0:T(8,128)(2,1)}, u32[]{:S(2)}) copy-start(bf16[256,128]{1,0:T(8,128)(2,1)} %copy-done.5) | copy-start | bytes 196612
  82.8 21.5 %copy-start.8 = (bf16[128,512]{1,0:T(8,128)(2,1)S(1)}, bf16[128,512]{1,0:T(8,128)(2,1)}, u32[]{:S(2)}) copy-start(bf16[128,512]{1,0:T(8,128)(2,1)} %copy-done.7) | copy-start | bytes 393220
  82.8 5.3 %collective-permute-start.18 = (bf16[128,512]{1,0:T(8,128)(2,1)S(1)}, bf16[128,512]{1,0:T(8,128)(2,1)S(1)}, u32[]{:S(2)}, u32[]{:S(2)}) collective-permute-start(bf16[128,512]{1,0:T(8,128)(2,1)S(1)} %get-tuple-element.87), channel_id=1, source_target_pairs={{0,1},{1,0},{2,3},{3,2},{4,5},{5,4},{6,7},{7,6},{8,9},{9,8},{10,11... | collective-permute-start | bytes 393224 | tf_op jit(solution)/shard_map/ppermute | solution.py:44
  82.9 4.5 %collective-permute-start.19 = (bf16[128,256]{1,0:T(8,128)(2,1)S(1)}, bf16[128,256]{1,0:T(8,128)(2,1)S(1)}, u32[]{:S(2)}, u32[]{:S(2)}) collective-permute-start(bf16[128,256]{1,0:T(8,128)(2,1)S(1)} %get-tuple-element.88), channel_id=1, source_target_pairs={{0,2},{1,3},{2,0},{3,1},{4,6},{5,7},{6,4},{7,5},{8,10},{9,11},{10,... | collective-permute-start | bytes 196616 | tf_op jit(solution)/shard_map/ppermute | solution.py:44
  88.0 1.4 %collective-permute-start.20 = (bf16[128,512]{1,0:T(8,128)(2,1)S(1)}, bf16[128,512]{1,0:T(8,128)(2,1)S(1)}, u32[]{:S(2)}, u32[]{:S(2)}) collective-permute-start(bf16[128,512]{1,0:T(8,128)(2,1)S(1)} %get-tuple-element.90), channel_id=1, source_target_pairs={{0,1},{1,0},{2,3},{3,2},{4,5},{5,4},{6,7},{7,6},{8,9},{9,8},{10,11... | collective-permute-start | bytes 393224 | tf_op jit(solution)/shard_map/ppermute | solution.py:44

commit v4 on v3

--- a/solution.py
+++ b/solution.py
@@ -251,7 +251,7 @@
     half, width = mine_all[0].shape
     place = lax.axis_index("sp")
     odd = (lax.axis_index("tp") & 1) == 1
-    capacity = out_ref.shape[0] // len(mine_all)
+    capacity = out_ref.shape[1] // len(mine_all)
     base = width - LANES
     hot_ref[...] = slots_of(route_ref[...], len(mine_all), capacity)
     for mask, mine, other in zip(masks, mine_all, other_all):
@@ -264,7 +264,10 @@
         order = prefix_count(here) - 1.0
         hot = jnp.where((iota((capacity, 2 * half), 0).astype(F32) == order) & (here > 0), 1.0, 0.0)
         start = pl.multiple_of((place ^ mask) * capacity, capacity)
-        out_ref[pl.ds(start, capacity), :] = dot(hot.astype(BF16), data)
+        weights = dot(hot.astype(BF16), data)
+        for e in range(out_ref.shape[0]):
+            column = weights[:, ROPE + e : ROPE + e + 1]
+            out_ref[e, pl.ds(start, capacity), :] = jnp.broadcast_to(column, (capacity, out_ref.shape[2]))
 
 
 def pair_kernel(masks, keep_ref, got_ref, stay_ref, *send_refs):
@@ -318,7 +321,7 @@
     firsts, seconds = [], []
     seen = 0.0
     for e in range(experts):
-        chosen = jnp.where(weight_ref[span, ROPE + e : ROPE + e + 1] != 0.0, 1.0, 0.0)
+        chosen = jnp.where(weight_ref[e, span, :] != 0.0, 1.0, 0.0)
         firsts.append((chosen > 0.0) & (seen == 0.0))
         seconds.append((chosen > 0.0) & (seen == 1.0))
         seen = seen + chosen
@@ -331,14 +334,14 @@
     rows = hidden_ref.shape[0]
     span = slice(first, first + rows)
     acts = [act_ref[e, span, :] for e in range(experts)]
-    square = expand_part(masks, gain_ref, gate_ref, up_ref, refs[:-2], acts, square_ref[span, :1])
+    square = expand_part(masks, gain_ref, gate_ref, up_ref, refs[:-2], acts, 0.0)
+    square = square_ref[span, :] + jnp.broadcast_to(square, (rows, hidden_width))
     scale = lax.rsqrt(square / model_width + EPSILON)
     firsts, seconds = places_of(weight_ref, span, experts)
     pair = [jnp.zeros((rows, hidden_width), F32)] * 2
     for e in range(experts):
         gate, up = acts[e][:, :hidden_width] * scale, acts[e][:, hidden_width:] * scale
-        weight = weight_ref[span, ROPE + e : ROPE + e + 1]
-        hidden = gate / (1.0 + jnp.exp(-gate)) * up * weight
+        hidden = gate / (1.0 + jnp.exp(-gate)) * up * weight_ref[e, span, :]
         hidden_ref[:, e * hidden_width : (e + 1) * hidden_width] = hidden.astype(BF16)
         pair = [jnp.where(firsts[e], hidden, pair[0]), jnp.where(seconds[e], hidden, pair[1])]
     pair_ref[...] = jnp.concatenate(pair, axis=1).astype(BF16)
@@ -468,6 +471,7 @@
     quarter = model_width // tp_size
     route = group_route[None, :]
     far_masks = list(range(2, tp_size, 2))
+    experts, _, hidden_width = gate_weight[0].shape
     down_rows = down_weight[0].reshape(-1, model_width)
 
     def resid_cut(ref):
@@ -527,7 +531,7 @@
     (keep,) = call(keep_kernel, [pieces_shape], [att_w, att_n, *out_weights], mib=4)
     slot_weights, hot, gate, up, down, gain, resid_cols = call(
         functools.partial(weights_kernel, first_masks + second_masks),
-        [held_shape((slots, LANES), F32), held_shape((slots, tokens))],
+        [held_shape((experts, slots, hidden_width), F32), held_shape((slots, tokens))],
         [route, *column, across, *column_rest, across_rest], [],
         [gate_weight[0], up_weight[0], down_rows, ffn_gain[None, :]],
         [(resid, resid_cut, (tokens, quarter))], mib=4,
@@ -551,10 +555,9 @@
     for first in (0, part_rows):
         far.append([exchange(routed[first : first + part_rows], "tp", mask) for mask in far_masks])
     near = exchange(routed, "tp", 1)
-    experts, _, hidden_width = gate_weight[0].shape
     acts, square = call(
         functools.partial(near_kernel, [0, 1]),
-        [held_shape((experts, slots, 2 * hidden_width), F32), held_shape((slots, LANES), F32)],
+        [held_shape((experts, slots, 2 * hidden_width), F32), held_shape((slots, hidden_width), F32)],
         [gain, gate, up, routed, near],
     )
     hidden, pairs = [], []

time: 106 us -> 106 us (level)
  Pallas kernels: 15.8 us -> 16.9 us
    pallas_call x16, Pallas kernels: 15.8 us -> 16.9 us  [call(): pl.pallas_call(wrapped, out_shape=list(outs) + [held_shape(dims, a.dtype)...]
    unnamed x24 -> x20, local copies, waits for them, and re-layouts: 8.4 us -> 7.88 us
  transfers between devices with their start and end apart: 22 -> 22, of which waited for: 11 -> 11; matrix products, arithmetic and copies ran while one was open for 0% -> 0% of each run, Pallas kernels for 10% -> 11%
where the time goes in v4:
time: 106 us
  waiting for transfers between devices  43.7 us (41%)
  starting transfers between devices  21.8 us (21%)
  Pallas kernels  16.9 us (16%)
  blocking collectives  14.7 us (14%)
  local copies, waits for them, and re-layouts  7.9 us (7%)
    ppermute x21, waiting for transfers between devices, exchange(): return lax.ppermute(values, axis, [(i, i ^ mask) for i in range(size)])  36.6 us
    ppermute x21, starting transfers between devices, exchange(): return lax.ppermute(values, axis, [(i, i ^ mask) for i in range(size)])  17.9 us
    pallas_call x16, Pallas kernels, call(): pl.pallas_call(wrapped, out_shape=list(outs) + [held_shape(dims, a.dtype)...  16.9 us
    all_to_all x1, blocking collectives, body(): lax.all_to_all(jnp.concatenate(summed).reshape(groups, capacity, quarter)...  14.7 us
    unnamed x20, local copies, waits for them, and re-layouts  7.88 us
    all_to_all x1, waiting for transfers between devices, body(): lax.all_to_all(placed, 'sp', split_axis=0, concat_axis=0, tiled=True)  7.15 us
    all_to_all x1, starting transfers between devices, body(): lax.all_to_all(placed, 'sp', split_axis=0, concat_axis=0, tiled=True)  3.96 us
  transfers between devices with their start and end apart: 22, of which 11 were waited for; matrix products, arithmetic and copies ran while one was open for 0% of the time, Pallas kernels for 11%

profile of v4, /device:TPU:0, one launch (start us, length us, event | category | flops | bytes accessed | tf_op | source)
XLA Modules:
  0.0 105.8 jit_solution(15246474244923487725)
XLA Ops:
  0.0 0.1 multiply_sine_fusion
  0.2 1.1 %shard_map.190 = (bf16[64,640]{1,0:T(8,128)(2,1)S(1)}, bf16[64,640]{1,0:T(8,128)(2,1)S(1)}) custom-call(f32[32,128]{1,0:T(8,128)S(1)} %get-tuple-element.94.refs_0_, f32[32,128]{1,0:T(8,128)S(1)} %get-tuple-element.93.refs_1_, bf16[128,512]{1,0:T(8,128)(2,1)} %refs_2_.2, bf16[64,128]{1,0:T(8,128)(2,1)} %bitcast.38, f32[1,512]{1,0:T(1,128)} %bitcast.40, ...), custom_call_target="tpu_custom_call" | custom-call | tf_op jit(solution)/shard_map/pallas_call | solution.py:420
  1.3 5.1 %collective-permute-start = (bf16[64,640]{1,0:T(8,128)(2,1)S(1)}, bf16[64,640]{1,0:T(8,128)(2,1)S(1)}, u32[]{:S(2)}, u32[]{:S(2)}) collective-permute-start(bf16[64,640]{1,0:T(8,128)(2,1)S(1)} %get-tuple-element.48.refs_1_.refs_5_), channel_id=1, source_target_pairs={{0,24},{4,28},{8,16},{12,20},{16,8},{20,12},{24,0},{28,4},{1,25},{... | collective-permute-start | bytes 245768 | tf_op jit(solution)/shard_map/ppermute | solution.py:44
  6.5 1.5 %collective-permute-start.3 = (bf16[64,640]{1,0:T(8,128)(2,1)S(1)}, bf16[64,640]{1,0:T(8,128)(2,1)S(1)}, u32[]{:S(2)}, u32[]{:S(2)}) collective-permute-start(bf16[64,640]{1,0:T(8,128)(2,1)S(1)} %get-tuple-element.48.refs_1_.refs_5_), channel_id=1, source_target_pairs={{0,4},{4,0},{8,12},{12,8},{16,20},{20,16},{24,28},{28,24},{1,5},{5... | collective-permute-start | bytes 245768 | tf_op jit(solution)/shard_map/ppermute | solution.py:44
  8.0 1.5 %collective-permute-done = bf16[64,640]{1,0:T(8,128)(2,1)S(1)} collective-permute-done((bf16[64,640]{1,0:T(8,128)(2,1)S(1)}, bf16[64,640]{1,0:T(8,128)(2,1)S(1)}, u32[]{:S(2)}, u32[]{:S(2)}) %collective-permute-start) | collective-permute-done | bytes 81952 | tf_op jit(solution)/shard_map/ppermute | solution.py:44
  9.4 3.9 %collective-permute-done.1 = bf16[64,640]{1,0:T(8,128)(2,1)S(1)} collective-permute-done((bf16[64,640]{1,0:T(8,128)(2,1)S(1)}, bf16[64,640]{1,0:T(8,128)(2,1)S(1)}, u32[]{:S(2)}, u32[]{:S(2)}) %collective-permute-start.1) | collective-permute-done | bytes 81952 | tf_op jit(solution)/shard_map/ppermute | solution.py:44
  13.3 1.6 %collective-permute-start.5 = (bf16[2,64,640]{2,1,0:T(8,128)(2,1)S(1)}, bf16[2,64,640]{2,1,0:T(8,128)(2,1)S(1)}, u32[]{:S(2)}, u32[]{:S(2)}) collective-permute-start(bf16[2,64,640]{2,1,0:T(8,128)(2,1)S(1)} %pad_maximum_fusion.3), channel_id=1, source_target_pairs={{0,4},{4,0},{8,12},{12,8},{16,20},{20,16},{24,28},{28,24},{1,5},{5... | collective-permute-start | bytes 491528 | tf_op jit(solution)/shard_map/ppermute | solution.py:44
  14.9 0.0 collective-permute-done.3
  14.9 0.0 collective-permute-start.4
  14.9 2.0 %collective-permute-start.2 = (bf16[64,640]{1,0:T(8,128)(2,1)S(1)}, bf16[64,640]{1,0:T(8,128)(2,1)S(1)}, u32[]{:S(2)}, u32[]{:S(2)}) collective-permute-start(bf16[64,640]{1,0:T(8,128)(2,1)S(1)} %get-tuple-element.48.refs_1_.refs_5_), channel_id=1, source_target_pairs={{0,8},{4,12},{8,0},{12,4},{16,24},{20,28},{24,16},{28,20},{1,9},{5... | collective-permute-start | bytes 245768 | tf_op jit(solution)/shard_map/ppermute | solution.py:44
  16.9 2.4 %collective-permute-done.4 = bf16[64,640]{1,0:T(8,128)(2,1)S(1)} collective-permute-done((bf16[64,640]{1,0:T(8,128)(2,1)S(1)}, bf16[64,640]{1,0:T(8,128)(2,1)S(1)}, u32[]{:S(2)}, u32[]{:S(2)}) %collective-permute-start.4) | collective-permute-done | bytes 81952 | tf_op jit(solution)/shard_map/ppermute | solution.py:44
  19.3 0.0 collective-permute-done.5
  19.4 0.1 collective-permute-start.7
  19.5 0.7 collective-permute-done.2
  20.3 0.1 collective-permute-start.6
  20.3 2.4 %shard_map.192 = (bf16[4,128,256]{2,1,0:T(8,128)(2,1)S(1)}, bf16[512,256]{1,0:T(8,128)(2,1)S(1)}, bf16[512,256]{1,0:T(8,128)(2,1)S(1)}, bf16[512,128]{1,0:T(8,12...) custom-call(f32[32,128]{1,0:T(8,128)S(1)} %get-tuple-element.94.refs, ...), custom_call_target="tpu_custom_call" | custom-call | tf_op jit(solution)/shard_map/pallas_call | solution.py:420
  22.8 0.8 copy-done.8
  23.6 0.8 copy-done.9
  24.4 0.8 shard_map.194
  25.2 0.0 collective-permute-done.6.refs_5_.refs_8_
  25.2 1.3 %shard_map.193 = (f32[4,128,128]{2,1,0:T(8,128)S(1)}, f32[4,128,128]{2,1,0:T(8,128)S(1)}, f32[4,128,128]{2,1,0:T(8,128)S(1)}) custom-call(bf16[4,128,256]{2,1,0:T(8,128)(2,1)S(1)} %get-tuple-element.52.refs_0_, bf16[512,256]{1,0:T(8,128)(2,1)S(1)} %get-tuple-element.53.refs_1_, bf16[512,256]{1,0:T(8,128)(2,1)S(1)} %get-tuple-element.54.refs_2_, ...), custom_call_target="tpu_custom_call" | custom-call | tf_op jit(solution)/shard_map/pallas_call | solution.py:420
  26.5 1.2 %shard_map.195 = (bf16[2,128,512]{2,1,0:T(8,128)(2,1)S(1)}, bf16[128,256]{1,0:T(8,128)(2,1)S(1)}, bf16[128,128]{1,0:T(8,128)(2,1)S(1)}) custom-call(bf16[4,128,256]{2,1,0:T(8,128)(2,1)S(1)} %get-tuple-element.52.refs_0_, bf16[512,256]{1,0:T(8,128)(2,1)S(1)} %get-tuple-element.53.refs_1_, bf16[512,256]{1,0:T(8,128)(2,1)S(1)} %get-tuple-element.54.refs_2_, ...), custom_call_target="tpu_custom_call" | custom-call | tf_op jit(solution)/shard_map/pallas_call | solution.py:420
  27.7 0.0 copy-start.7
  27.7 0.5 collective-permute-start.8
  28.2 0.3 shard_map.196.refs_0_
  28.5 0.9 collective-permute-done.8.refs_1_
  29.4 0.1 shard_map.197
  29.5 1.6 %collective-permute-start.9 = (bf16[128,512]{1,0:T(8,128)(2,1)S(1)}, bf16[128,512]{1,0:T(8,128)(2,1)S(1)}, u32[]{:S(2)}, u32[]{:S(2)}) collective-permute-start(bf16[128,512]{1,0:T(8,128)(2,1)S(1)} %get-tuple-element.69), channel_id=1, source_target_pairs={{0,2},{1,3},{2,0},{3,1},{4,6},{5,7},{6,4},{7,5},{8,10},{9,11},{10,... | collective-permute-start | bytes 393224 | tf_op jit(solution)/shard_map/ppermute | solution.py:44
  31.0 3.0 %shard_map.191 = (f32[4,256,128]{2,1,0:T(8,128)S(1)}, bf16[256,128]{1,0:T(8,128)(2,1)S(1)}, bf16[4,2048,128]{2,1,0:T(8,128)(2,1)S(1)}, bf16[4,2048,128]{2,1,0:T(...) custom-call(s32[1,128]{1,0:T(1,128)S(1)} %bitcast.22, ...), custom_call_target="tpu_custom_call" | custom-call | tf_op jit(solution)/shard_map/pallas_call | solution.py:420
  34.0 1.3 %copy-done = bf16[4,2048,128]{2,1,0:T(8,128)(2,1)} copy-done((bf16[4,2048,128]{2,1,0:T(8,128)(2,1)}, bf16[4,2048,128]{2,1,0:T(8,128)(2,1)S(1)}, u32[]{:S(2)}) %copy-start) | copy-done | bytes 2097176
  35.4 1.3 %copy-done.3 = bf16[512,2048]{1,0:T(8,128)(2,1)} copy-done((bf16[512,2048]{1,0:T(8,128)(2,1)}, bf16[512,2048]{1,0:T(8,128)(2,1)S(1)}, u32[]{:S(2)}) %copy-start.3) | copy-done | bytes 2097176
  36.7 0.0 collective-permute-done.9.refs_3_
  36.7 1.0 shard_map.198
  37.7 0.7 copy-done.5
  38.3 4.0 %all-to-all-start = ((bf16[8,32,512]{2,1,0:T(8,128)(2,1)}), bf16[8,32,512]{2,1,0:T(8,128)(2,1)S(1)}, u32[]{:S(2)}, u32[]{:S(2)}) async-start(bf16[8,32,512]{2,1,0:T(8,128)(2,1)} %get-tuple-element.76), calls=%async_computation | async-start | bytes 524288 | tf_op jit(solution)/shard_map/all_to_all | solution.py:551
  42.3 0.5 collective-permute-start.15
  42.8 1.5 %collective-permute-start.16 = (bf16[256,1024]{1,0:T(8,128)(2,1)}, bf16[256,1024]{1,0:T(8,128)(2,1)}, u32[]{:S(2)}, u32[]{:S(2)}) collective-permute-start(bf16[256,1024]{1,0:T(8,128)(2,1)} %copy-done.8), channel_id=1, source_target_pairs={{0,2},{1,3},{2,0},{3,1},{4,6},{5,7},{6,4},{7,5},{8,10},{9,11},{10,... | collective-permute-start | bytes 1572872 | tf_op jit(solution)/shard_map/ppermute | solution.py:44
  44.3 7.2 %all-to-all-done = bf16[8,32,512]{2,1,0:T(8,128)(2,1)S(1)} async-done(((bf16[8,32,512]{2,1,0:T(8,128)(2,1)}), bf16[8,32,512]{2,1,0:T(8,128)(2,1)S(1)}, u32[]{:S(2)}, u32[]{:S(2)}) %all-to-all-start) | async-done | bytes 262176 | tf_op jit(solution)/shard_map/all_to_all | solution.py:551
  51.5 0.0 collective-permute-start.10
  51.5 0.6 collective-permute-start.11
  52.1 1.5 %collective-permute-start.13 = (bf16[128,512]{1,0:T(8,128)(2,1)S(1)}, bf16[128,512]{1,0:T(8,128)(2,1)S(1)}, u32[]{:S(2)}, u32[]{:S(2)}) collective-permute-start(bf16[128,512]{1,0:T(8,128)(2,1)S(1)} %bitcast.33), channel_id=1, source_target_pairs={{0,2},{1,3},{2,0},{3,1},{4,6},{5,7},{6,4},{7,5},{8,10},{9,11},{10,... | collective-permute-start | bytes 393224 | tf_op jit(solution)/shard_map/ppermute | solution.py:44
  53.6 17.8 %collective-permute-done.11.refs_6_ = bf16[128,512]{1,0:T(8,128)(2,1)S(1)} collective-permute-done((bf16[128,512]{1,0:T(8,128)(2,1)S(1)}, bf16[128,512]{1,0:T(8,128)(2,1)S(1)}, u32[]{:S(2)}, u32[]{:S(2)}) %collective-permute-start.11) | collective-permute-done | bytes 131104 | tf_op jit(solution)/shard_map/ppermute | solution.py:44
  71.3 1.7 %collective-permute-done.13.refs_6_ = bf16[128,512]{1,0:T(8,128)(2,1)S(1)} collective-permute-done((bf16[128,512]{1,0:T(8,128)(2,1)S(1)}, bf16[128,512]{1,0:T(8,128)(2,1)S(1)}, u32[]{:S(2)}, u32[]{:S(2)}) %collective-permute-start.13) | collective-permute-done | bytes 131104 | tf_op jit(solution)/shard_map/ppermute | solution.py:44
  73.0 1.6 %copy-done.1 = bf16[4,2048,128]{2,1,0:T(8,128)(2,1)S(1)} copy-done((bf16[4,2048,128]{2,1,0:T(8,128)(2,1)S(1)}, bf16[4,2048,128]{2,1,0:T(8,128)(2,1)}, u32[]{:S(2)}) %copy-start.1) | copy-done | bytes 2097176
  74.6 0.7 shard_map.199
  75.3 0.9 copy-done.2
  76.2 0.5 shard_map.200
  76.7 0.6 collective-permute-start.17
  77.3 0.0 collective-permute-done.14.refs_7_
  77.3 0.5 shard_map.201
  77.8 0.5 copy-done.4
  78.3 0.4 shard_map.202
  78.8 0.0 collective-permute-done.15.refs_3_
  78.8 2.5 %collective-permute-done.17.refs_5_ = bf16[128,256]{1,0:T(8,128)(2,1)S(1)} collective-permute-done((bf16[128,256]{1,0:T(8,128)(2,1)S(1)}, bf16[128,256]{1,0:T(8,128)(2,1)S(1)}, u32[]{:S(2)}, u32[]{:S(2)}) %collective-permute-start.17) | collective-permute-done | bytes 65568 | tf_op jit(solution)/shard_map/ppermute | solution.py:44
  81.3 1.4 %shard_map.203 = (bf16[128,512]{1,0:T(8,128)(2,1)S(1)}, bf16[128,512]{1,0:T(8,128)(2,1)S(1)}) custom-call(f32[4,256,128]{2,1,0:T(8,128)S(1)} %get-tuple-element.71.refs_3_.refs_0_, f32[256,512]{1,0:T(8,128)S(1)} %get-tuple-element.81.refs_1_, f32[256,512]{1,0:T(8,128)S(1)} %get-tuple-element.82.refs_2_, ...), custom_call_target="tpu_custom_call" | custom-call | tf_op jit(solution)/shard_map/pallas_call | solution.py:420
  82.7 0.1 collective-permute-start.18
  82.8 0.0 copy-start.6
  82.8 0.6 collective-permute-start.19
  83.3 3.9 %collective-permute-done.19.refs_5_ = bf16[128,256]{1,0:T(8,128)(2,1)S(1)} collective-permute-done((bf16[128,256]{1,0:T(8,128)(2,1)S(1)}, bf16[128,256]{1,0:T(8,128)(2,1)S(1)}, u32[]{:S(2)}, u32[]{:S(2)}) %collective-permute-start.19) | collective-permute-done | bytes 65568 | tf_op jit(solution)/shard_map/ppermute | solution.py:44
  87.3 1.4 %shard_map.204 = (bf16[128,512]{1,0:T(8,128)(2,1)S(1)}, bf16[128,512]{1,0:T(8,128)(2,1)S(1)}) custom-call(f32[4,256,128]{2,1,0:T(8,128)S(1)} %get-tuple-element.71.refs_3_.refs_0_, f32[256,512]{1,0:T(8,128)S(1)} %get-tuple-element.81.refs_1_, f32[256,512]{1,0:T(8,128)S(1)} %get-tuple-element.82.refs_2_, ...), custom_call_target="tpu_custom_call" | custom-call | tf_op jit(solution)/shard_map/pallas_call | solution.py:420
  88.7 0.1 collective-permute-start.20
  88.8 1.3 %collective-permute-done.20 = bf16[128,512]{1,0:T(8,128)(2,1)S(1)} collective-permute-done((bf16[128,512]{1,0:T(8,128)(2,1)S(1)}, bf16[128,512]{1,0:T(8,128)(2,1)S(1)}, u32[]{:S(2)}, u32[]{:S(2)}) %collective-permute-start.20) | collective-permute-done | bytes 131104 | tf_op jit(solution)/shard_map/ppermute | solution.py:44
  90.1 14.7 %all_to_all.10.refs_1_ = bf16[8,32,512]{2,1,0:T(8,128)(2,1)S(1)} all-to-all(bf16[8,32,512]{2,1,0:T(8,128)(2,1)S(1)} %bitcast.28), channel_id=1, replica_groups=mesh['sp'=8,'tp'=4] {'sp'}, dimensions={0} | all-to-all | bytes 524288 | tf_op jit(solution)/shard_map/all_to_all | solution.py:584
  104.9 0.9 shard_map.205
  (27 shorter events, 0.3 us)
Async XLA Ops:
  1.3 8.1 %collective-permute-start = (bf16[64,640]{1,0:T(8,128)(2,1)S(1)}, bf16[64,640]{1,0:T(8,128)(2,1)S(1)}, u32[]{:S(2)}, u32[]{:S(2)}) collective-permute-start(bf16[64,640]{1,0:T(8,128)(2,1)S(1)} %get-tuple-element.48.refs_1_.refs_5_), channel_id=1, source_target_pairs={{0,24},{4,28},{8,16},{12,20},{16,8},{20,12},{24,0},{28,4},{1,25},{... | collective-permute-start | bytes 245768 | tf_op jit(solution)/shard_map/ppermute | solution.py:44
  6.5 6.9 %collective-permute-start.1 = (bf16[64,640]{1,0:T(8,128)(2,1)S(1)}, bf16[64,640]{1,0:T(8,128)(2,1)S(1)}, u32[]{:S(2)}, u32[]{:S(2)}) collective-permute-start(bf16[64,640]{1,0:T(8,128)(2,1)S(1)} %get-tuple-element.48.refs_1_.refs_5_), channel_id=1, source_target_pairs={{0,16},{4,20},{8,24},{12,28},{16,0},{20,4},{24,8},{28,12},{1,17},{... | collective-permute-start | bytes 245768 | tf_op jit(solution)/shard_map/ppermute | solution.py:44
  6.5 8.4 %collective-permute-start.3 = (bf16[64,640]{1,0:T(8,128)(2,1)S(1)}, bf16[64,640]{1,0:T(8,128)(2,1)S(1)}, u32[]{:S(2)}, u32[]{:S(2)}) collective-permute-start(bf16[64,640]{1,0:T(8,128)(2,1)S(1)} %get-tuple-element.48.refs_1_.refs_5_), channel_id=1, source_target_pairs={{0,4},{4,0},{8,12},{12,8},{16,20},{20,16},{24,28},{28,24},{1,5},{5... | collective-permute-start | bytes 245768 | tf_op jit(solution)/shard_map/ppermute | solution.py:44
  13.3 6.0 %collective-permute-start.5 = (bf16[2,64,640]{2,1,0:T(8,128)(2,1)S(1)}, bf16[2,64,640]{2,1,0:T(8,128)(2,1)S(1)}, u32[]{:S(2)}, u32[]{:S(2)}) collective-permute-start(bf16[2,64,640]{2,1,0:T(8,128)(2,1)S(1)} %pad_maximum_fusion.3), channel_id=1, source_target_pairs={{0,4},{4,0},{8,12},{12,8},{16,20},{20,16},{24,28},{28,24},{1,5},{5... | collective-permute-start | bytes 491528 | tf_op jit(solution)/shard_map/ppermute | solution.py:44
  14.9 4.4 %collective-permute-start.4 = (bf16[64,640]{1,0:T(8,128)(2,1)S(1)}, bf16[64,640]{1,0:T(8,128)(2,1)S(1)}, u32[]{:S(2)}, u32[]{:S(2)}) collective-permute-start(bf16[64,640]{1,0:T(8,128)(2,1)S(1)} %collective-permute-done.3), channel_id=1, source_target_pairs={{0,8},{4,12},{8,0},{12,4},{16,24},{20,28},{24,16},{28,20},{1,9},{5... | collective-permute-start | bytes 245768 | tf_op jit(solution)/shard_map/ppermute | solution.py:44
  14.9 5.3 %collective-permute-start.2 = (bf16[64,640]{1,0:T(8,128)(2,1)S(1)}, bf16[64,640]{1,0:T(8,128)(2,1)S(1)}, u32[]{:S(2)}, u32[]{:S(2)}) collective-permute-start(bf16[64,640]{1,0:T(8,128)(2,1)S(1)} %get-tuple-element.48.refs_1_.refs_5_), channel_id=1, source_target_pairs={{0,8},{4,12},{8,0},{12,4},{16,24},{20,28},{24,16},{28,20},{1,9},{5... | collective-permute-start | bytes 245768 | tf_op jit(solution)/shard_map/ppermute | solution.py:44
  19.4 7.1 %collective-permute-start.7 = (bf16[4,64,640]{2,1,0:T(8,128)(2,1)S(1)}, bf16[4,64,640]{2,1,0:T(8,128)(2,1)S(1)}, u32[]{:S(2)}, u32[]{:S(2)}) collective-permute-start(bf16[4,64,640]{2,1,0:T(8,128)(2,1)S(1)} %pad_maximum_fusion.refs_3_.refs_5_), channel_id=1, source_target_pairs={{0,1},{1,0},{2,3},{3,2},{4,5},{5,4},{6,7},{7,6},{8,9},{9,8},{10,11... | collective-permute-start | bytes 983048 | tf_op jit(solution)/shard_map/ppermute | solution.py:44
  20.3 4.9 %collective-permute-start.6 = (bf16[3,64,640]{2,1,0:T(8,128)(2,1)S(1)}, bf16[3,64,640]{2,1,0:T(8,128)(2,1)S(1)}, u32[]{:S(2)}, u32[]{:S(2)}) collective-permute-start(bf16[3,64,640]{2,1,0:T(8,128)(2,1)S(1)} %pad_maximum_fusion.2.refs_2_.refs_6_), channel_id=1, source_target_pairs={{0,1},{1,0},{2,3},{3,2},{4,5},{5,4},{6,7},{7,6},{8,9},{9,8},{10,11... | collective-permute-start | bytes 737288 | tf_op jit(solution)/shard_map/ppermute | solution.py:44
  22.8 0.8 copy-start.8
  23.6 0.8 copy-start.9
  27.7 3.4 %copy-start.7 = (s32[128]{0:T(128)S(1)}, s32[128]{0:T(128)}, u32[]{:S(2)}) copy-start(s32[128]{0:T(128)} %param.33) | copy-start | bytes 1540
  27.7 1.7 %collective-permute-start.8 = (bf16[2,128,512]{2,1,0:T(8,128)(2,1)S(1)}, bf16[2,128,512]{2,1,0:T(8,128)(2,1)S(1)}, u32[]{:S(2)}, u32[]{:S(2)}) collective-permute-start(bf16[2,128,512]{2,1,0:T(8,128)(2,1)S(1)} %get-tuple-element.67), channel_id=1, source_target_pairs={{0,1},{1,0},{2,3},{3,2},{4,5},{5,4},{6,7},{7,6},{8,9},{9,8},{10,11... | collective-permute-start | bytes 786440 | tf_op jit(solution)/shard_map/ppermute | solution.py:44
  29.5 7.3 %collective-permute-start.9 = (bf16[128,512]{1,0:T(8,128)(2,1)S(1)}, bf16[128,512]{1,0:T(8,128)(2,1)S(1)}, u32[]{:S(2)}, u32[]{:S(2)}) collective-permute-start(bf16[128,512]{1,0:T(8,128)(2,1)S(1)} %get-tuple-element.69), channel_id=1, source_target_pairs={{0,2},{1,3},{2,0},{3,1},{4,6},{5,7},{6,4},{7,5},{8,10},{9,11},{10,... | collective-permute-start | bytes 393224 | tf_op jit(solution)/shard_map/ppermute | solution.py:44
  34.0 1.3 %copy-start = (bf16[4,2048,128]{2,1,0:T(8,128)(2,1)}, bf16[4,2048,128]{2,1,0:T(8,128)(2,1)S(1)}, u32[]{:S(2)}) copy-start(bf16[4,2048,128]{2,1,0:T(8,128)(2,1)S(1)} %get-tuple-element.75.refs_2_) | copy-start | bytes 6291460
  35.4 1.3 %copy-start.3 = (bf16[512,2048]{1,0:T(8,128)(2,1)}, bf16[512,2048]{1,0:T(8,128)(2,1)S(1)}, u32[]{:S(2)}) copy-start(bf16[512,2048]{1,0:T(8,128)(2,1)S(1)} %get-tuple-element.72.refs_0_) | copy-start | bytes 6291460
  37.7 0.7 copy-start.5
  38.3 13.1 %all-to-all-start = ((bf16[8,32,512]{2,1,0:T(8,128)(2,1)}), bf16[8,32,512]{2,1,0:T(8,128)(2,1)S(1)}, u32[]{:S(2)}, u32[]{:S(2)}) async-start(bf16[8,32,512]{2,1,0:T(8,128)(2,1)} %get-tuple-element.76), calls=%async_computation | async-start | bytes 524288 | tf_op jit(solution)/shard_map/all_to_all | solution.py:551
  42.3 36.5 %collective-permute-start.15 = (bf16[256,1024]{1,0:T(8,128)(2,1)}, bf16[256,1024]{1,0:T(8,128)(2,1)S(1)}, u32[]{:S(2)}, u32[]{:S(2)}) collective-permute-start(bf16[256,1024]{1,0:T(8,128)(2,1)} %copy-done.9), channel_id=1, source_target_pairs={{0,2},{1,3},{2,0},{3,1},{4,6},{5,7},{6,4},{7,5},{8,10},{9,11},{10,... | collective-permute-start | bytes 1572872 | tf_op jit(solution)/shard_map/ppermute | solution.py:44
  42.8 36.0 %collective-permute-start.16 = (bf16[256,1024]{1,0:T(8,128)(2,1)}, bf16[256,1024]{1,0:T(8,128)(2,1)}, u32[]{:S(2)}, u32[]{:S(2)}) collective-permute-start(bf16[256,1024]{1,0:T(8,128)(2,1)} %copy-done.8), channel_id=1, source_target_pairs={{0,2},{1,3},{2,0},{3,1},{4,6},{5,7},{6,4},{7,5},{8,10},{9,11},{10,... | collective-permute-start | bytes 1572872 | tf_op jit(solution)/shard_map/ppermute | solution.py:44
  51.5 21.5 %collective-permute-start.10 = (bf16[256,512]{1,0:T(8,128)(2,1)S(1)}, bf16[256,512]{1,0:T(8,128)(2,1)S(1)}, u32[]{:S(2)}, u32[]{:S(2)}) collective-permute-start(bf16[256,512]{1,0:T(8,128)(2,1)S(1)} %bitcast.19), channel_id=1, source_target_pairs={{0,1},{1,0},{2,3},{3,2},{4,5},{5,4},{6,7},{7,6},{8,9},{9,8},{10,11... | collective-permute-start | bytes 786440 | tf_op jit(solution)/shard_map/ppermute | solution.py:44
  51.5 19.8 %collective-permute-start.11 = (bf16[128,512]{1,0:T(8,128)(2,1)S(1)}, bf16[128,512]{1,0:T(8,128)(2,1)S(1)}, u32[]{:S(2)}, u32[]{:S(2)}) collective-permute-start(bf16[128,512]{1,0:T(8,128)(2,1)S(1)} %bitcast.34), channel_id=1, source_target_pairs={{0,2},{1,3},{2,0},{3,1},{4,6},{5,7},{6,4},{7,5},{8,10},{9,11},{10,... | collective-permute-start | bytes 393224 | tf_op jit(solution)/shard_map/ppermute | solution.py:44
  52.1 20.9 %collective-permute-start.13 = (bf16[128,512]{1,0:T(8,128)(2,1)S(1)}, bf16[128,512]{1,0:T(8,128)(2,1)S(1)}, u32[]{:S(2)}, u32[]{:S(2)}) collective-permute-start(bf16[128,512]{1,0:T(8,128)(2,1)S(1)} %bitcast.33), channel_id=1, source_target_pairs={{0,2},{1,3},{2,0},{3,1},{4,6},{5,7},{6,4},{7,5},{8,10},{9,11},{10,... | collective-permute-start | bytes 393224 | tf_op jit(solution)/shard_map/ppermute | solution.py:44
  71.3 4.0 %collective-permute-start.12 = (bf16[128,512]{1,0:T(8,128)(2,1)S(1)}, bf16[128,512]{1,0:T(8,128)(2,1)S(1)}, u32[]{:S(2)}, u32[]{:S(2)}) collective-permute-start(bf16[128,512]{1,0:T(8,128)(2,1)S(1)} %collective-permute-done.11.refs_6_), channel_id=1, source_target_pairs={{0,1},{1,0},{2,3},{3,2},{4,5},{5,4},{6,7},{7,6},{8,9},{9,8},{10,11... | collective-permute-start | bytes 393224 | tf_op jit(solution)/shard_map/ppermute | solution.py:44
  73.0 4.3 %collective-permute-start.14 = (bf16[128,512]{1,0:T(8,128)(2,1)S(1)}, bf16[128,512]{1,0:T(8,128)(2,1)S(1)}, u32[]{:S(2)}, u32[]{:S(2)}) collective-permute-start(bf16[128,512]{1,0:T(8,128)(2,1)S(1)} %collective-permute-done.13.refs_6_), channel_id=1, source_target_pairs={{0,1},{1,0},{2,3},{3,2},{4,5},{5,4},{6,7},{7,6},{8,9},{9,8},{10,11... | collective-permute-start | bytes 393224 | tf_op jit(solution)/shard_map/ppermute | solution.py:44
  73.0 1.6 %copy-start.1 = (bf16[4,2048,128]{2,1,0:T(8,128)(2,1)S(1)}, bf16[4,2048,128]{2,1,0:T(8,128)(2,1)}, u32[]{:S(2)}) copy-start(bf16[4,2048,128]{2,1,0:T(8,128)(2,1)} %copy-done) | copy-start | bytes 6291460
  74.6 1.6 %copy-start.2 = (bf16[4,2048,128]{2,1,0:T(8,128)(2,1)S(1)}, bf16[4,2048,128]{2,1,0:T(8,128)(2,1)}, u32[]{:S(2)}) copy-start(bf16[4,2048,128]{2,1,0:T(8,128)(2,1)} %copy-done) | copy-start | bytes 6291460
  76.7 1.6 %copy-start.4 = (bf16[512,2048]{1,0:T(8,128)(2,1)S(1)}, bf16[512,2048]{1,0:T(8,128)(2,1)}, u32[]{:S(2)}) copy-start(bf16[512,2048]{1,0:T(8,128)(2,1)} %copy-done.3) | copy-start | bytes 6291460
  76.7 4.6 %collective-permute-start.17 = (bf16[128,256]{1,0:T(8,128)(2,1)S(1)}, bf16[128,256]{1,0:T(8,128)(2,1)S(1)}, u32[]{:S(2)}, u32[]{:S(2)}) collective-permute-start(bf16[128,256]{1,0:T(8,128)(2,1)S(1)} %get-tuple-element.85), channel_id=1, source_target_pairs={{0,2},{1,3},{2,0},{3,1},{4,6},{5,7},{6,4},{7,5},{8,10},{9,11},{10,... | collective-permute-start | bytes 196616 | tf_op jit(solution)/shard_map/ppermute | solution.py:44
  82.7 6.0 %collective-permute-start.18 = (bf16[128,512]{1,0:T(8,128)(2,1)S(1)}, bf16[128,512]{1,0:T(8,128)(2,1)S(1)}, u32[]{:S(2)}, u32[]{:S(2)}) collective-permute-start(bf16[128,512]{1,0:T(8,128)(2,1)S(1)} %get-tuple-element.87), channel_id=1, source_target_pairs={{0,1},{1,0},{2,3},{3,2},{4,5},{5,4},{6,7},{7,6},{8,9},{9,8},{10,11... | collective-permute-start | bytes 393224 | tf_op jit(solution)/shard_map/ppermute | solution.py:44
  82.8 22.1 %copy-start.6 = (bf16[128,512]{1,0:T(8,128)(2,1)S(1)}, bf16[128,512]{1,0:T(8,128)(2,1)}, u32[]{:S(2)}) copy-start(bf16[128,512]{1,0:T(8,128)(2,1)} %copy-done.5) | copy-start | bytes 393220
  82.8 4.5 %collective-permute-start.19 = (bf16[128,256]{1,0:T(8,128)(2,1)S(1)}, bf16[128,256]{1,0:T(8,128)(2,1)S(1)}, u32[]{:S(2)}, u32[]{:S(2)}) collective-permute-start(bf16[128,256]{1,0:T(8,128)(2,1)S(1)} %get-tuple-element.88), channel_id=1, source_target_pairs={{0,2},{1,3},{2,0},{3,1},{4,6},{5,7},{6,4},{7,5},{8,10},{9,11},{10,... | collective-permute-start | bytes 196616 | tf_op jit(solution)/shard_map/ppermute | solution.py:44
  88.7 1.4 %collective-permute-start.20 = (bf16[128,512]{1,0:T(8,128)(2,1)S(1)}, bf16[128,512]{1,0:T(8,128)(2,1)S(1)}, u32[]{:S(2)}, u32[]{:S(2)}) collective-permute-start(bf16[128,512]{1,0:T(8,128)(2,1)S(1)} %get-tuple-element.90), channel_id=1, source_target_pairs={{0,1},{1,0},{2,3},{3,2},{4,5},{5,4},{6,7},{7,6},{8,9},{9,8},{10,11... | collective-permute-start | bytes 393224 | tf_op jit(solution)/shard_map/ppermute | solution.py:44
